TPU v7x, 512 devices: a whole 4x4x16 slice. The times are simulated.
512 devices in a mesh: kv: 16 (over y, x), tp: 32 (over z, core).
Axes of the slice: x: 4, y: 4, z: 16, core: 2. Of those that a mesh axis runs over, the one named last changes fastest.
Arguments:
- tokens: bfloat16 [256, 4096], P('tp', 'kv'), may hold values from -100 to 100
- state: float32 [256, 32, 128, 128], P('kv', 'tp'), may hold values from -3 to 3
- gain_pre: bfloat16 [4096], P('kv'), may hold values from 0.099609375 to 1.8984375
- w_gate_pre: bfloat16 [4096, 11264], P('kv', 'tp'), may hold values from -0.09375 to 0.09375
- w_up_pre: bfloat16 [4096, 11264], P('kv', 'tp'), may hold values from -0.09375 to 0.09375
- w_down_pre: bfloat16 [11264, 4096], P('tp', 'kv'), may hold values from -0.109375 to 0.109375
- gain_mix: bfloat16 [4096], P('kv'), may hold values from 0.099609375 to 1.8984375
- w_query: bfloat16 [4096, 4096], P('kv', 'tp'), may hold values from -0.09375 to 0.09375
- w_key: bfloat16 [4096, 4096], P('kv', 'tp'), may hold values from -0.09375 to 0.09375
- w_value: bfloat16 [4096, 4096], P('kv', 'tp'), may hold values from -0.09375 to 0.09375
- w_decay: bfloat16 [4096, 32], P('kv'), may hold values from -0.09375 to 0.09375
- w_blend: bfloat16 [4096, 32], P('kv'), may hold values from -0.09375 to 0.09375
- decay_base: float32 [32], P('tp'), may hold values from -3 to 0.7
- decay_shift: float32 [32], P('tp'), may hold values from -2 to 0.5
- head_gain: bfloat16 [128], replicated, may hold values from 0.099609375 to 1.8984375
- w_out: bfloat16 [4096, 4096], P('tp', 'kv'), may hold values from -0.09375 to 0.09375
- gain_post: bfloat16 [4096], P('kv'), may hold values from 0.099609375 to 1.8984375
- w_gate_post: bfloat16 [4096, 11264], P('kv', 'tp'), may hold values from -0.09375 to 0.09375
- w_up_post: bfloat16 [4096, 11264], P('kv', 'tp'), may hold values from -0.09375 to 0.09375
- w_down_post: bfloat16 [11264, 4096], P('tp', 'kv'), may hold values from -0.109375 to 0.109375
Outputs:
- result: bfloat16 [256, 4096], P('tp', 'kv')
- new_state: float32 [256, 32, 128, 128], P('kv', 'tp')
All inputs are finite; a program needn't handle non-finite values.
Results may differ from a plain program's by a relative error of at most 0.015.
Values may be sent and summed in bfloat16 or wider, within the bound.
No kernel may reach another device: no remote copies, remote signals or barrier semaphores. Data moves between devices by JAX's collectives and lax.ppermute only.
A program may use at most 64 MiB of HBM per device.

v0:
```python
import jax
import jax.numpy as jnp
from jax import lax
from jax.sharding import Mesh
from jax.sharding import PartitionSpec as P

D = 4096
KV = ("kv_0", "kv_1")


EPS = 1e-06


def copy_for_each(x, axis):
    length = lax.axis_size(axis)
    return lax.all_to_all(jnp.broadcast_to(x[None], (length, *x.shape)), axis, 0, 0, tiled=True)


def joined_along(parts, dim):
    lengths = list(parts.shape[1:])
    lengths[dim] *= parts.shape[0]
    return jnp.moveaxis(parts, 0, dim).reshape(lengths)


def gathered_copies(x, axis, dim):
    parts = copy_for_each(x, axis)
    return joined_along(parts, dim)


def over_axes(x, axes):
    for axis in axes:
        x = lax.psum(x, axis)
    return x


def cut_along(x, dim, length):
    before, after = (x.shape[:dim], x.shape[dim + 1 :])
    return jnp.moveaxis(x.reshape(*before, length, -1, *after), dim, 0)


def sent_and_summed(x, axis, dim):
    length = lax.axis_size(axis)
    parts = lax.all_to_all(cut_along(x, dim, length), axis, 0, 0, tiled=True)
    return jnp.sum(parts.astype(jnp.float32), axis=0)


def in_one_piece(arrays, axis, dim, along):
    widths = [a.shape[along] for a in arrays]
    both = jnp.concatenate(arrays, axis=along)
    result = sent_and_summed(both, axis, dim)
    return tuple(jnp.split(result, [sum(widths[:k]) for k in range(1, len(widths))], axis=along))


def sent_together(arrays, axis, dim, along):
    both = jnp.concatenate(arrays, axis=along)
    result, at, outs = (lax.psum_scatter(both, axis, scatter_dimension=dim, tiled=True), 0, [])
    for a in arrays:
        outs.append(lax.slice_in_dim(result, at, at + a.shape[along], axis=along))
        at += a.shape[along]
    return tuple(outs)


def spread(own_rows):
    return gathered_copies(own_rows, "tp", 0)


def inverse_rms(stream):
    values = stream.astype(jnp.float32)
    squares = over_axes(jnp.sum(values * values, axis=1), KV)
    return lax.rsqrt(squares / D + EPS)[:, None]


def gained(stream, gain_vec):
    return (stream.astype(jnp.float32) * gain_vec.astype(jnp.float32)).astype(jnp.bfloat16)


def residual_add(stream, branch, weight):
    return (stream.astype(jnp.float32) + weight * branch).astype(jnp.bfloat16)


def unit_rows(values):
    return values * lax.rsqrt(jnp.sum(values * values, axis=-1, keepdims=True) + EPS)


def kv_rows(values):
    count = values.shape[0] // lax.axis_size(KV)
    return lax.dynamic_slice_in_dim(values, lax.axis_index(KV) * count, count, 0)


def half_block(stream, gain_vec, w_gate, w_up, w_down):
    factor = inverse_rms(stream)
    scaled = gained(stream, gain_vec)
    gate_part = jnp.dot(scaled, w_gate, preferred_element_type=jnp.float32)
    up_part = jnp.dot(scaled, w_up, preferred_element_type=jnp.float32)
    gate_sum, up_sum = in_one_piece(
        (gate_part.astype(jnp.bfloat16), up_part.astype(jnp.bfloat16)), KV, 0, 1
    )
    own_factor = kv_rows(factor)
    hidden = (jax.nn.silu(own_factor * gate_sum) * (own_factor * up_sum)).astype(jnp.bfloat16)
    return jnp.dot(gathered_copies(hidden, KV, 0), w_down, preferred_element_type=jnp.float32)


def settle(partial_value):
    return sent_and_summed(partial_value.astype(jnp.bfloat16), "tp", 0)


def advance(own_rows, partial_value, weight):
    own_rows = residual_add(own_rows, settle(partial_value), weight)
    return (spread(own_rows), own_rows)


def on_device(
    tokens,
    state,
    gain_pre,
    w_gate_pre,
    w_up_pre,
    w_down_pre,
    gain_mix,
    w_query,
    w_key,
    w_value,
    w_decay,
    w_blend,
    decay_base,
    decay_shift,
    head_gain,
    w_out,
    gain_post,
    w_gate_post,
    w_up_post,
    w_down_post,
):
    own_rows = tokens
    stream = spread(own_rows)
    partial_value = half_block(stream, gain_pre, w_gate_pre, w_up_pre, w_down_pre)
    stream, own_rows = advance(own_rows, partial_value, 0.5)
    factor = inverse_rms(stream)
    scaled = gained(stream, gain_mix)
    queries, keys_new, values_new, decay_in, blend_in = tuple(
        (
            part.astype(jnp.float32)
            for part in sent_together(
                (
                    jnp.dot(scaled, w_query, preferred_element_type=jnp.float32).astype(
                        jnp.bfloat16
                    ),
                    jnp.dot(scaled, w_key, preferred_element_type=jnp.float32).astype(jnp.bfloat16),
                    jnp.dot(scaled, w_value, preferred_element_type=jnp.float32).astype(
                        jnp.bfloat16
                    ),
                    jnp.dot(scaled, w_decay, preferred_element_type=jnp.float32).astype(
                        jnp.bfloat16
                    ),
                    jnp.dot(scaled, w_blend, preferred_element_type=jnp.float32).astype(
                        jnp.bfloat16
                    ),
                ),
                KV,
                0,
                1,
            )
        )
    )
    own_factor = kv_rows(factor)
    seqs = state.shape[0]
    heads_dev = state.shape[1]
    head_dim = state.shape[3]
    queries = unit_rows((own_factor * queries).reshape(seqs, heads_dev, head_dim)) * head_dim ** (
        -0.5
    )
    keys_unit = unit_rows((own_factor * keys_new).reshape(seqs, heads_dev, head_dim))
    values_new = (own_factor * values_new).reshape(seqs, heads_dev, head_dim)
    head_start = lax.axis_index("tp") * heads_dev
    decay_in = lax.dynamic_slice_in_dim(own_factor * decay_in, head_start, heads_dev, 1)
    blend_in = lax.dynamic_slice_in_dim(own_factor * blend_in, head_start, heads_dev, 1)
    log_rate = -jnp.exp(decay_base) * jax.nn.softplus(decay_in + decay_shift)
    rate = jnp.exp(log_rate)
    beta = jax.nn.sigmoid(blend_in)
    recalled = jnp.einsum("bhk,bhkv->bhv", keys_unit, state, precision=lax.Precision.HIGHEST)
    correction = beta[:, :, None] * (values_new - rate[:, :, None] * recalled)
    new_state = (
        rate[:, :, None, None] * state + keys_unit[:, :, :, None] * correction[:, :, None, :]
    )
    read_out = jnp.einsum("bhk,bhkv->bhv", queries, new_state, precision=lax.Precision.HIGHEST)
    normed = read_out * lax.rsqrt(jnp.mean(read_out * read_out, axis=2, keepdims=True) + EPS)
    normed = (
        (normed * head_gain.astype(jnp.float32))
        .astype(jnp.bfloat16)
        .reshape(seqs, heads_dev * head_dim)
    )
    partial_value = jnp.dot(
        gathered_copies(normed, KV, 0), w_out, preferred_element_type=jnp.float32
    )
    stream, own_rows = advance(own_rows, partial_value, 1.0)
    partial_value = half_block(stream, gain_post, w_gate_post, w_up_post, w_down_post)
    result = residual_add(own_rows, settle(partial_value), 0.5)
    return (result, new_state)


def solution(mesh):
    finer = Mesh(mesh.devices.reshape(4, 4, mesh.shape["tp"]), ("kv_0", "kv_1", "tp"))
    in_specs = (
        P("tp", KV),
        P(KV, "tp", None, None),
        P(KV),
        P(KV, "tp"),
        P(KV, "tp"),
        P("tp", KV),
        P(KV),
        P(KV, "tp"),
        P(KV, "tp"),
        P(KV, "tp"),
        P(KV, None),
        P(KV, None),
        P("tp"),
        P("tp"),
        P(),
        P("tp", KV),
        P(KV),
        P(KV, "tp"),
        P(KV, "tp"),
        P("tp", KV),
    )
    out_specs = (P("tp", KV), P(KV, "tp", None, None))
    return jax.shard_map(
        on_device, mesh=finer, in_specs=in_specs, out_specs=out_specs, check_vma=False
    )
```

profile of v0, /device:TPU:1, one launch (start us, length us, event | category | flops | bytes accessed | tf_op | source)
XLA Modules:
  0.0 338.1 jit_solution(18254645089981805368)
XLA Ops:
  7.2 1.4 broadcast_in_dim.12
  8.6 16.7 %all-to-all-start = ((bf16[32,8,256]{2,1,0:T(8,128)(2,1)}), bf16[32,8,256]{2,1,0:T(8,128)(2,1)S(1)}, u32[]{:S(2)}, u32[]{:S(2)}) async-start(bf16[32,8,256]{2,1,0:T(8,128)(2,1)} %broadcast_in_dim.12), calls=%async_computation | async-start | bytes 262144 | tf_op jit(solution)/shard_map/all_to_all | solution.py:16
  26.0 15.2 %all-to-all-done = bf16[32,8,256]{2,1,0:T(8,128)(2,1)S(1)} async-done(((bf16[32,8,256]{2,1,0:T(8,128)(2,1)}), bf16[32,8,256]{2,1,0:T(8,128)(2,1)S(1)}, u32[]{:S(2)}, u32[]{:S(2)}) %all-to-all-start) | async-done | bytes 131104 | tf_op jit(solution)/shard_map/all_to_all | solution.py:16
  42.6 6.8 %all-to-all-start.1 = ((bf16[16,16,704]{2,1,0:T(8,128)(2,1)}), bf16[16,16,704]{2,1,0:T(8,128)(2,1)S(1)}, u32[]{:S(2)}, u32[]{:S(2)}) async-start(bf16[16,16,704]{2,1,0:T(8,128)(2,1)} %bitcast.1), calls=%async_computation.1 | async-start | bytes 786432 | tf_op jit(solution)/shard_map/all_to_all | solution.py:43
  49.6 9.6 %psum.42 = f32[256]{0:T(256)S(1)} all-reduce(f32[256]{0:T(256)S(1)} %reduce_sum.106), channel_id=1, replica_groups=mesh['kv_0'=4,'kv_1'=4,'tp'=32] {'kv_0'}, use_global_device_ids=true, to_apply=%region_1.0 | all-reduce | flops 256 | bytes 2048 | tf_op jit(solution)/shard_map/psum | solution.py:32
  59.2 8.0 %psum.43 = f32[256]{0:T(256)S(1)} all-reduce(f32[256]{0:T(256)S(1)} %psum.42), channel_id=1, replica_groups=mesh['kv_0'=4,'kv_1'=4,'tp'=32] {'kv_1'}, use_global_device_ids=true, to_apply=%region_2.0 | all-reduce | flops 256 | bytes 2048 | tf_op jit(solution)/shard_map/psum | solution.py:32
  67.5 10.1 %all_to_all.55 = bf16[16,16,352]{2,1,0:T(8,128)(2,1)S(1)} all-to-all(bf16[16,16,352]{2,1,0:T(8,128)(2,1)S(1)} %broadcast_in_dim.13), channel_id=1, replica_groups=mesh['kv_0'=4,'kv_1'=4,'tp'=32] {'kv_0','kv_1'}, dimensions={0} | all-to-all | bytes 360448 | tf_op jit(solution)/shard_map/all_to_all | solution.py:16
  77.8 25.3 %all_to_all.56 = bf16[32,8,256]{2,1,0:T(8,128)(2,1)S(1)} all-to-all(bf16[32,8,256]{2,1,0:T(8,128)(2,1)S(1)} %fusion), channel_id=1, replica_groups=mesh['kv_0'=4,'kv_1'=4,'tp'=32] {'tp'}, dimensions={0} | all-to-all | bytes 262144 | tf_op jit(solution)/shard_map/all_to_all | solution.py:43
  104.5 5.0 %all-to-all-start.4 = ((bf16[32,8,256]{2,1,0:T(8,128)(2,1)}), bf16[32,8,256]{2,1,0:T(8,128)(2,1)S(1)}, u32[]{:S(2)}, u32[]{:S(2)}) async-start(bf16[32,8,256]{2,1,0:T(8,128)(2,1)} %broadcast_in_dim.14), calls=%async_computation.4 | async-start | bytes 262144 | tf_op jit(solution)/shard_map/all_to_all | solution.py:16
  109.6 16.1 %all-to-all-done.4 = bf16[32,8,256]{2,1,0:T(8,128)(2,1)S(1)} async-done(((bf16[32,8,256]{2,1,0:T(8,128)(2,1)}), bf16[32,8,256]{2,1,0:T(8,128)(2,1)S(1)}, u32[]{:S(2)}, u32[]{:S(2)}) %all-to-all-start.4) | async-done | bytes 131104 | tf_op jit(solution)/shard_map/all_to_all | solution.py:16
  129.8 6.9 %psum.44 = f32[256]{0:T(256)S(1)} all-reduce(f32[256]{0:T(256)S(1)} %reduce_sum.110), channel_id=1, replica_groups=mesh['kv_0'=4,'kv_1'=4,'tp'=32] {'kv_0'}, use_global_device_ids=true, to_apply=%region_6.7 | all-reduce | flops 256 | bytes 2048 | tf_op jit(solution)/shard_map/psum | solution.py:32
  136.8 7.4 %psum.45 = f32[256]{0:T(256)S(1)} all-reduce(f32[256]{0:T(256)S(1)} %psum.44), channel_id=1, replica_groups=mesh['kv_0'=4,'kv_1'=4,'tp'=32] {'kv_1'}, use_global_device_ids=true, to_apply=%region_7.8 | all-reduce | flops 256 | bytes 2048 | tf_op jit(solution)/shard_map/psum | solution.py:32
  144.2 58.5 %reduce-scatter.4.cloned.1.call-done = bf16[16,448]{1,0:T(8,128)(2,1)} async-done(((bf16[256,448]{1,0:T(8,128)(2,1)}), bf16[16,448]{1,0:T(8,128)(2,1)}) %reduce-scatter.4.cloned.1.call-update) | async-done | bytes 14352 | tf_op jit(solution)/shard_map/reduce_scatter | solution.py:56
  204.5 1.0 fusion.10
  206.0 1.0 fusion.8
  207.3 10.9 %all_to_all.57 = bf16[16,16,128]{2,1,0:T(8,128)(2,1)S(1)} all-to-all(bf16[16,16,128]{2,1,0:T(8,128)(2,1)S(1)} %broadcast_in_dim.15), channel_id=1, replica_groups=mesh['kv_0'=4,'kv_1'=4,'tp'=32] {'kv_0','kv_1'}, dimensions={0} | all-to-all | bytes 131072 | tf_op jit(solution)/shard_map/all_to_all | solution.py:16
  218.3 32.0 %all_to_all.58 = bf16[32,8,256]{2,1,0:T(8,128)(2,1)S(1)} all-to-all(bf16[32,8,256]{2,1,0:T(8,128)(2,1)S(1)} %fusion.2), channel_id=1, replica_groups=mesh['kv_0'=4,'kv_1'=4,'tp'=32] {'tp'}, dimensions={0} | all-to-all | bytes 262144 | tf_op jit(solution)/shard_map/all_to_all | solution.py:43
  251.0 5.2 %all-to-all-start.7 = ((bf16[32,8,256]{2,1,0:T(8,128)(2,1)}), bf16[32,8,256]{2,1,0:T(8,128)(2,1)S(1)}, u32[]{:S(2)}, u32[]{:S(2)}) async-start(bf16[32,8,256]{2,1,0:T(8,128)(2,1)} %broadcast_in_dim.16), calls=%async_computation.7 | async-start | bytes 262144 | tf_op jit(solution)/shard_map/all_to_all | solution.py:16
  256.3 16.2 %all-to-all-done.7 = bf16[32,8,256]{2,1,0:T(8,128)(2,1)S(1)} async-done(((bf16[32,8,256]{2,1,0:T(8,128)(2,1)}), bf16[32,8,256]{2,1,0:T(8,128)(2,1)S(1)}, u32[]{:S(2)}, u32[]{:S(2)}) %all-to-all-start.7) | async-done | bytes 131104 | tf_op jit(solution)/shard_map/all_to_all | solution.py:16
  273.9 3.6 %all-to-all-start.8 = ((bf16[16,16,704]{2,1,0:T(8,128)(2,1)}), bf16[16,16,704]{2,1,0:T(8,128)(2,1)S(1)}, u32[]{:S(2)}, u32[]{:S(2)}) async-start(bf16[16,16,704]{2,1,0:T(8,128)(2,1)} %bitcast.22), calls=%async_computation.8 | async-start | bytes 786432 | tf_op jit(solution)/shard_map/all_to_all | solution.py:43
  277.7 9.7 %psum.46 = f32[256]{0:T(256)S(1)} all-reduce(f32[256]{0:T(256)S(1)} %reduce_sum.116), channel_id=1, replica_groups=mesh['kv_0'=4,'kv_1'=4,'tp'=32] {'kv_0'}, use_global_device_ids=true, to_apply=%region_14.15 | all-reduce | flops 256 | bytes 2048 | tf_op jit(solution)/shard_map/psum | solution.py:32
  287.3 8.5 %psum.47 = f32[256]{0:T(256)S(1)} all-reduce(f32[256]{0:T(256)S(1)} %psum.46), channel_id=1, replica_groups=mesh['kv_0'=4,'kv_1'=4,'tp'=32] {'kv_1'}, use_global_device_ids=true, to_apply=%region_15.16 | all-reduce | flops 256 | bytes 2048 | tf_op jit(solution)/shard_map/psum | solution.py:32
  296.1 9.9 %all_to_all.59 = bf16[16,16,352]{2,1,0:T(8,128)(2,1)S(1)} all-to-all(bf16[16,16,352]{2,1,0:T(8,128)(2,1)S(1)} %broadcast_in_dim.17), channel_id=1, replica_groups=mesh['kv_0'=4,'kv_1'=4,'tp'=32] {'kv_0','kv_1'}, dimensions={0} | all-to-all | bytes 360448 | tf_op jit(solution)/shard_map/all_to_all | solution.py:16
  306.3 24.3 %all_to_all.60 = bf16[32,8,256]{2,1,0:T(8,128)(2,1)S(1)} all-to-all(bf16[32,8,256]{2,1,0:T(8,128)(2,1)S(1)} %fusion.1), channel_id=1, replica_groups=mesh['kv_0'=4,'kv_1'=4,'tp'=32] {'tp'}, dimensions={0} | all-to-all | bytes 262144 | tf_op jit(solution)/shard_map/all_to_all | solution.py:43
  (105 shorter events, 13.1 us)
Async XLA Ops:
  7.2 34.0 %copy-start = (bf16[256,352]{0,1:T(8,128)(2,1)S(1)}, bf16[256,352]{0,1:T(8,128)(2,1)}, u32[]{:S(2)}) copy-start(bf16[256,352]{0,1:T(8,128)(2,1)} %param.24) | copy-start | bytes 540676
  8.6 32.6 %all-to-all-start = ((bf16[32,8,256]{2,1,0:T(8,128)(2,1)}), bf16[32,8,256]{2,1,0:T(8,128)(2,1)S(1)}, u32[]{:S(2)}, u32[]{:S(2)}) async-start(bf16[32,8,256]{2,1,0:T(8,128)(2,1)} %broadcast_in_dim.12), calls=%async_computation | async-start | bytes 262144 | tf_op jit(solution)/shard_map/all_to_all | solution.py:16
  26.0 15.4 %copy-start.3 = (bf16[256,352]{0,1:T(8,128)(2,1)S(1)}, bf16[256,352]{0,1:T(8,128)(2,1)}, u32[]{:S(2)}) copy-start(bf16[256,352]{0,1:T(8,128)(2,1)} %param.23) | copy-start | bytes 540676
  42.6 24.7 %all-to-all-start.1 = ((bf16[16,16,704]{2,1,0:T(8,128)(2,1)}), bf16[16,16,704]{2,1,0:T(8,128)(2,1)S(1)}, u32[]{:S(2)}, u32[]{:S(2)}) async-start(bf16[16,16,704]{2,1,0:T(8,128)(2,1)} %bitcast.1), calls=%async_computation.1 | async-start | bytes 786432 | tf_op jit(solution)/shard_map/all_to_all | solution.py:43
  67.5 10.1 %copy-start.4 = (bf16[352,256]{1,0:T(8,128)(2,1)S(1)}, bf16[352,256]{1,0:T(8,128)(2,1)}, u32[]{:S(2)}) copy-start(bf16[352,256]{1,0:T(8,128)(2,1)} %param.25) | copy-start | bytes 540676
  103.1 0.7 copy-start.12
  104.5 5.1 %copy-start.17 = (bf16[256]{0:T(256)(128)(2,1)S(1)}, bf16[256]{0:T(256)(128)(2,1)}, u32[]{:S(2)}) copy-start(bf16[256]{0:T(256)(128)(2,1)} %param.26) | copy-start | bytes 1540
  104.5 21.2 %copy-start.13 = (bf16[256,128]{1,0:T(8,128)(2,1)S(1)}, bf16[256,128]{1,0:T(8,128)(2,1)}, u32[]{:S(2)}) copy-start(bf16[256,128]{1,0:T(8,128)(2,1)} %param.27) | copy-start | bytes 196612
  104.5 21.7 %copy-start.9 = (bf16[256,128]{1,0:T(8,128)(2,1)S(1)}, bf16[256,128]{1,0:T(8,128)(2,1)}, u32[]{:S(2)}) copy-start(bf16[256,128]{1,0:T(8,128)(2,1)} %param.29) | copy-start | bytes 196612
  104.5 21.9 %copy-start.14 = (bf16[256,32]{0,1:T(8,128)(2,1)S(1)}, bf16[256,32]{0,1:T(8,128)(2,1)}, u32[]{:S(2)}) copy-start(bf16[256,32]{0,1:T(8,128)(2,1)} %param.30) | copy-start | bytes 49156
  104.5 22.1 %copy-start.15 = (bf16[256,32]{0,1:T(8,128)(2,1)S(1)}, bf16[256,32]{0,1:T(8,128)(2,1)}, u32[]{:S(2)}) copy-start(bf16[256,32]{0,1:T(8,128)(2,1)} %param.31) | copy-start | bytes 49156
  104.5 21.2 %all-to-all-start.4 = ((bf16[32,8,256]{2,1,0:T(8,128)(2,1)}), bf16[32,8,256]{2,1,0:T(8,128)(2,1)S(1)}, u32[]{:S(2)}, u32[]{:S(2)}) async-start(bf16[32,8,256]{2,1,0:T(8,128)(2,1)} %broadcast_in_dim.14), calls=%async_computation.4 | async-start | bytes 262144 | tf_op jit(solution)/shard_map/all_to_all | solution.py:16
  109.5 93.3 %reduce-scatter.4.cloned.1.call-start = ((), (), s32[]{:S(2)}) async-start(), calls=%async_computation.12 | async-start | bytes 278528 | tf_op jit(solution)/shard_map/reduce_scatter | solution.py:56
  109.5 16.4 %copy-start.8 = (bf16[256,128]{1,0:T(8,128)(2,1)S(1)}, bf16[256,128]{1,0:T(8,128)(2,1)}, u32[]{:S(2)}) copy-start(bf16[256,128]{1,0:T(8,128)(2,1)} %param.28) | copy-start | bytes 196612
  109.6 95.0 %copy-start.1 = (f32[16,1,128,128]{3,2,1,0:T(8,128)S(1)}, f32[16,1,128,128]{3,2,1,0:T(8,128)}, u32[]{:S(2)}) copy-start(f32[16,1,128,128]{3,2,1,0:T(8,128)} %param.21) | copy-start | bytes 3145732
  203.6 0.7 copy-start.11
  206.0 45.0 %copy-start.2 = (f32[16,1,128,128]{3,2,1,0:T(8,128)}, f32[16,1,128,128]{3,2,1,0:T(8,128)S(1)}, u32[]{:S(2)}) copy-start(f32[16,1,128,128]{3,2,1,0:T(8,128)S(1)} %multiply_add_fusion) | copy-start | bytes 3145732
  207.3 10.9 %copy-start.10 = (bf16[128,256]{1,0:T(8,128)(2,1)S(1)}, bf16[128,256]{1,0:T(8,128)(2,1)}, u32[]{:S(2)}) copy-start(bf16[128,256]{1,0:T(8,128)(2,1)} %param.35) | copy-start | bytes 196612
  250.4 22.1 %copy-start.5 = (bf16[256,352]{0,1:T(8,128)(2,1)S(1)}, bf16[256,352]{0,1:T(8,128)(2,1)}, u32[]{:S(2)}) copy-start(bf16[256,352]{0,1:T(8,128)(2,1)} %param.38) | copy-start | bytes 540676
  251.0 5.2 %copy-start.19 = (bf16[256]{0:T(256)(128)(2,1)S(1)}, bf16[256]{0:T(256)(128)(2,1)}, u32[]{:S(2)}) copy-start(bf16[256]{0:T(256)(128)(2,1)} %param.36) | copy-start | bytes 1540
  251.0 21.4 %all-to-all-start.7 = ((bf16[32,8,256]{2,1,0:T(8,128)(2,1)}), bf16[32,8,256]{2,1,0:T(8,128)(2,1)S(1)}, u32[]{:S(2)}, u32[]{:S(2)}) async-start(bf16[32,8,256]{2,1,0:T(8,128)(2,1)} %broadcast_in_dim.16), calls=%async_computation.7 | async-start | bytes 262144 | tf_op jit(solution)/shard_map/all_to_all | solution.py:16
  256.3 16.4 %copy-start.6 = (bf16[256,352]{0,1:T(8,128)(2,1)S(1)}, bf16[256,352]{0,1:T(8,128)(2,1)}, u32[]{:S(2)}) copy-start(bf16[256,352]{0,1:T(8,128)(2,1)} %param.37) | copy-start | bytes 540676
  273.9 22.0 %all-to-all-start.8 = ((bf16[16,16,704]{2,1,0:T(8,128)(2,1)}), bf16[16,16,704]{2,1,0:T(8,128)(2,1)S(1)}, u32[]{:S(2)}, u32[]{:S(2)}) async-start(bf16[16,16,704]{2,1,0:T(8,128)(2,1)} %bitcast.22), calls=%async_computation.8 | async-start | bytes 786432 | tf_op jit(solution)/shard_map/all_to_all | solution.py:43
  296.1 9.9 %copy-start.7 = (bf16[352,256]{1,0:T(8,128)(2,1)S(1)}, bf16[352,256]{1,0:T(8,128)(2,1)}, u32[]{:S(2)}) copy-start(bf16[352,256]{1,0:T(8,128)(2,1)} %param.39) | copy-start | bytes 540676
  (2 other events, 1.3 us)
Sparse Core Ops, SparseCore 0:
  127.7 74.9 reduce-scatter.3
where the time goes:
time: 339 us; the launch traced here: 338 us
  blocking collectives  163 us (48%)
  waiting for transfers between devices  106 us (31%)
  starting transfers between devices  37.3 us (11%)
  between operations  15.8 us (5%)
  local copies, waits for them, and re-layouts  9.52 us (3%)
  matrix products  4.5 us (1%)
    all_to_all x3, blocking collectives, sent_and_summed(): parts = lax.all_to_all(cut_along(x, dim, length), axis, 0, 0, tiled=True)  81.6 us
    reduce_scatter x1, waiting for transfers between devices, sent_together(): lax.psum_scatter(both, axis, scatter_dimension=dim, tiled=True)  58.5 us
    psum x6, blocking collectives, over_axes(): x = lax.psum(x, axis)  50.1 us
    all_to_all x3, waiting for transfers between devices, copy_for_each(): lax.all_to_all(jnp.broadcast_to(x[None], (length, *x.shape)), axis, 0, 0,...  47.4 us
    all_to_all x3, blocking collectives, copy_for_each(): lax.all_to_all(jnp.broadcast_to(x[None], (length, *x.shape)), axis, 0, 0,...  30.9 us
    all_to_all x3, starting transfers between devices, copy_for_each(): lax.all_to_all(jnp.broadcast_to(x[None], (length, *x.shape)), axis, 0, 0,...  26.9 us
    all_to_all x2, starting transfers between devices, sent_and_summed(): parts = lax.all_to_all(cut_along(x, dim, length), axis, 0, 0, tiled=True)  10.3 us
  transfers between devices with their start and end apart: 6, of which 4 were waited for; matrix products, arithmetic and copies ran while one was open for 0% of the time, Pallas kernels for 0%

commit v1 on v0

--- a/solution.py
+++ b/solution.py
@@ -27,12 +27,6 @@
     return joined_along(parts, dim)
 
 
-def over_axes(x, axes):
-    for axis in axes:
-        x = lax.psum(x, axis)
-    return x
-
-
 def cut_along(x, dim, length):
     before, after = (x.shape[:dim], x.shape[dim + 1 :])
     return jnp.moveaxis(x.reshape(*before, length, -1, *after), dim, 0)
@@ -44,30 +38,28 @@
     return jnp.sum(parts.astype(jnp.float32), axis=0)
 
 
-def in_one_piece(arrays, axis, dim, along):
-    widths = [a.shape[along] for a in arrays]
-    both = jnp.concatenate(arrays, axis=along)
-    result = sent_and_summed(both, axis, dim)
-    return tuple(jnp.split(result, [sum(widths[:k]) for k in range(1, len(widths))], axis=along))
-
-
-def sent_together(arrays, axis, dim, along):
-    both = jnp.concatenate(arrays, axis=along)
-    result, at, outs = (lax.psum_scatter(both, axis, scatter_dimension=dim, tiled=True), 0, [])
-    for a in arrays:
-        outs.append(lax.slice_in_dim(result, at, at + a.shape[along], axis=along))
-        at += a.shape[along]
-    return tuple(outs)
+def split_widths(joined, widths):
+    return tuple(jnp.split(joined, [sum(widths[:k]) for k in range(1, len(widths))], axis=1))
 
 
 def spread(own_rows):
     return gathered_copies(own_rows, "tp", 0)
 
 
-def inverse_rms(stream):
+def square_sums(stream):
     values = stream.astype(jnp.float32)
-    squares = over_axes(jnp.sum(values * values, axis=1), KV)
-    return lax.rsqrt(squares / D + EPS)[:, None]
+    rest = jnp.sum(values * values, axis=1, keepdims=True)
+    pieces = []
+    for _ in range(3):
+        piece = lax.reduce_precision(rest, exponent_bits=8, mantissa_bits=7)
+        pieces.append(piece.astype(jnp.bfloat16))
+        rest = rest - piece
+    return pieces
+
+
+def inverse_rms(summed_pieces):
+    squares = jnp.sum(summed_pieces, axis=1, keepdims=True)
+    return lax.rsqrt(squares / D + EPS)
 
 
 def gained(stream, gain_vec):
@@ -82,20 +74,26 @@
     return values * lax.rsqrt(jnp.sum(values * values, axis=-1, keepdims=True) + EPS)
 
 
-def kv_rows(values):
-    count = values.shape[0] // lax.axis_size(KV)
-    return lax.dynamic_slice_in_dim(values, lax.axis_index(KV) * count, count, 0)
-
-
 def half_block(stream, gain_vec, w_gate, w_up, w_down):
-    factor = inverse_rms(stream)
     scaled = gained(stream, gain_vec)
     gate_part = jnp.dot(scaled, w_gate, preferred_element_type=jnp.float32)
     up_part = jnp.dot(scaled, w_up, preferred_element_type=jnp.float32)
-    gate_sum, up_sum = in_one_piece(
-        (gate_part.astype(jnp.bfloat16), up_part.astype(jnp.bfloat16)), KV, 0, 1
-    )
-    own_factor = kv_rows(factor)
+    gate_sum, up_sum, squares = split_widths(
+        sent_and_summed(
+            jnp.concatenate(
+                [
+                    gate_part.astype(jnp.bfloat16),
+                    up_part.astype(jnp.bfloat16),
+                    *square_sums(stream),
+                ],
+                axis=1,
+            ),
+            KV,
+            0,
+        ),
+        (w_gate.shape[1], w_up.shape[1], 3),
+    )
+    own_factor = inverse_rms(squares)
     hidden = (jax.nn.silu(own_factor * gate_sum) * (own_factor * up_sum)).astype(jnp.bfloat16)
     return jnp.dot(gathered_copies(hidden, KV, 0), w_down, preferred_element_type=jnp.float32)
 
@@ -135,34 +133,26 @@
     stream = spread(own_rows)
     partial_value = half_block(stream, gain_pre, w_gate_pre, w_up_pre, w_down_pre)
     stream, own_rows = advance(own_rows, partial_value, 0.5)
-    factor = inverse_rms(stream)
     scaled = gained(stream, gain_mix)
-    queries, keys_new, values_new, decay_in, blend_in = tuple(
-        (
-            part.astype(jnp.float32)
-            for part in sent_together(
-                (
-                    jnp.dot(scaled, w_query, preferred_element_type=jnp.float32).astype(
-                        jnp.bfloat16
+    weights = (w_query, w_key, w_value, w_decay, w_blend)
+    queries, keys_new, values_new, decay_in, blend_in, squares = split_widths(
+        sent_and_summed(
+            jnp.concatenate(
+                [
+                    *(
+                        jnp.dot(scaled, w, preferred_element_type=jnp.float32).astype(jnp.bfloat16)
+                        for w in weights
                     ),
-                    jnp.dot(scaled, w_key, preferred_element_type=jnp.float32).astype(jnp.bfloat16),
-                    jnp.dot(scaled, w_value, preferred_element_type=jnp.float32).astype(
-                        jnp.bfloat16
-                    ),
-                    jnp.dot(scaled, w_decay, preferred_element_type=jnp.float32).astype(
-                        jnp.bfloat16
-                    ),
-                    jnp.dot(scaled, w_blend, preferred_element_type=jnp.float32).astype(
-                        jnp.bfloat16
-                    ),
-                ),
-                KV,
-                0,
-                1,
-            )
-        )
-    )
-    own_factor = kv_rows(factor)
+                    *square_sums(stream),
+                ],
+                axis=1,
+            ),
+            KV,
+            0,
+        ),
+        (*(w.shape[1] for w in weights), 3),
+    )
+    own_factor = inverse_rms(squares)
     seqs = state.shape[0]
     heads_dev = state.shape[1]
     head_dim = state.shape[3]

time: 339 us -> 232 us (0.68)
  waiting for transfers between devices: 106 us -> 53.8 us
  blocking collectives: 163 us -> 124 us
  between operations: 15.8 us -> 2.38 us
  starting transfers between devices: 37.3 us -> 30.3 us
  local copies, waits for them, and re-layouts: 9.52 us -> 13 us
    reduce_scatter x1 -> x0, waiting for transfers between devices: 58.5 us -> none  [sent_together(): lax.psum_scatter(both, axis, scatter_dimension=dim, tiled=True)]
    psum x6 -> x0, blocking collectives: 50.1 us -> none  [over_axes(): x = lax.psum(x, axis)]
    all_to_all x3 -> x5, blocking collectives: 81.6 us -> 94.3 us  [sent_and_summed(): parts = lax.all_to_all(cut_along(x, dim, length), axis, 0, 0, tiled=True)]
    all_to_all x2 -> x1, starting transfers between devices: 10.3 us -> 3.53 us  [sent_and_summed(): parts = lax.all_to_all(cut_along(x, dim, length), axis, 0, 0, tiled=True)]
    all_to_all x2 -> x1, waiting for transfers between devices: 0.01 us -> 5.67 us  [sent_and_summed(): parts = lax.all_to_all(cut_along(x, dim, length), axis, 0, 0, tiled=True)]
  transfers between devices with their start and end apart: 6 -> 4, of which waited for: 4 -> 4; matrix products, arithmetic and copies ran while one was open for 0% -> 0% of each run, Pallas kernels for 0% -> 0%
where the time goes in v1:
time: 232 us; the launch traced here: 231 us
  blocking collectives  124 us (53%)
  waiting for transfers between devices  53.8 us (23%)
  starting transfers between devices  30.3 us (13%)
  local copies, waits for them, and re-layouts  13 us (6%)
  matrix products  4.32 us (2%)
  other arithmetic  3.16 us (1%)
  between operations  2.38 us (1%)
    all_to_all x5, blocking collectives, sent_and_summed(): parts = lax.all_to_all(cut_along(x, dim, length), axis, 0, 0, tiled=True)  94.3 us
    all_to_all x3, waiting for transfers between devices, copy_for_each(): lax.all_to_all(jnp.broadcast_to(x[None], (length, *x.shape)), axis, 0, 0,...  48.2 us
    all_to_all x3, blocking collectives, copy_for_each(): lax.all_to_all(jnp.broadcast_to(x[None], (length, *x.shape)), axis, 0, 0,...  29.4 us
    all_to_all x3, starting transfers between devices, copy_for_each(): lax.all_to_all(jnp.broadcast_to(x[None], (length, *x.shape)), axis, 0, 0,...  26.8 us
    unnamed x38, local copies, waits for them, and re-layouts  5.88 us
    all_to_all x1, waiting for transfers between devices, sent_and_summed(): parts = lax.all_to_all(cut_along(x, dim, length), axis, 0, 0, tiled=True)  5.67 us
  transfers between devices with their start and end apart: 4, of which 4 were waited for; matrix products, arithmetic and copies ran while one was open for 0% of the time, Pallas kernels for 0%

profile of v1, /device:TPU:1, one launch (start us, length us, event | category | flops | bytes accessed | tf_op | source)
XLA Modules:
  0.0 230.6 jit_solution(15530631019709165113)
XLA Ops:
  0.6 1.4 broadcast_in_dim.12
  2.0 16.9 %all-to-all-start = ((bf16[32,8,256]{2,1,0:T(8,128)(2,1)}), bf16[32,8,256]{2,1,0:T(8,128)(2,1)S(1)}, u32[]{:S(2)}, u32[]{:S(2)}) async-start(bf16[32,8,256]{2,1,0:T(8,128)(2,1)} %broadcast_in_dim.12), calls=%async_computation | async-start | bytes 262144 | tf_op jit(solution)/shard_map/all_to_all | solution.py:16
  18.9 15.8 %all-to-all-done = bf16[32,8,256]{2,1,0:T(8,128)(2,1)S(1)} async-done(((bf16[32,8,256]{2,1,0:T(8,128)(2,1)}), bf16[32,8,256]{2,1,0:T(8,128)(2,1)S(1)}, u32[]{:S(2)}, u32[]{:S(2)}) %all-to-all-start) | async-done | bytes 131104 | tf_op jit(solution)/shard_map/all_to_all | solution.py:16
  36.0 0.7 copy-done.3
  37.4 14.8 %all_to_all.60 = bf16[16,16,707]{2,1,0:T(8,128)(2,1)S(1)} all-to-all(bf16[16,16,707]{2,1,0:T(8,128)(2,1)S(1)} %concatenate.32), channel_id=1, replica_groups=mesh['kv_0'=4,'kv_1'=4,'tp'=32] {'kv_0','kv_1'}, dimensions={0} | all-to-all | bytes 723968 | tf_op jit(solution)/shard_map/all_to_all | solution.py:37
  52.6 10.1 %all_to_all.61 = bf16[16,16,352]{2,1,0:T(8,128)(2,1)S(1)} all-to-all(bf16[16,16,352]{2,1,0:T(8,128)(2,1)S(1)} %broadcast_in_dim.13), channel_id=1, replica_groups=mesh['kv_0'=4,'kv_1'=4,'tp'=32] {'kv_0','kv_1'}, dimensions={0} | all-to-all | bytes 360448 | tf_op jit(solution)/shard_map/all_to_all | solution.py:16
  62.9 23.1 %all_to_all.62 = bf16[32,8,256]{2,1,0:T(8,128)(2,1)S(1)} all-to-all(bf16[32,8,256]{2,1,0:T(8,128)(2,1)S(1)} %fusion), channel_id=1, replica_groups=mesh['kv_0'=4,'kv_1'=4,'tp'=32] {'tp'}, dimensions={0} | all-to-all | bytes 262144 | tf_op jit(solution)/shard_map/all_to_all | solution.py:37
  86.7 0.7 broadcast_in_dim.14
  87.4 5.0 %all-to-all-start.4 = ((bf16[32,8,256]{2,1,0:T(8,128)(2,1)}), bf16[32,8,256]{2,1,0:T(8,128)(2,1)S(1)}, u32[]{:S(2)}, u32[]{:S(2)}) async-start(bf16[32,8,256]{2,1,0:T(8,128)(2,1)} %broadcast_in_dim.14), calls=%async_computation.4 | async-start | bytes 262144 | tf_op jit(solution)/shard_map/all_to_all | solution.py:16
  92.3 16.2 %all-to-all-done.4 = bf16[32,8,256]{2,1,0:T(8,128)(2,1)S(1)} async-done(((bf16[32,8,256]{2,1,0:T(8,128)(2,1)}), bf16[32,8,256]{2,1,0:T(8,128)(2,1)S(1)}, u32[]{:S(2)}, u32[]{:S(2)}) %all-to-all-start.4) | async-done | bytes 131104 | tf_op jit(solution)/shard_map/all_to_all | solution.py:16
  112.6 0.7 copy-done.10
  113.5 0.9 concatenate.38
  114.4 3.5 %all-to-all-start.5 = ((bf16[16,16,451]{2,1,0:T(8,128)(2,1)}), bf16[16,16,451]{2,1,0:T(8,128)(2,1)S(1)}, u32[]{:S(2)}, u32[]{:S(2)}) async-start(bf16[16,16,451]{2,1,0:T(8,128)(2,1)} %concatenate.38), calls=%async_computation.5 | async-start | bytes 524288 | tf_op jit(solution)/shard_map/all_to_all | solution.py:37
  119.9 5.7 %all-to-all-done.5 = bf16[16,16,451]{2,1,0:T(8,128)(2,1)S(1)} async-done(((bf16[16,16,451]{2,1,0:T(8,128)(2,1)}), bf16[16,16,451]{2,1,0:T(8,128)(2,1)S(1)}, u32[]{:S(2)}, u32[]{:S(2)}) %all-to-all-start.5) | async-done | bytes 230944 | tf_op jit(solution)/shard_map/all_to_all | solution.py:37
  126.2 1.0 fusion.5
  127.9 1.0 fusion.3
  129.1 9.4 %all_to_all.63 = bf16[16,16,128]{2,1,0:T(8,128)(2,1)S(1)} all-to-all(bf16[16,16,128]{2,1,0:T(8,128)(2,1)S(1)} %broadcast_in_dim.15), channel_id=1, replica_groups=mesh['kv_0'=4,'kv_1'=4,'tp'=32] {'kv_0','kv_1'}, dimensions={0} | all-to-all | bytes 131072 | tf_op jit(solution)/shard_map/all_to_all | solution.py:16
  138.7 22.4 %all_to_all.64 = bf16[32,8,256]{2,1,0:T(8,128)(2,1)S(1)} all-to-all(bf16[32,8,256]{2,1,0:T(8,128)(2,1)S(1)} %fusion.2), channel_id=1, replica_groups=mesh['kv_0'=4,'kv_1'=4,'tp'=32] {'tp'}, dimensions={0} | all-to-all | bytes 262144 | tf_op jit(solution)/shard_map/all_to_all | solution.py:37
  161.8 5.0 %all-to-all-start.8 = ((bf16[32,8,256]{2,1,0:T(8,128)(2,1)}), bf16[32,8,256]{2,1,0:T(8,128)(2,1)S(1)}, u32[]{:S(2)}, u32[]{:S(2)}) async-start(bf16[32,8,256]{2,1,0:T(8,128)(2,1)} %broadcast_in_dim.16), calls=%async_computation.8 | async-start | bytes 262144 | tf_op jit(solution)/shard_map/all_to_all | solution.py:16
  166.8 16.2 %all-to-all-done.8 = bf16[32,8,256]{2,1,0:T(8,128)(2,1)S(1)} async-done(((bf16[32,8,256]{2,1,0:T(8,128)(2,1)}), bf16[32,8,256]{2,1,0:T(8,128)(2,1)S(1)}, u32[]{:S(2)}, u32[]{:S(2)}) %all-to-all-start.8) | async-done | bytes 131104 | tf_op jit(solution)/shard_map/all_to_all | solution.py:16
  184.1 0.7 copy-done.6
  185.5 11.3 %all_to_all.65 = bf16[16,16,707]{2,1,0:T(8,128)(2,1)S(1)} all-to-all(bf16[16,16,707]{2,1,0:T(8,128)(2,1)S(1)} %concatenate.41), channel_id=1, replica_groups=mesh['kv_0'=4,'kv_1'=4,'tp'=32] {'kv_0','kv_1'}, dimensions={0} | all-to-all | bytes 723968 | tf_op jit(solution)/shard_map/all_to_all | solution.py:37
  197.2 9.9 %all_to_all.66 = bf16[16,16,352]{2,1,0:T(8,128)(2,1)S(1)} all-to-all(bf16[16,16,352]{2,1,0:T(8,128)(2,1)S(1)} %broadcast_in_dim.17), channel_id=1, replica_groups=mesh['kv_0'=4,'kv_1'=4,'tp'=32] {'kv_0','kv_1'}, dimensions={0} | all-to-all | bytes 360448 | tf_op jit(solution)/shard_map/all_to_all | solution.py:16
  207.4 22.6 %all_to_all.67 = bf16[32,8,256]{2,1,0:T(8,128)(2,1)S(1)} all-to-all(bf16[32,8,256]{2,1,0:T(8,128)(2,1)S(1)} %fusion.1), channel_id=1, replica_groups=mesh['kv_0'=4,'kv_1'=4,'tp'=32] {'tp'}, dimensions={0} | all-to-all | bytes 262144 | tf_op jit(solution)/shard_map/all_to_all | solution.py:37
  (108 shorter events, 13.4 us)
Async XLA Ops:
  0.6 34.9 %copy-start = (bf16[256,352]{0,1:T(8,128)(2,1)S(1)}, bf16[256,352]{0,1:T(8,128)(2,1)}, u32[]{:S(2)}) copy-start(bf16[256,352]{0,1:T(8,128)(2,1)} %param.24) | copy-start | bytes 540676
  2.0 16.9 %copy-start.15 = (bf16[256]{0:T(256)(128)(2,1)S(1)}, bf16[256]{0:T(256)(128)(2,1)}, u32[]{:S(2)}) copy-start(bf16[256]{0:T(256)(128)(2,1)} %param.22) | copy-start | bytes 1540
  2.0 32.7 %all-to-all-start = ((bf16[32,8,256]{2,1,0:T(8,128)(2,1)}), bf16[32,8,256]{2,1,0:T(8,128)(2,1)S(1)}, u32[]{:S(2)}, u32[]{:S(2)}) async-start(bf16[32,8,256]{2,1,0:T(8,128)(2,1)} %broadcast_in_dim.12), calls=%async_computation | async-start | bytes 262144 | tf_op jit(solution)/shard_map/all_to_all | solution.py:16
  35.8 0.9 copy-start.3
  52.6 10.1 %copy-start.4 = (bf16[352,256]{1,0:T(8,128)(2,1)S(1)}, bf16[352,256]{1,0:T(8,128)(2,1)}, u32[]{:S(2)}) copy-start(bf16[352,256]{1,0:T(8,128)(2,1)} %param.25) | copy-start | bytes 540676
  86.0 0.7 copy-start.12
  87.4 5.0 %copy-start.16 = (bf16[256]{0:T(256)(128)(2,1)S(1)}, bf16[256]{0:T(256)(128)(2,1)}, u32[]{:S(2)}) copy-start(bf16[256]{0:T(256)(128)(2,1)} %param.26) | copy-start | bytes 1540
  87.4 21.2 %all-to-all-start.4 = ((bf16[32,8,256]{2,1,0:T(8,128)(2,1)}), bf16[32,8,256]{2,1,0:T(8,128)(2,1)S(1)}, u32[]{:S(2)}, u32[]{:S(2)}) async-start(bf16[32,8,256]{2,1,0:T(8,128)(2,1)} %broadcast_in_dim.14), calls=%async_computation.4 | async-start | bytes 262144 | tf_op jit(solution)/shard_map/all_to_all | solution.py:16
  108.6 0.7 copy-start.13
  109.5 0.8 copy-start.14
  110.8 0.8 copy-start.8
  111.6 0.8 copy-start.9
  112.4 0.8 copy-start.10
  113.3 12.9 %copy-start.1 = (f32[16,1,128,128]{3,2,1,0:T(8,128)S(1)}, f32[16,1,128,128]{3,2,1,0:T(8,128)}, u32[]{:S(2)}) copy-start(f32[16,1,128,128]{3,2,1,0:T(8,128)} %param.21) | copy-start | bytes 3145732
  114.4 11.2 %all-to-all-start.5 = ((bf16[16,16,451]{2,1,0:T(8,128)(2,1)}), bf16[16,16,451]{2,1,0:T(8,128)(2,1)S(1)}, u32[]{:S(2)}, u32[]{:S(2)}) async-start(bf16[16,16,451]{2,1,0:T(8,128)(2,1)} %concatenate.38), calls=%async_computation.5 | async-start | bytes 524288 | tf_op jit(solution)/shard_map/all_to_all | solution.py:37
  119.2 0.7 copy-start.17
  127.8 33.9 %copy-start.2 = (f32[16,1,128,128]{3,2,1,0:T(8,128)}, f32[16,1,128,128]{3,2,1,0:T(8,128)S(1)}, u32[]{:S(2)}) copy-start(f32[16,1,128,128]{3,2,1,0:T(8,128)S(1)} %multiply_add_fusion) | copy-start | bytes 3145732
  129.1 9.4 %copy-start.11 = (bf16[128,256]{1,0:T(8,128)(2,1)S(1)}, bf16[128,256]{1,0:T(8,128)(2,1)}, u32[]{:S(2)}) copy-start(bf16[128,256]{1,0:T(8,128)(2,1)} %param.35) | copy-start | bytes 196612
  161.8 5.0 %copy-start.18 = (bf16[256]{0:T(256)(128)(2,1)S(1)}, bf16[256]{0:T(256)(128)(2,1)}, u32[]{:S(2)}) copy-start(bf16[256]{0:T(256)(128)(2,1)} %param.36) | copy-start | bytes 1540
  161.8 21.2 %all-to-all-start.8 = ((bf16[32,8,256]{2,1,0:T(8,128)(2,1)}), bf16[32,8,256]{2,1,0:T(8,128)(2,1)S(1)}, u32[]{:S(2)}, u32[]{:S(2)}) async-start(bf16[32,8,256]{2,1,0:T(8,128)(2,1)} %broadcast_in_dim.16), calls=%async_computation.8 | async-start | bytes 262144 | tf_op jit(solution)/shard_map/all_to_all | solution.py:16
  166.8 16.9 %copy-start.5 = (bf16[256,352]{0,1:T(8,128)(2,1)S(1)}, bf16[256,352]{0,1:T(8,128)(2,1)}, u32[]{:S(2)}) copy-start(bf16[256,352]{0,1:T(8,128)(2,1)} %param.38) | copy-start | bytes 540676
  184.0 0.9 copy-start.6
  197.2 9.9 %copy-start.7 = (bf16[352,256]{1,0:T(8,128)(2,1)S(1)}, bf16[352,256]{1,0:T(8,128)(2,1)}, u32[]{:S(2)}) copy-start(bf16[352,256]{1,0:T(8,128)(2,1)} %param.39) | copy-start | bytes 540676

commit v2 on v1

v2 whole, which is shorter than its diff:
```python
import jax
import jax.numpy as jnp
from jax import lax
from jax.sharding import Mesh
from jax.sharding import PartitionSpec as P

D = 4096
EPS = 1e-06
KV = ("kv_0", "kv_1")
TP = ("z", "core")
KVC = ("kv_0", "kv_1", "core")
ALL = ("kv_0", "kv_1", "z", "core")
BF16 = jnp.bfloat16
F32 = jnp.float32


def dot_nn(a, b):
    return jnp.dot(a, b, preferred_element_type=F32)


def dot_nt(a, b):
    return lax.dot_general(a, b, (((1,), (1,)), ((), ())), preferred_element_type=F32)


def exchanged(parts, axis):
    return lax.all_to_all(parts, axis, 0, 0, tiled=True)


def copies(x, axis):
    return exchanged(jnp.broadcast_to(x[None], (lax.axis_size(axis), *x.shape)), axis)


def summed(parts, axis):
    return jnp.sum(exchanged(parts, axis).astype(F32), axis=0)


def from_partner(x):
    return lax.ppermute(x, "core", [(0, 1), (1, 0)])


def turned(x):
    n = lax.axis_size("z")
    pairs = [
        ((k * n + z) * 2 + c, (z * n + k) * 2 + c)
        for k in range(n)
        for z in range(n)
        for c in range(2)
    ]
    return lax.ppermute(x, ALL, pairs)


def square_sums(stream):
    values = stream.astype(F32)
    rest = jnp.sum(values * values, axis=1, keepdims=True)
    pieces = []
    for _ in range(3):
        piece = lax.reduce_precision(rest, exponent_bits=8, mantissa_bits=7)
        pieces.append(piece.astype(BF16))
        rest = rest - piece
    return pieces


def inverse_rms(summed_pieces):
    squares = jnp.sum(summed_pieces, axis=1, keepdims=True)
    return lax.rsqrt(squares / D + EPS)


def gained(stream, gain_vec):
    return (stream.astype(F32) * gain_vec.astype(F32)).astype(BF16)


def residual_add(stream, branch, weight):
    return (stream.astype(F32) + weight * branch).astype(BF16)


def unit_rows(values):
    return values * lax.rsqrt(jnp.sum(values * values, axis=-1, keepdims=True) + EPS)


def gated(sums, half):
    factor = inverse_rms(sums[:, 2 * half :])
    gate, up = factor * sums[:, :half], factor * sums[:, half : 2 * half]
    return (jax.nn.silu(gate) * up).astype(BF16)


def on_device(
    tokens,
    state,
    gain_pre,
    w_gate_pre,
    w_up_pre,
    w_down_pre,
    gain_mix,
    w_query,
    w_key,
    w_value,
    w_decay,
    w_blend,
    decay_base,
    decay_shift,
    head_gain,
    w_out,
    gain_post,
    w_gate_post,
    w_up_post,
    w_down_post,
):
    n_kv = lax.axis_size(KV)
    rows, width = tokens.shape
    units = w_gate_pre.shape[1]
    head_dim = w_query.shape[1]
    core = lax.axis_index("core")

    later = jnp.concatenate([w_out, w_gate_post.T, w_up_post.T, w_down_post], axis=0)
    later = lax.all_gather(later, TP, axis=0, tiled=False)
    cuts = [0, head_dim, head_dim + units, head_dim + 2 * units, head_dim + 3 * units]
    w_out_all, w_gate_all, w_up_all, w_down_all = (
        later[:, a:b] for a, b in zip(cuts[:-1], cuts[1:], strict=True)
    )

    own = jnp.concatenate([w_gate_pre.T, w_up_pre.T, w_down_pre], axis=0)
    other = from_partner(own)
    stream = copies(tokens, "z").reshape(-1, width)
    scaled = gained(stream, gain_pre)
    gate_own, up_own = dot_nt(scaled, own[:units]), dot_nt(scaled, own[units : 2 * units])
    gate_other, up_other = (
        dot_nt(scaled, other[:units]),
        dot_nt(scaled, other[units : 2 * units]),
    )
    sent = jnp.concatenate(
        [*(p.astype(BF16) for p in (gate_own, gate_other, up_own, up_other)), *square_sums(stream)],
        axis=1,
    )
    hidden = gated(summed(sent.reshape(n_kv, rows, -1), KV), 2 * units)
    hidden = copies(hidden, KV).reshape(-1, 2 * units)
    w_down = jnp.concatenate([own[2 * units :], other[2 * units :]], axis=0)
    branch = summed(dot_nn(hidden, w_down).astype(BF16).reshape(n_kv, rows, width), "z")
    first = residual_add(tokens, branch, 0.5)

    own = jnp.concatenate([w_query, w_key, w_value], axis=1)
    other = from_partner(own)
    pair = 2 * lax.axis_index("z")
    gates = jnp.concatenate(
        [
            lax.dynamic_slice_in_dim(w_decay.T, pair, 2, 0),
            lax.dynamic_slice_in_dim(w_blend.T, pair, 2, 0),
        ],
        axis=0,
    )
    stream = copies(first, "z").reshape(-1, width)
    scaled = gained(stream, gain_mix)
    own_part, other_part = dot_nn(scaled, own).astype(BF16), dot_nn(scaled, other).astype(BF16)
    gate_part = dot_nt(scaled, gates).astype(BF16)
    pieces = square_sums(stream)
    sent = jnp.stack(
        [
            jnp.concatenate(
                [
                    jnp.where(core == to, own_part, other_part),
                    gate_part[:, to : to + 1],
                    gate_part[:, 2 + to : 3 + to],
                    *pieces,
                ],
                axis=1,
            ).reshape(n_kv, rows, -1)
            for to in range(2)
        ],
        axis=1,
    )
    got = exchanged(sent.reshape(2 * n_kv, rows, -1), KVC)
    got = jnp.sum(got.reshape(n_kv, 2 * rows, -1).astype(F32), axis=0)
    factor = inverse_rms(got[:, 3 * head_dim + 2 :])
    got = factor * got[:, : 3 * head_dim + 2]
    queries = unit_rows(got[:, :head_dim]) * head_dim**-0.5
    keys = unit_rows(got[:, head_dim : 2 * head_dim])
    values = got[:, 2 * head_dim : 3 * head_dim]
    decay_in = got[:, 3 * head_dim : 3 * head_dim + 1]
    blend_in = got[:, 3 * head_dim + 1 :]
    rate = jnp.exp(-jnp.exp(decay_base) * jax.nn.softplus(decay_in + decay_shift))
    beta = jax.nn.sigmoid(blend_in)
    held = state[:, 0]
    recalled = jnp.einsum("bk,bkv->bv", keys, held, precision=lax.Precision.HIGHEST)
    correction = beta * (values - rate * recalled)
    new_state = rate[:, :, None] * held + keys[:, :, None] * correction[:, None, :]
    read_out = jnp.einsum("bk,bkv->bv", queries, new_state, precision=lax.Precision.HIGHEST)
    normed = read_out * lax.rsqrt(jnp.mean(read_out * read_out, axis=1, keepdims=True) + EPS)
    normed = (normed * head_gain.astype(F32)).astype(BF16)
    normed = turned(normed).reshape(1, 2, rows, head_dim)
    normed = exchanged(
        jnp.broadcast_to(normed, (n_kv, 2, rows, head_dim)).reshape(2 * n_kv, rows, head_dim), KVC
    )
    branch = jnp.einsum("trk,tkn->rn", normed, w_out_all, preferred_element_type=F32)
    second = residual_add(first, branch, 1.0)

    scaled = gained(second, gain_post)
    gate_part = jnp.einsum("rk,tnk->rtn", scaled, w_gate_all, preferred_element_type=F32)
    up_part = jnp.einsum("rk,tnk->rtn", scaled, w_up_all, preferred_element_type=F32)
    sent = jnp.concatenate(
        [
            gate_part.astype(BF16).reshape(rows, n_kv, 2 * units),
            up_part.astype(BF16).reshape(rows, n_kv, 2 * units),
            jnp.broadcast_to(
                jnp.concatenate(square_sums(second), axis=1)[:, None], (rows, n_kv, 3)
            ),
        ],
        axis=2,
    )
    hidden = gated(summed(jnp.moveaxis(sent, 1, 0), KV), 2 * units)
    hidden = copies(hidden, KV).reshape(n_kv, rows, 2, units)
    branch = jnp.einsum(
        "krcu,kcun->rn",
        hidden,
        w_down_all.reshape(n_kv, 2, units, width),
        preferred_element_type=F32,
    )
    result = residual_add(second, branch, 0.5)
    return (result, new_state[:, None])


def solution(mesh):
    finer = Mesh(mesh.devices.reshape(4, 4, mesh.shape["tp"] // 2, 2), ALL)
    in_specs = (
        P(TP, KV),
        P(KV, TP, None, None),
        P(KV),
        P(KV, TP),
        P(KV, TP),
        P(TP, KV),
        P(KV),
        P(KV, TP),
        P(KV, TP),
        P(KV, TP),
        P(KV, None),
        P(KV, None),
        P(TP),
        P(TP),
        P(),
        P(TP, KV),
        P(KV),
        P(KV, TP),
        P(KV, TP),
        P(TP, KV),
    )
    out_specs = (P(TP, KV), P(KV, TP, None, None))
    return jax.shard_map(
        on_device, mesh=finer, in_specs=in_specs, out_specs=out_specs, check_vma=False
    )
```

time: 232 us -> 206 us (0.89)
  blocking collectives: 124 us -> 26.9 us
  starting transfers between devices: 30.3 us -> 71.2 us
  matrix products: 4.32 us -> 20.9 us
  between operations: 2.38 us -> 15.9 us
  waiting for transfers between devices: 53.8 us -> 47 us
  other arithmetic: 3.16 us -> 7.78 us
    all_to_all x8 -> x2, blocking collectives: 124 us -> 26.9 us  [exchanged(): return lax.all_to_all(parts, axis, 0, 0, tiled=True)]
    all_to_all x4 -> x7, starting transfers between devices: 30.3 us -> 61.8 us  [exchanged(): return lax.all_to_all(parts, axis, 0, 0, tiled=True)]
    dot_general x14, matrix products: 4.32 us -> 20.9 us  [the longest x1 4.31 us: on_device(): jnp.einsum('rk,tnk->rtn', scaled, w_up_all, preferred_element_type=F32)]
    ppermute x0 -> x3, starting transfers between devices: none -> 9.38 us  [the longest x2 8.71 us: from_partner(): return lax.ppermute(x, 'core', [(0, 1), (1, 0)])]
    all_to_all x4 -> x7, waiting for transfers between devices: 53.8 us -> 47 us  [exchanged(): return lax.all_to_all(parts, axis, 0, 0, tiled=True)]
    unnamed x38 -> x20, local copies, waits for them, and re-layouts: 5.88 us -> 0.08 us
    slice x0 -> x3, local copies, waits for them, and re-layouts: none -> 5.5 us  [the longest x1 5.45 us: on_device(): later[:, a:b]]
    concatenate x0 -> x3, other arithmetic: none -> 3.26 us  [the longest x1 2.03 us: on_device(): jnp.concatenate([w_out, w_gate_post.T, w_up_post.T, w_down_post], axis=0)]
  transfers between devices with their start and end apart: 4 -> 11, of which waited for: 4 -> 7; matrix products, arithmetic and copies ran while one was open for 0% -> 12% of each run, Pallas kernels for 0% -> 0%
where the time goes in v2:
time: 206 us; the launch traced here: 204 us
  starting transfers between devices  71.2 us (35%)
  waiting for transfers between devices  47 us (23%)
  blocking collectives  26.9 us (13%)
  matrix products  20.9 us (10%)
  between operations  15.9 us (8%)
  local copies, waits for them, and re-layouts  14.4 us (7%)
  other arithmetic  7.78 us (4%)
    all_to_all x7, starting transfers between devices, exchanged(): return lax.all_to_all(parts, axis, 0, 0, tiled=True)  61.8 us
    all_to_all x7, waiting for transfers between devices, exchanged(): return lax.all_to_all(parts, axis, 0, 0, tiled=True)  47 us
    all_to_all x2, blocking collectives, exchanged(): return lax.all_to_all(parts, axis, 0, 0, tiled=True)  26.9 us
    ppermute x2, starting transfers between devices, from_partner(): return lax.ppermute(x, 'core', [(0, 1), (1, 0)])  8.71 us
    slice x1, local copies, waits for them, and re-layouts, on_device(): later[:, a:b]  5.45 us
    dot_general x1, matrix products, on_device(): jnp.einsum('rk,tnk->rtn', scaled, w_up_all, preferred_element_type=F32)  4.31 us
    dot_general x1, matrix products, on_device(): jnp.einsum('rk,tnk->rtn', scaled, w_gate_all, preferred_element_type=F32)  4.3 us
  transfers between devices with their start and end apart: 11, of which 7 were waited for; matrix products, arithmetic and copies ran while one was open for 12% of the time, Pallas kernels for 0%

profile of v2, /device:TPU:1, one launch (start us, length us, event | category | flops | bytes accessed | tf_op | source)
XLA Modules:
  0.0 204.1 jit_solution(13035426626673182453)
XLA Ops:
  7.3 2.0 pad_maximum_fusion
  10.6 15.9 %all-to-all-start = ((bf16[16,8,256]{2,1,0:T(8,128)(2,1)}), bf16[16,8,256]{2,1,0:T(8,128)(2,1)S(1)}, u32[]{:S(2)}, u32[]{:S(2)}) async-start(bf16[16,8,256]{2,1,0:T(8,128)(2,1)} %broadcast_in_dim.14), calls=%async_computation | async-start | bytes 131072 | tf_op jit(solution)/shard_map/all_to_all | solution.py:26
  27.7 2.9 %collective-permute-start = (bf16[1056,256]{1,0:T(8,128)(2,1)S(1)}, bf16[1056,256]{1,0:T(8,128)(2,1)S(1)}, u32[]{:S(2)}, u32[]{:S(2)}) collective-permute-start(bf16[1056,256]{1,0:T(8,128)(2,1)S(1)} %pad_maximum_fusion.1), channel_id=1, source_target_pairs={{0,1},{1,0},{2,3},{3,2},{4,5},{5,4},{6,7},{7,6},{8,9},{9,8},{10,11... | collective-permute-start | bytes 1622024 | tf_op jit(solution)/shard_map/ppermute | solution.py:38
  31.3 6.8 %all-to-all-done = bf16[16,8,256]{2,1,0:T(8,128)(2,1)S(1)} async-done(((bf16[16,8,256]{2,1,0:T(8,128)(2,1)}), bf16[16,8,256]{2,1,0:T(8,128)(2,1)S(1)}, u32[]{:S(2)}, u32[]{:S(2)}) %all-to-all-start) | async-done | bytes 65568 | tf_op jit(solution)/shard_map/all_to_all | solution.py:26
  42.2 14.8 %all_to_all.45 = bf16[16,8,1411]{2,1,0:T(8,128)(2,1)S(1)} all-to-all(bf16[16,8,1411]{2,1,0:T(8,128)(2,1)S(1)} %concatenate.58), channel_id=1, replica_groups=mesh['kv_0'=4,'kv_1'=4,'z'=16,'core'=2] {'kv_0','kv_1'}, dimensions={0} | all-to-all | bytes 722432 | tf_op jit(solution)/shard_map/all_to_all | solution.py:26
  58.0 3.5 %all-to-all-start.2 = ((bf16[16,8,704]{2,1,0:T(8,128)(2,1)}), bf16[16,8,704]{2,1,0:T(8,128)(2,1)S(1)}, u32[]{:S(2)}, u32[]{:S(2)}) async-start(bf16[16,8,704]{2,1,0:T(8,128)(2,1)} %broadcast_in_dim.15), calls=%async_computation.2 | async-start | bytes 393216 | tf_op jit(solution)/shard_map/all_to_all | solution.py:26
  61.5 7.1 %all-to-all-done.2 = bf16[16,8,704]{2,1,0:T(8,128)(2,1)S(1)} async-done(((bf16[16,8,704]{2,1,0:T(8,128)(2,1)}), bf16[16,8,704]{2,1,0:T(8,128)(2,1)S(1)}, u32[]{:S(2)}, u32[]{:S(2)}) %all-to-all-start.2) | async-done | bytes 180256 | tf_op jit(solution)/shard_map/all_to_all | solution.py:26
  69.5 6.3 %all-to-all-start.3 = ((bf16[16,8,256]{2,1,0:T(8,128)(2,1)}), bf16[16,8,256]{2,1,0:T(8,128)(2,1)S(1)}, u32[]{:S(2)}, u32[]{:S(2)}) async-start(bf16[16,8,256]{2,1,0:T(8,128)(2,1)} %fusion.14), calls=%async_computation.3 | async-start | bytes 131072 | tf_op jit(solution)/shard_map/all_to_all | solution.py:26
  75.8 12.2 %all-to-all-done.3 = bf16[16,8,256]{2,1,0:T(8,128)(2,1)S(1)} async-done(((bf16[16,8,256]{2,1,0:T(8,128)(2,1)}), bf16[16,8,256]{2,1,0:T(8,128)(2,1)S(1)}, u32[]{:S(2)}, u32[]{:S(2)}) %all-to-all-start.3) | async-done | bytes 65568 | tf_op jit(solution)/shard_map/all_to_all | solution.py:26
  88.7 3.5 %all-to-all-start.4 = ((bf16[16,8,256]{2,1,0:T(8,128)(2,1)}), bf16[16,8,256]{2,1,0:T(8,128)(2,1)S(1)}, u32[]{:S(2)}, u32[]{:S(2)}) async-start(bf16[16,8,256]{2,1,0:T(8,128)(2,1)} %broadcast_in_dim.16), calls=%async_computation.4 | async-start | bytes 131072 | tf_op jit(solution)/shard_map/all_to_all | solution.py:26
  92.3 5.9 %collective-permute-start.1 = (bf16[256,384]{1,0:T(8,128)(2,1)S(1)}, bf16[256,384]{1,0:T(8,128)(2,1)S(1)}, u32[]{:S(2)}, u32[]{:S(2)}) collective-permute-start(bf16[256,384]{1,0:T(8,128)(2,1)S(1)} %constant_dynamic-update-slice_fusion), channel_id=1, source_target_pairs={{0,1},{1,0},{2,3},{3,2},{4,5},{5,4},{6,7},{7,6},{8,9},{9,8},{10,11... | collective-permute-start | bytes 589832 | tf_op jit(solution)/shard_map/ppermute | solution.py:38
  98.9 5.5 %all-to-all-done.4 = bf16[16,8,256]{2,1,0:T(8,128)(2,1)S(1)} async-done(((bf16[16,8,256]{2,1,0:T(8,128)(2,1)}), bf16[16,8,256]{2,1,0:T(8,128)(2,1)S(1)}, u32[]{:S(2)}, u32[]{:S(2)}) %all-to-all-start.4) | async-done | bytes 65568 | tf_op jit(solution)/shard_map/all_to_all | solution.py:26
  107.6 8.6 %all-to-all-start.5 = ((bf16[32,8,389]{2,1,0:T(8,128)(2,1)}), bf16[32,8,389]{2,1,0:T(8,128)(2,1)S(1)}, u32[]{:S(2)}, u32[]{:S(2)}) async-start(bf16[32,8,389]{2,1,0:T(8,128)(2,1)} %bitcast.18), calls=%async_computation.5 | async-start | bytes 524288 | tf_op jit(solution)/shard_map/all_to_all | solution.py:26
  117.6 7.6 %all-to-all-done.5 = bf16[32,8,389]{2,1,0:T(8,128)(2,1)S(1)} async-done(((bf16[32,8,389]{2,1,0:T(8,128)(2,1)}), bf16[32,8,389]{2,1,0:T(8,128)(2,1)S(1)}, u32[]{:S(2)}, u32[]{:S(2)}) %all-to-all-start.5) | async-done | bytes 199200 | tf_op jit(solution)/shard_map/all_to_all | solution.py:26
  129.6 20.4 %all-to-all-start.6 = ((bf16[32,8,128]{2,1,0:T(8,128)(2,1)}), bf16[32,8,128]{2,1,0:T(8,128)(2,1)S(1)}, u32[]{:S(2)}, u32[]{:S(2)}) async-start(bf16[32,8,128]{2,1,0:T(8,128)(2,1)} %bitcast.32), calls=%async_computation.6 | async-start | bytes 131072 | tf_op jit(solution)/shard_map/all_to_all | solution.py:26
  150.1 7.3 %all-to-all-done.6 = bf16[32,8,128]{2,1,0:T(8,128)(2,1)S(1)} async-done(((bf16[32,8,128]{2,1,0:T(8,128)(2,1)}), bf16[32,8,128]{2,1,0:T(8,128)(2,1)S(1)}, u32[]{:S(2)}, u32[]{:S(2)}) %all-to-all-start.6) | async-done | bytes 65568 | tf_op jit(solution)/shard_map/all_to_all | solution.py:26
  157.4 2.1 %multiply_reduce_fusion = (f32[8]{0:T(128)S(1)}, f32[8,256]{1,0:T(8,128)S(1)}) fusion(bf16[32,8,128]{2,1,0:T(8,128)(2,1)S(1)} %all-to-all-done.6, bf16[32,1184,256]{2,1,0:T(8,128)(2,1)} %bitcast.127, bf16[8,256]{1,0:T(8,128)(2,1)S(1)} %add_convert_fusion), kind=kOutput, calls=%fused_computation.87 | convolution fusion | flops 16789496 | bytes 2175008 | tf_op jit(solution)/shard_map/trk,tkn->rn/dot_general | solution.py:192
  159.5 4.3 %fusion.8 = bf16[8,32,352]{2,0,1:T(8,128)(2,1)S(1)} fusion(bf16[32,1184,256]{2,1,0:T(8,128)(2,1)} %bitcast.128, f32[8,256]{1,0:T(8,128)S(1)} %get-tuple-element.24, f32[256]{0:T(256)S(1)} %convert_element_type.259), kind=kOutput, calls=%fused_computation.8 | convolution fusion | flops 46231552 | bytes 5956608 | tf_op jit(solution)/shard_map/rk,tnk->rtn/dot_general | solution.py:196
  163.8 4.3 %fusion.11 = bf16[8,32,352]{2,0,1:T(8,128)(2,1)S(1)} fusion(bf16[32,1184,256]{2,1,0:T(8,128)(2,1)} %bitcast.129, f32[8,256]{1,0:T(8,128)S(1)} %get-tuple-element.24, f32[256]{0:T(256)S(1)} %convert_element_type.259), kind=kOutput, calls=%fused_computation.9 | convolution fusion | flops 46231552 | bytes 5956608 | tf_op jit(solution)/shard_map/rk,tnk->rtn/dot_general | solution.py:197
  169.1 12.1 %all_to_all.46 = bf16[16,8,1411]{2,1,0:T(8,128)(2,1)S(1)} all-to-all(bf16[16,8,1411]{2,1,0:T(8,128)(2,1)S(1)} %copy.166), channel_id=1, replica_groups=mesh['kv_0'=4,'kv_1'=4,'z'=16,'core'=2] {'kv_0','kv_1'}, dimensions={0} | all-to-all | bytes 722432 | tf_op jit(solution)/shard_map/all_to_all | solution.py:26
  182.2 3.5 %all-to-all-start.8 = ((bf16[16,8,704]{2,1,0:T(8,128)(2,1)}), bf16[16,8,704]{2,1,0:T(8,128)(2,1)S(1)}, u32[]{:S(2)}, u32[]{:S(2)}) async-start(bf16[16,8,704]{2,1,0:T(8,128)(2,1)} %broadcast_in_dim.20), calls=%async_computation.8 | async-start | bytes 393216 | tf_op jit(solution)/shard_map/all_to_all | solution.py:26
  185.8 1.3 multiply_add_fusion
  187.1 5.4 %slice.115 = bf16[32,352,256]{2,1,0:T(8,128)(2,1)} slice(bf16[32,1184,256]{2,1,0:T(8,128)(2,1)} %bitcast.130), slice={[0:32], [832:1184], [0:256]} | slice | bytes 11534336 | tf_op jit(solution)/shard_map/slice | solution.py:118
  193.2 4.1 %fusion.36 = bf16[8,256]{1,0:T(8,128)(2,1)} fusion(f32[8,256]{1,0:T(8,128)S(1)} %get-tuple-element.24, bf16[16,2,352,256]{3,2,1,0:T(8,128)(2,1)} %bitcast.126, bf16[16,8,2,352]{3,2,1,0:T(2,128)(2,1)S(1)} %reshape.282), kind=kOutput, calls=%fused_computation.25 | convolution fusion | flops 46143488 | bytes 5959680 | tf_op jit(solution)/shard_map/krcu,kcun->rn/dot_general | solution.py:210
  (110 shorter events, 20.6 us)
Async XLA Ops:
  7.2 80.9 %copy-start.5 = (bf16[8,256]{1,0:T(8,128)(2,1)S(1)}, bf16[8,256]{1,0:T(8,128)(2,1)}, u32[]{:S(2)}) copy-start(bf16[8,256]{1,0:T(8,128)(2,1)} %param.20) | copy-start | bytes 12292
  7.2 61.5 %copy-start.1 = (bf16[352,256]{1,0:T(8,128)(2,1)S(1)}, bf16[352,256]{1,0:T(8,128)(2,1)}, u32[]{:S(2)}) copy-start(bf16[352,256]{1,0:T(8,128)(2,1)} %param.25) | copy-start | bytes 540676
  7.2 68.6 %copy-start.2 = (bf16[256,128]{1,0:T(8,128)(2,1)S(1)}, bf16[256,128]{1,0:T(8,128)(2,1)}, u32[]{:S(2)}) copy-start(bf16[256,128]{1,0:T(8,128)(2,1)} %param.27) | copy-start | bytes 196612
  7.2 85.0 %copy-start.3 = (bf16[256,128]{1,0:T(8,128)(2,1)S(1)}, bf16[256,128]{1,0:T(8,128)(2,1)}, u32[]{:S(2)}) copy-start(bf16[256,128]{1,0:T(8,128)(2,1)} %param.28) | copy-start | bytes 196612
  7.2 85.1 %copy-start.4 = (bf16[256,128]{1,0:T(8,128)(2,1)S(1)}, bf16[256,128]{1,0:T(8,128)(2,1)}, u32[]{:S(2)}) copy-start(bf16[256,128]{1,0:T(8,128)(2,1)} %param.29) | copy-start | bytes 196612
  7.2 91.0 %copy-start.6 = (bf16[256]{0:T(256)(128)(2,1)S(1)}, bf16[256]{0:T(256)(128)(2,1)}, u32[]{:S(2)}) copy-start(bf16[256]{0:T(256)(128)(2,1)} %param.26) | copy-start | bytes 1540
  7.2 150.2 %all-gather.3.cloned.1.call-start = ((), (), s32[]{:S(2)}) async-start(), calls=%async_computation.9 | async-start | bytes 20004864 | tf_op jit(solution)/shard_map/all_gather | solution.py:115
  10.6 106.9 %copy-start.7 = (bf16[128]{0:T(256)(128)(2,1)S(1)}, bf16[128]{0:T(256)(128)(2,1)}, u32[]{:S(2)}) copy-start(bf16[128]{0:T(256)(128)(2,1)} %param.34) | copy-start | bytes 772
  10.6 27.4 %all-to-all-start = ((bf16[16,8,256]{2,1,0:T(8,128)(2,1)}), bf16[16,8,256]{2,1,0:T(8,128)(2,1)S(1)}, u32[]{:S(2)}, u32[]{:S(2)}) async-start(bf16[16,8,256]{2,1,0:T(8,128)(2,1)} %broadcast_in_dim.14), calls=%async_computation | async-start | bytes 131072 | tf_op jit(solution)/shard_map/all_to_all | solution.py:26
  26.5 99.4 %copy-start = (f32[16,1,128,128]{3,2,1,0:T(8,128)S(1)}, f32[16,1,128,128]{3,2,1,0:T(8,128)}, u32[]{:S(2)}) copy-start(f32[16,1,128,128]{3,2,1,0:T(8,128)} %param.21) | copy-start | bytes 3145732
  27.7 13.5 %collective-permute-start = (bf16[1056,256]{1,0:T(8,128)(2,1)S(1)}, bf16[1056,256]{1,0:T(8,128)(2,1)S(1)}, u32[]{:S(2)}, u32[]{:S(2)}) collective-permute-start(bf16[1056,256]{1,0:T(8,128)(2,1)S(1)} %pad_maximum_fusion.1), channel_id=1, source_target_pairs={{0,1},{1,0},{2,3},{3,2},{4,5},{5,4},{6,7},{7,6},{8,9},{9,8},{10,11... | collective-permute-start | bytes 1622024 | tf_op jit(solution)/shard_map/ppermute | solution.py:38
  41.5 108.6 %copy-start.8 = (bf16[256]{0:T(256)(128)(2,1)S(1)}, bf16[256]{0:T(256)(128)(2,1)}, u32[]{:S(2)}) copy-start(bf16[256]{0:T(256)(128)(2,1)} %param.36) | copy-start | bytes 1540
  58.0 10.7 %all-to-all-start.2 = ((bf16[16,8,704]{2,1,0:T(8,128)(2,1)}), bf16[16,8,704]{2,1,0:T(8,128)(2,1)S(1)}, u32[]{:S(2)}, u32[]{:S(2)}) async-start(bf16[16,8,704]{2,1,0:T(8,128)(2,1)} %broadcast_in_dim.15), calls=%async_computation.2 | async-start | bytes 393216 | tf_op jit(solution)/shard_map/all_to_all | solution.py:26
  69.5 18.6 %all-to-all-start.3 = ((bf16[16,8,256]{2,1,0:T(8,128)(2,1)}), bf16[16,8,256]{2,1,0:T(8,128)(2,1)S(1)}, u32[]{:S(2)}, u32[]{:S(2)}) async-start(bf16[16,8,256]{2,1,0:T(8,128)(2,1)} %fusion.14), calls=%async_computation.3 | async-start | bytes 131072 | tf_op jit(solution)/shard_map/all_to_all | solution.py:26
  88.7 15.7 %all-to-all-start.4 = ((bf16[16,8,256]{2,1,0:T(8,128)(2,1)}), bf16[16,8,256]{2,1,0:T(8,128)(2,1)S(1)}, u32[]{:S(2)}, u32[]{:S(2)}) async-start(bf16[16,8,256]{2,1,0:T(8,128)(2,1)} %broadcast_in_dim.16), calls=%async_computation.4 | async-start | bytes 131072 | tf_op jit(solution)/shard_map/all_to_all | solution.py:26
  92.3 14.0 %collective-permute-start.1 = (bf16[256,384]{1,0:T(8,128)(2,1)S(1)}, bf16[256,384]{1,0:T(8,128)(2,1)S(1)}, u32[]{:S(2)}, u32[]{:S(2)}) collective-permute-start(bf16[256,384]{1,0:T(8,128)(2,1)S(1)} %constant_dynamic-update-slice_fusion), channel_id=1, source_target_pairs={{0,1},{1,0},{2,3},{3,2},{4,5},{5,4},{6,7},{7,6},{8,9},{9,8},{10,11... | collective-permute-start | bytes 589832 | tf_op jit(solution)/shard_map/ppermute | solution.py:38
  107.6 17.6 %all-to-all-start.5 = ((bf16[32,8,389]{2,1,0:T(8,128)(2,1)}), bf16[32,8,389]{2,1,0:T(8,128)(2,1)S(1)}, u32[]{:S(2)}, u32[]{:S(2)}) async-start(bf16[32,8,389]{2,1,0:T(8,128)(2,1)} %bitcast.18), calls=%async_computation.5 | async-start | bytes 524288 | tf_op jit(solution)/shard_map/all_to_all | solution.py:26
  128.3 0.7 collective-permute-start.2
  129.6 27.7 %all-to-all-start.6 = ((bf16[32,8,128]{2,1,0:T(8,128)(2,1)}), bf16[32,8,128]{2,1,0:T(8,128)(2,1)S(1)}, u32[]{:S(2)}, u32[]{:S(2)}) async-start(bf16[32,8,128]{2,1,0:T(8,128)(2,1)} %bitcast.32), calls=%async_computation.6 | async-start | bytes 131072 | tf_op jit(solution)/shard_map/all_to_all | solution.py:26
  182.2 10.8 %all-to-all-start.8 = ((bf16[16,8,704]{2,1,0:T(8,128)(2,1)}), bf16[16,8,704]{2,1,0:T(8,128)(2,1)S(1)}, u32[]{:S(2)}, u32[]{:S(2)}) async-start(bf16[16,8,704]{2,1,0:T(8,128)(2,1)} %broadcast_in_dim.20), calls=%async_computation.8 | async-start | bytes 393216 | tf_op jit(solution)/shard_map/all_to_all | solution.py:26
Sparse Core Ops, SparseCore 0:
  10.7 131.9 all-gather.2

commit v3 on v2

v3 whole, which is shorter than its diff:
```python
import functools

import jax
import jax.numpy as jnp
from jax import lax
from jax.experimental import pallas as pl
from jax.experimental.pallas import tpu as pltpu
from jax.sharding import Mesh
from jax.sharding import PartitionSpec as P

D = 4096
EPS = 1e-06
KV = ("kv_0", "kv_1")
TP = ("z", "core")
KVC = ("kv_0", "kv_1", "core")
ALL = ("kv_0", "kv_1", "z", "core")
BF16 = jnp.bfloat16
F32 = jnp.float32


PAD = 384


def dot_nn(a, b):
    return jnp.dot(a, b, preferred_element_type=F32)


def dot_nt(a, b):
    return lax.dot_general(a, b, (((1,), (1,)), ((), ())), preferred_element_type=F32)


def exchanged(parts, axis):
    return lax.all_to_all(parts, axis, 0, 0, tiled=True)


def from_partner(x):
    return lax.ppermute(x, "core", [(0, 1), (1, 0)])


def local_call(kernel, shapes, args, *, scalars=0, far=(), scratch=(), limit=None):
    specs = [
        pl.BlockSpec(
            memory_space=pltpu.SMEM if i < scalars else pl.ANY if i in far else pltpu.VMEM
        )
        for i in range(len(args))
    ]
    outs = tuple(jax.ShapeDtypeStruct(shape, dtype) for shape, dtype in shapes)
    return pl.pallas_call(
        kernel,
        out_shape=outs,
        in_specs=specs,
        out_specs=tuple(pl.BlockSpec(memory_space=pltpu.VMEM) for _ in outs),
        scratch_shapes=list(scratch),
        compiler_params=pltpu.CompilerParams(vmem_limit_bytes=limit),
    )(*args)


def rows_of(ref):
    values = ref[...].astype(F32)
    return values.reshape(values.shape[0] * values.shape[1], values.shape[2])


def in_three(total):
    high = total.astype(BF16)
    rest = total - high.astype(F32)
    middle = rest.astype(BF16)
    return (high, middle, (rest - middle.astype(F32)).astype(BF16))


def scale_of(squares):
    return lax.rsqrt(squares / D + EPS)


def gate_up_kernel(rows_ref, gain_ref, gate_ref, up_ref, other_ref, out_ref):
    units = gate_ref.shape[0]
    n, rows, _ = rows_ref.shape
    stream = rows_of(rows_ref)
    scaled = (stream * gain_ref[...].astype(F32)).astype(BF16)
    weights = (gate_ref[...], other_ref[:units], up_ref[...], other_ref[units : 2 * units])
    for i, weight in enumerate(weights):
        out_ref[:, :, i * PAD + units : (i + 1) * PAD] = jnp.zeros((n, rows, PAD - units), BF16)
        product = dot_nt(scaled, weight).reshape(n, rows, units)
        out_ref[:, :, i * PAD : i * PAD + units] = product.astype(BF16)
    pieces = in_three(jnp.sum(stream * stream, axis=1, keepdims=True))
    for i, piece in enumerate(pieces):
        out_ref[:, :, units + i : units + i + 1] = (
            piece.astype(F32).reshape(n, rows, 1).astype(BF16)
        )


def hidden_kernel(units, parts_ref, out_ref):
    total = jnp.sum(parts_ref[...].astype(F32), axis=0)
    squares = jnp.sum(total[:, units : units + 3], axis=1, keepdims=True)
    factor = scale_of(squares)
    gate, up = factor * total[:, : 2 * PAD], factor * total[:, 2 * PAD :]
    hidden = (gate * jax.nn.sigmoid(gate) * up).astype(BF16)
    for i in range(out_ref.shape[0]):
        out_ref[i] = hidden


def down_kernel(hidden_ref, own_ref, other_ref, out_ref):
    units = own_ref.shape[0]
    hidden = rows_of(hidden_ref).astype(BF16)
    total = dot_nn(hidden[:, :units], own_ref[...])
    total += dot_nn(hidden[:, PAD : PAD + units], other_ref[2 * units : 3 * units])
    out_ref[...] = total.reshape(out_ref.shape).astype(BF16)


def first_kernel(parts_ref, own_ref, first_ref, out_ref):
    branch = jnp.sum(parts_ref[...].astype(F32), axis=0)
    first = (own_ref[...].astype(F32) + 0.5 * branch).astype(BF16)
    first_ref[...] = first
    for i in range(out_ref.shape[0]):
        out_ref[i] = first


def query_kernel(core_ref, rows_ref, gain_ref, q_ref, k_ref, v_ref, other_ref, gates_ref, out_ref):
    n, rows, _ = rows_ref.shape
    dim = q_ref.shape[1]
    stream = rows_of(rows_ref)
    scaled = (stream * gain_ref[...].astype(F32)).astype(BF16)
    is_first = core_ref[0] == 0
    for i, weight in enumerate((q_ref, k_ref, v_ref)):
        own = dot_nn(scaled, weight[...])
        other = dot_nn(scaled, other_ref[:, i * dim : (i + 1) * dim])
        for to, part in enumerate(
            (jnp.where(is_first, own, other), jnp.where(is_first, other, own))
        ):
            out_ref[:, to, :, i * dim : (i + 1) * dim] = part.reshape(n, rows, dim).astype(BF16)
    gates = dot_nt(scaled, gates_ref[...])
    pieces = in_three(jnp.sum(stream * stream, axis=1, keepdims=True))
    for to in range(2):
        columns = [gates[:, to : to + 1], gates[:, 2 + to : 3 + to]]
        columns += [piece.astype(F32) for piece in pieces]
        for i, column in enumerate(columns):
            at = 3 * dim + i
            out_ref[:, to, :, at : at + 1] = column.reshape(n, rows, 1).astype(BF16)


def state_kernel(
    parts_ref, state_ref, base_ref, shift_ref, head_gain_ref, state_out_ref, out_ref, held
):
    dim = state_ref.shape[2]
    got = jnp.sum(parts_ref[...].astype(F32), axis=0)
    squares = jnp.sum(got[:, 3 * dim + 2 : 3 * dim + 5], axis=1, keepdims=True)
    got = scale_of(squares) * got[:, : 3 * dim + 2]
    queries, keys, values = (got[:, i * dim : (i + 1) * dim] for i in range(3))
    decay_in, blend_in = got[:, 3 * dim : 3 * dim + 1], got[:, 3 * dim + 1 : 3 * dim + 2]

    def unit(v):
        return v * lax.rsqrt(jnp.sum(v * v, axis=1, keepdims=True) + EPS)

    queries, keys = unit(queries) * dim**-0.5, unit(keys)
    inner = decay_in + shift_ref[...]
    soft = jnp.maximum(inner, 0.0) + jnp.log1p(jnp.exp(-jnp.abs(inner)))
    rate = jnp.exp(-jnp.exp(base_ref[...]) * soft)
    beta = jax.nn.sigmoid(blend_in)
    queries_t, keys_t = queries.T, keys.T
    for b in range(state_ref.shape[0]):
        old = state_ref[b]
        key, query = keys_t[:, b : b + 1], queries_t[:, b : b + 1]
        rate_b = rate[b : b + 1]
        recalled = jnp.sum(key * old, axis=0, keepdims=True)
        correction = beta[b : b + 1] * (values[b : b + 1] - rate_b * recalled)
        new = rate_b * old + key * correction
        state_out_ref[b] = new
        held[b : b + 1] = jnp.sum(query * new, axis=0, keepdims=True)
    read = held[...]
    normed = read * lax.rsqrt(jnp.mean(read * read, axis=1, keepdims=True) + EPS)
    normed = (normed * head_gain_ref[...].astype(F32)).astype(BF16)
    for i in range(out_ref.shape[0]):
        out_ref[i] = normed


def out_kernel(core_ref, heads_ref, own_ref, other_ref, out_ref):
    n, both, dim = heads_ref.shape
    heads = heads_ref[...].astype(F32)
    zero = heads[:, : both // 2].reshape(n * both // 2, dim).astype(BF16)
    one = heads[:, both // 2 :].reshape(n * both // 2, dim).astype(BF16)
    from_zero, from_one = dot_nn, dot_nn
    is_first = core_ref[0] == 0
    own, other = own_ref[...], other_ref[other_ref.shape[0] - dim :]
    total = from_zero(zero, jnp.where(is_first, own, other))
    total += from_one(one, jnp.where(is_first, other, own))
    out_ref[...] = total.reshape(out_ref.shape).astype(BF16)


def wide_kernel(
    units, parts_ref, first_ref, gain_ref, weights_ref, out_ref, second_ref, held, sems
):
    n, rows, _ = out_ref.shape

    def copy(k):
        return pltpu.make_async_copy(
            weights_ref.at[pl.ds(2 * k, 2), pl.ds(0, 2 * units)], held.at[k], sems.at[k]
        )

    for k in range(n):
        copy(k).start()
    branch = jnp.sum(parts_ref[...].astype(F32), axis=0)
    second = (first_ref[...].astype(F32) + branch).astype(BF16)
    second_ref[...] = second
    stream = second.astype(F32)
    scaled = (stream * gain_ref[...].astype(F32)).astype(BF16)
    pieces = in_three(jnp.sum(stream * stream, axis=1, keepdims=True))
    for k in range(n):
        copy(k).wait()
        for i in range(4):
            out_ref[k, :, i * PAD + units : (i + 1) * PAD] = jnp.zeros((rows, PAD - units), BF16)
            weight = held[k, i % 2, (i // 2) * units : (i // 2 + 1) * units]
            out_ref[k, :, i * PAD : i * PAD + units] = dot_nt(scaled, weight).astype(BF16)
        for i, piece in enumerate(pieces):
            out_ref[k, :, units + i : units + i + 1] = piece


def last_kernel(units, hidden_ref, second_ref, weights_ref, out_ref, held, sems):
    n = hidden_ref.shape[0]

    def copy(k):
        return pltpu.make_async_copy(
            weights_ref.at[pl.ds(2 * k, 2), pl.ds(2 * units, units)], held.at[k], sems.at[k]
        )

    for k in range(n):
        copy(k).start()
    total = jnp.zeros(out_ref.shape, F32)
    for k in range(n):
        copy(k).wait()
        for i in range(2):
            total += dot_nn(hidden_ref[k, :, i * PAD : i * PAD + units], held[k, i])
    out_ref[...] = (second_ref[...].astype(F32) + 0.5 * total).astype(BF16)


def on_device(
    tokens,
    state,
    gain_pre,
    w_gate_pre,
    w_up_pre,
    w_down_pre,
    gain_mix,
    w_query,
    w_key,
    w_value,
    w_decay,
    w_blend,
    decay_base,
    decay_shift,
    head_gain,
    w_out,
    gain_post,
    w_gate_post,
    w_up_post,
    w_down_post,
):
    n = lax.axis_size(KV)
    rows, width = tokens.shape
    units = w_gate_pre.shape[1]
    seqs, _, dim, _ = state.shape
    core = lax.axis_index("core").reshape(1)
    block = (n, rows, width)
    wide = (n, rows, 4 * PAD)
    narrow = (n, rows, 2 * PAD)

    later = jnp.concatenate([w_gate_post.T, w_up_post.T, w_down_post], axis=0)
    later = lax.all_gather(later, TP, axis=0, tiled=False)

    gate_t, up_t = w_gate_pre.T, w_up_pre.T
    other = from_partner(jnp.concatenate([gate_t, up_t, w_down_pre, w_out], axis=0))
    stream = exchanged(jnp.broadcast_to(tokens[None], block), "z")
    (sent,) = local_call(
        gate_up_kernel, [(wide, BF16)], (stream, gain_pre[None], gate_t, up_t, other)
    )
    (hidden,) = local_call(
        functools.partial(hidden_kernel, units), [(narrow, BF16)], (exchanged(sent, KV),)
    )
    (sent,) = local_call(
        down_kernel, [(block, BF16)], (exchanged(hidden, KV), w_down_pre, other)
    )
    first, sent = local_call(
        first_kernel, [(tokens.shape, BF16), (block, BF16)], (exchanged(sent, "z"), tokens)
    )

    other_query = from_partner(jnp.concatenate([w_query, w_key, w_value], axis=1))
    pair = 2 * lax.axis_index("z")
    gates = jnp.concatenate(
        [
            lax.dynamic_slice_in_dim(w_decay.T, pair, 2, 0),
            lax.dynamic_slice_in_dim(w_blend.T, pair, 2, 0),
        ],
        axis=0,
    )
    (sent,) = local_call(
        query_kernel,
        [((n, 2, rows, 4 * dim), BF16)],
        (
            core,
            exchanged(sent, "z"),
            gain_mix[None],
            w_query,
            w_key,
            w_value,
            other_query,
            gates,
        ),
        scalars=1,
    )
    got = exchanged(sent.reshape(2 * n, rows, 4 * dim), KVC).reshape(n, 2 * rows, 4 * dim)
    new_state, sent = local_call(
        state_kernel,
        [((seqs, dim, dim), F32), ((n, seqs, dim), BF16)],
        (
            got,
            state.reshape(seqs, dim, dim),
            decay_base[None],
            decay_shift[None],
            head_gain[None],
        ),
        scratch=(pltpu.VMEM((seqs, dim), F32),),
    )
    heads = exchanged(sent.reshape(2 * n, rows, dim), KVC).reshape(n, 2 * rows, dim)
    (sent,) = local_call(
        out_kernel, [(block, BF16)], (core, heads, w_out, other), scalars=1
    )

    sent, second = local_call(
        functools.partial(wide_kernel, units),
        [(wide, BF16), (tokens.shape, BF16)],
        (exchanged(sent, "z"), first, gain_post[None], later),
        far=(3,),
        scratch=(pltpu.VMEM((n, 2, 2 * units, width), BF16), pltpu.SemaphoreType.DMA((n,))),
        limit=24 << 20,
    )
    (hidden,) = local_call(
        functools.partial(hidden_kernel, units), [(narrow, BF16)], (exchanged(sent, KV),)
    )
    (result,) = local_call(
        functools.partial(last_kernel, units),
        [(tokens.shape, BF16)],
        (exchanged(hidden, KV), second, later),
        far=(2,),
        scratch=(pltpu.VMEM((n, 2, units, width), BF16), pltpu.SemaphoreType.DMA((n,))),
        limit=16 << 20,
    )
    return (result, new_state.reshape(state.shape))


def solution(mesh):
    finer = Mesh(mesh.devices.reshape(4, 4, mesh.shape["tp"] // 2, 2), ALL)
    in_specs = (
        P(TP, KV),
        P(KV, TP, None, None),
        P(KV),
        P(KV, TP),
        P(KV, TP),
        P(TP, KV),
        P(KV),
        P(KV, TP),
        P(KV, TP),
        P(KV, TP),
        P(KV, None),
        P(KV, None),
        P(TP),
        P(TP),
        P(),
        P(TP, KV),
        P(KV),
        P(KV, TP),
        P(KV, TP),
        P(TP, KV),
    )
    out_specs = (P(TP, KV), P(KV, TP, None, None))
    return jax.shard_map(
        on_device, mesh=finer, in_specs=in_specs, out_specs=out_specs, check_vma=False
    )
```

time: 206 us -> 221 us (1.073)
  blocking collectives: 26.9 us -> 77.8 us
  Pallas kernels: 0 us -> 29.5 us
  starting transfers between devices: 71.2 us -> 42.2 us
  matrix products: 20.9 us -> 0 us
  waiting for transfers between devices: 47 us -> 33.6 us
  other arithmetic: 7.78 us -> 2.69 us
  local copies, waits for them, and re-layouts: 14.4 us -> 17.1 us
    all_to_all x2 -> x6, blocking collectives: 26.9 us -> 77.8 us  [exchanged(): return lax.all_to_all(parts, axis, 0, 0, tiled=True)]
    all_to_all x7 -> x4, starting transfers between devices: 61.8 us -> 26.4 us  [exchanged(): return lax.all_to_all(parts, axis, 0, 0, tiled=True)]
    pallas_call x0 -> x10, Pallas kernels: none -> 29.5 us  [local_call(): pl.pallas_call(kernel, out_shape=outs, in_specs=specs, out_specs=tuple((p...]
    dot_general x14 -> x0, matrix products: 20.9 us -> none  [the longest x1 4.31 us: on_device(): jnp.einsum('rk,tnk->rtn', scaled, w_up_all, preferred_element_type=F32)]
    unnamed x20 -> x38, local copies, waits for them, and re-layouts: 0.08 us -> 14.7 us
    all_to_all x7 -> x4, waiting for transfers between devices: 47 us -> 33.6 us  [exchanged(): return lax.all_to_all(parts, axis, 0, 0, tiled=True)]
    ppermute x2, starting transfers between devices: 8.71 us -> 15.8 us  [from_partner(): return lax.ppermute(x, 'core', [(0, 1), (1, 0)])]
    slice x3 -> x0, local copies, waits for them, and re-layouts: 5.5 us -> none  [the longest x1 5.45 us: on_device(): later[:, a:b]]
  transfers between devices with their start and end apart: 11 -> 7, of which waited for: 7 -> 4; matrix products, arithmetic and copies ran while one was open for 12% -> 1% of each run, Pallas kernels for 0% -> 7%
where the time goes in v3:
time: 221 us; the launch traced here: 218 us
  blocking collectives  77.8 us (35%)
  starting transfers between devices  42.2 us (19%)
  waiting for transfers between devices  33.6 us (15%)
  Pallas kernels  29.5 us (13%)
  local copies, waits for them, and re-layouts  17.1 us (8%)
  between operations  15.6 us (7%)
  other arithmetic  2.69 us (1%)
    all_to_all x6, blocking collectives, exchanged(): return lax.all_to_all(parts, axis, 0, 0, tiled=True)  77.8 us
    all_to_all x4, waiting for transfers between devices, exchanged(): return lax.all_to_all(parts, axis, 0, 0, tiled=True)  33.6 us
    pallas_call x10, Pallas kernels, local_call(): pl.pallas_call(kernel, out_shape=outs, in_specs=specs, out_specs=tuple((p...  29.5 us
    all_to_all x4, starting transfers between devices, exchanged(): return lax.all_to_all(parts, axis, 0, 0, tiled=True)  26.4 us
    ppermute x2, starting transfers between devices, from_partner(): return lax.ppermute(x, 'core', [(0, 1), (1, 0)])  15.8 us
    unnamed x38, local copies, waits for them, and re-layouts  14.7 us
  transfers between devices with their start and end apart: 7, of which 4 were waited for; matrix products, arithmetic and copies ran while one was open for 1% of the time, Pallas kernels for 7%

profile of v3, /device:TPU:1, one launch (start us, length us, event | category | flops | bytes accessed | tf_op | source)
XLA Modules:
  0.0 218.5 jit_solution(5628201391358033740)
XLA Ops:
  9.4 8.7 %collective-permute-start = (bf16[1184,256]{1,0:T(8,128)(2,1)S(1)}, bf16[1184,256]{1,0:T(8,128)(2,1)S(1)}, u32[]{:S(2)}, u32[]{:S(2)}) collective-permute-start(bf16[1184,256]{1,0:T(8,128)(2,1)S(1)} %pad_maximum_fusion), channel_id=1, source_target_pairs={{0,1},{1,0},{2,3},{3,2},{4,5},{5,4},{6,7},{7,6},{8,9},{9,8},{10,11... | collective-permute-start | bytes 1818632 | tf_op jit(solution)/shard_map/ppermute | solution.py:37
  18.8 9.6 %all-to-all-start = ((bf16[16,8,256]{2,1,0:T(8,128)(2,1)}), bf16[16,8,256]{2,1,0:T(8,128)(2,1)S(1)}, u32[]{:S(2)}, u32[]{:S(2)}) async-start(bf16[16,8,256]{2,1,0:T(8,128)(2,1)} %broadcast_in_dim.24), calls=%async_computation | async-start | bytes 131072 | tf_op jit(solution)/shard_map/all_to_all | solution.py:33
  29.0 11.1 %all-to-all-done.rows_ref = bf16[16,8,256]{2,1,0:T(8,128)(2,1)S(1)} async-done(((bf16[16,8,256]{2,1,0:T(8,128)(2,1)}), bf16[16,8,256]{2,1,0:T(8,128)(2,1)S(1)}, u32[]{:S(2)}, u32[]{:S(2)}) %all-to-all-start) | async-done | bytes 65568 | tf_op jit(solution)/shard_map/all_to_all | solution.py:33
  41.5 2.4 %shard_map.203 = bf16[16,8,1536]{2,1,0:T(8,128)(2,1)} custom-call(bf16[16,8,256]{2,1,0:T(8,128)(2,1)} %copy-done.9, bf16[1,256]{1,0:T(2,128)(2,1)} %broadcast_in_dim.25.gain_ref, bf16[352,256]{1,0:T(8,128)(2,1)} %bitcast.28, bf16[352,256]{1,0:T(8,128)(2,1)} %bitcast.30, bf16[1184,256]{1,0:T(8,128)(2,1)} %copy-done.3), custom_call_target="tpu_custom_call" | custom-call | tf_op jit(solution)/shard_map/pallas_call | solution.py:48
  44.0 15.1 %all_to_all.50.parts_ref = bf16[16,8,1536]{2,1,0:T(8,128)(2,1)} all-to-all(bf16[16,8,1536]{2,1,0:T(8,128)(2,1)} %shard_map.203), channel_id=1, replica_groups=mesh['kv_0'=4,'kv_1'=4,'z'=16,'core'=2] {'kv_0','kv_1'}, dimensions={0} | all-to-all | bytes 786432 | tf_op jit(solution)/shard_map/all_to_all | solution.py:33
  61.0 11.5 %all_to_all.51.hidden_ref = bf16[16,8,768]{2,1,0:T(8,128)(2,1)} all-to-all(bf16[16,8,768]{2,1,0:T(8,128)(2,1)} %shard_map.204), channel_id=1, replica_groups=mesh['kv_0'=4,'kv_1'=4,'z'=16,'core'=2] {'kv_0','kv_1'}, dimensions={0} | all-to-all | bytes 393216 | tf_op jit(solution)/shard_map/all_to_all | solution.py:33
  72.5 2.1 shard_map.205
  74.6 17.1 %all_to_all.52.parts_ref = bf16[16,8,256]{2,1,0:T(8,128)(2,1)} all-to-all(bf16[16,8,256]{2,1,0:T(8,128)(2,1)} %shard_map.205), channel_id=1, replica_groups=mesh['kv_0'=4,'kv_1'=4,'z'=16,'core'=2] {'z'}, dimensions={0} | all-to-all | bytes 131072 | tf_op jit(solution)/shard_map/all_to_all | solution.py:33
  93.2 3.5 %all-to-all-start.4 = ((bf16[16,8,256]{2,1,0:T(8,128)(2,1)}), bf16[16,8,256]{2,1,0:T(8,128)(2,1)S(1)}, u32[]{:S(2)}, u32[]{:S(2)}) async-start(bf16[16,8,256]{2,1,0:T(8,128)(2,1)} %get-tuple-element.8), calls=%async_computation.4 | async-start | bytes 131072 | tf_op jit(solution)/shard_map/all_to_all | solution.py:33
  96.8 7.0 %collective-permute-start.1 = (bf16[256,384]{1,0:T(8,128)(2,1)S(1)}, bf16[256,384]{1,0:T(8,128)(2,1)S(1)}, u32[]{:S(2)}, u32[]{:S(2)}) collective-permute-start(bf16[256,384]{1,0:T(8,128)(2,1)S(1)} %pad_maximum_fusion.2), channel_id=1, source_target_pairs={{0,1},{1,0},{2,3},{3,2},{4,5},{5,4},{6,7},{7,6},{8,9},{9,8},{10,11... | collective-permute-start | bytes 589832 | tf_op jit(solution)/shard_map/ppermute | solution.py:37
  105.6 3.2 %all-to-all-done.4.rows_ref = bf16[16,8,256]{2,1,0:T(8,128)(2,1)S(1)} async-done(((bf16[16,8,256]{2,1,0:T(8,128)(2,1)}), bf16[16,8,256]{2,1,0:T(8,128)(2,1)S(1)}, u32[]{:S(2)}, u32[]{:S(2)}) %all-to-all-start.4) | async-done | bytes 65568 | tf_op jit(solution)/shard_map/all_to_all | solution.py:33
  109.5 2.1 shard_map.207
  111.6 9.8 %all-to-all-start.5 = ((bf16[32,8,512]{2,1,0:T(8,128)(2,1)}), bf16[32,8,512]{2,1,0:T(8,128)(2,1)S(1)}, u32[]{:S(2)}, u32[]{:S(2)}) async-start(bf16[32,8,512]{2,1,0:T(8,128)(2,1)} %bitcast.25), calls=%async_computation.5 | async-start | bytes 524288 | tf_op jit(solution)/shard_map/all_to_all | solution.py:33
  122.7 7.6 %all-to-all-done.5 = bf16[32,8,512]{2,1,0:T(8,128)(2,1)S(1)} async-done(((bf16[32,8,512]{2,1,0:T(8,128)(2,1)}), bf16[32,8,512]{2,1,0:T(8,128)(2,1)S(1)}, u32[]{:S(2)}, u32[]{:S(2)}) %all-to-all-start.5) | async-done | bytes 262176 | tf_op jit(solution)/shard_map/all_to_all | solution.py:33
  131.1 3.3 %shard_map.208 = (f32[16,128,128]{2,1,0:T(8,128)}, bf16[16,16,128]{2,1,0:T(8,128)(2,1)}) custom-call(bf16[16,16,512]{2,1,0:T(8,128)(2,1)} %bitcast.27, f32[16,128,128]{2,1,0:T(8,128)} %bitcast.26, f32[1,1]{1,0:T(1,128)} %bitcast.21.base_ref, f32[1,1]{1,0:T(1,128)} %bitcast.22.shift_ref, bf16[1,128]{1,0:T(2,128)(2,1)} %bitcast.36), custom_call_target="tpu_custom_call" | custom-call | tf_op jit(solution)/shard_map/pallas_call | solution.py:48
  134.4 11.7 %all_to_all.53 = bf16[32,8,128]{2,1,0:T(8,128)(2,1)} all-to-all(bf16[32,8,128]{2,1,0:T(8,128)(2,1)} %bitcast.35), channel_id=1, replica_groups=mesh['kv_0'=4,'kv_1'=4,'z'=16,'core'=2] {'kv_0','kv_1','core'}, dimensions={0} | all-to-all | bytes 131072 | tf_op jit(solution)/shard_map/all_to_all | solution.py:33
  148.0 3.5 %all-to-all-start.7 = ((bf16[16,8,256]{2,1,0:T(8,128)(2,1)}), bf16[16,8,256]{2,1,0:T(8,128)(2,1)S(1)}, u32[]{:S(2)}, u32[]{:S(2)}) async-start(bf16[16,8,256]{2,1,0:T(8,128)(2,1)} %shard_map.209), calls=%async_computation.7 | async-start | bytes 131072 | tf_op jit(solution)/shard_map/all_to_all | solution.py:33
  151.6 11.6 %all-to-all-done.7.parts_ref = bf16[16,8,256]{2,1,0:T(8,128)(2,1)S(1)} async-done(((bf16[16,8,256]{2,1,0:T(8,128)(2,1)}), bf16[16,8,256]{2,1,0:T(8,128)(2,1)S(1)}, u32[]{:S(2)}, u32[]{:S(2)}) %all-to-all-start.7) | async-done | bytes 65568 | tf_op jit(solution)/shard_map/all_to_all | solution.py:33
  163.2 5.9 %copy-done = bf16[33792,256]{1,0:T(8,128)(2,1)S(1)} copy-done((bf16[33792,256]{1,0:T(8,128)(2,1)S(1)}, bf16[33792,256]{1,0:T(8,128)(2,1)}, u32[]{:S(2)}) %copy-start) | copy-done | bytes 17301528
  169.1 7.7 %shard_map.210 = (bf16[16,8,1536]{2,1,0:T(8,128)(2,1)S(1)}, bf16[8,256]{1,0:T(8,128)(2,1)S(1)}) custom-call(bf16[16,8,256]{2,1,0:T(8,128)(2,1)S(1)} %all-to-all-done.7.parts_ref, bf16[8,256]{1,0:T(8,128)(2,1)S(1)} %copy-done.2, bf16[1,256]{1,0:T(2,128)(2,1)S(1)} %broadcast_in_dim.30.gain_ref, bf16[32,1056,256]{2,1,0:T(8,128)(2,1)S(1)} %bitcast.23), custom_call_target="tpu_custom_call" | custom-call | tf_op jit(solution)/shard_map/pallas_call | solution.py:48
  176.8 11.7 %all_to_all.54.parts_ref = bf16[16,8,1536]{2,1,0:T(8,128)(2,1)} all-to-all(bf16[16,8,1536]{2,1,0:T(8,128)(2,1)S(1)} %get-tuple-element.11), channel_id=1, replica_groups=mesh['kv_0'=4,'kv_1'=4,'z'=16,'core'=2] {'kv_0','kv_1'}, dimensions={0} | all-to-all | bytes 786432 | tf_op jit(solution)/shard_map/all_to_all | solution.py:33
  190.4 10.7 %all_to_all.55.hidden_ref = bf16[16,8,768]{2,1,0:T(8,128)(2,1)S(1)} all-to-all(bf16[16,8,768]{2,1,0:T(8,128)(2,1)} %shard_map.211), channel_id=1, replica_groups=mesh['kv_0'=4,'kv_1'=4,'z'=16,'core'=2] {'kv_0','kv_1'}, dimensions={0} | all-to-all | bytes 393216 | tf_op jit(solution)/shard_map/all_to_all | solution.py:33
  201.0 5.9 %copy-done.1 = bf16[33792,256]{1,0:T(8,128)(2,1)S(1)} copy-done((bf16[33792,256]{1,0:T(8,128)(2,1)S(1)}, bf16[33792,256]{1,0:T(8,128)(2,1)}, u32[]{:S(2)}) %copy-start.1) | copy-done | bytes 17301528
  207.0 4.6 %shard_map.212 = bf16[8,256]{1,0:T(8,128)(2,1)} custom-call(bf16[16,8,768]{2,1,0:T(8,128)(2,1)S(1)} %all_to_all.55.hidden_ref, bf16[8,256]{1,0:T(8,128)(2,1)S(1)} %get-tuple-element.12.second_ref, bf16[32,1056,256]{2,1,0:T(8,128)(2,1)S(1)} %bitcast.24), custom_call_target="tpu_custom_call" | custom-call | tf_op jit(solution)/shard_map/pallas_call | solution.py:48
  (54 shorter events, 15.2 us)
Async XLA Ops:
  7.2 2.2 %copy-start.5 = (bf16[256,352]{0,1:T(8,128)(2,1)S(1)}, bf16[256,352]{0,1:T(8,128)(2,1)}, u32[]{:S(2)}) copy-start(bf16[256,352]{0,1:T(8,128)(2,1)} %param.23) | copy-start | bytes 540676
  7.2 2.2 %copy-start.6 = (bf16[256,352]{0,1:T(8,128)(2,1)S(1)}, bf16[256,352]{0,1:T(8,128)(2,1)}, u32[]{:S(2)}) copy-start(bf16[256,352]{0,1:T(8,128)(2,1)} %param.24) | copy-start | bytes 540676
  7.2 2.2 %copy-start.7 = (bf16[352,256]{1,0:T(8,128)(2,1)S(1)}, bf16[352,256]{1,0:T(8,128)(2,1)}, u32[]{:S(2)}) copy-start(bf16[352,256]{1,0:T(8,128)(2,1)} %own_ref.3) | copy-start | bytes 540676
  7.2 2.2 %copy-start.13 = (bf16[128,256]{1,0:T(8,128)(2,1)S(1)}, bf16[128,256]{1,0:T(8,128)(2,1)}, u32[]{:S(2)}) copy-start(bf16[128,256]{1,0:T(8,128)(2,1)} %own_ref.5) | copy-start | bytes 196612
  7.2 156.0 %all-gather.3.cloned.1.call-start = ((), (), s32[]{:S(2)}) async-start(), calls=%async_computation.10 | async-start | bytes 17842176 | tf_op jit(solution)/shard_map/all_gather | solution.py:266
  7.3 10.9 %copy-start.15 = (bf16[8,256]{1,0:T(8,128)(2,1)S(1)}, bf16[8,256]{1,0:T(8,128)(2,1)}, u32[]{:S(2)}) copy-start(bf16[8,256]{1,0:T(8,128)(2,1)} %own_ref.4) | copy-start | bytes 12292
  9.3 19.1 %copy-start.16 = (bf16[256]{0:T(256)(128)(2,1)S(1)}, bf16[256]{0:T(256)(128)(2,1)}, u32[]{:S(2)}) copy-start(bf16[256]{0:T(256)(128)(2,1)} %param.22) | copy-start | bytes 1540
  9.4 30.6 %collective-permute-start = (bf16[1184,256]{1,0:T(8,128)(2,1)S(1)}, bf16[1184,256]{1,0:T(8,128)(2,1)S(1)}, u32[]{:S(2)}, u32[]{:S(2)}) collective-permute-start(bf16[1184,256]{1,0:T(8,128)(2,1)S(1)} %pad_maximum_fusion), channel_id=1, source_target_pairs={{0,1},{1,0},{2,3},{3,2},{4,5},{5,4},{6,7},{7,6},{8,9},{9,8},{10,11... | collective-permute-start | bytes 1818632 | tf_op jit(solution)/shard_map/ppermute | solution.py:37
  18.8 21.2 %all-to-all-start = ((bf16[16,8,256]{2,1,0:T(8,128)(2,1)}), bf16[16,8,256]{2,1,0:T(8,128)(2,1)S(1)}, u32[]{:S(2)}, u32[]{:S(2)}) async-start(bf16[16,8,256]{2,1,0:T(8,128)(2,1)} %broadcast_in_dim.24), calls=%async_computation | async-start | bytes 131072 | tf_op jit(solution)/shard_map/all_to_all | solution.py:33
  40.7 0.8 copy-start.3
  59.1 37.7 %copy-start.10 = (bf16[256,128]{1,0:T(8,128)(2,1)S(1)}, bf16[256,128]{1,0:T(8,128)(2,1)}, u32[]{:S(2)}) copy-start(bf16[256,128]{1,0:T(8,128)(2,1)} %q_ref.1) | copy-start | bytes 196612
  59.1 37.7 %copy-start.11 = (bf16[256,128]{1,0:T(8,128)(2,1)S(1)}, bf16[256,128]{1,0:T(8,128)(2,1)}, u32[]{:S(2)}) copy-start(bf16[256,128]{1,0:T(8,128)(2,1)} %k_ref.1) | copy-start | bytes 196612
  59.1 37.7 %copy-start.12 = (bf16[256,128]{1,0:T(8,128)(2,1)S(1)}, bf16[256,128]{1,0:T(8,128)(2,1)}, u32[]{:S(2)}) copy-start(bf16[256,128]{1,0:T(8,128)(2,1)} %v_ref.1) | copy-start | bytes 196612
  61.0 42.9 %copy-start.17 = (bf16[256]{0:T(256)(128)(2,1)S(1)}, bf16[256]{0:T(256)(128)(2,1)}, u32[]{:S(2)}) copy-start(bf16[256]{0:T(256)(128)(2,1)} %param.26) | copy-start | bytes 1540
  93.2 15.6 %all-to-all-start.4 = ((bf16[16,8,256]{2,1,0:T(8,128)(2,1)}), bf16[16,8,256]{2,1,0:T(8,128)(2,1)S(1)}, u32[]{:S(2)}, u32[]{:S(2)}) async-start(bf16[16,8,256]{2,1,0:T(8,128)(2,1)} %get-tuple-element.8), calls=%async_computation.4 | async-start | bytes 131072 | tf_op jit(solution)/shard_map/all_to_all | solution.py:33
  96.8 8.9 %collective-permute-start.1 = (bf16[256,384]{1,0:T(8,128)(2,1)S(1)}, bf16[256,384]{1,0:T(8,128)(2,1)S(1)}, u32[]{:S(2)}, u32[]{:S(2)}) collective-permute-start(bf16[256,384]{1,0:T(8,128)(2,1)S(1)} %pad_maximum_fusion.2), channel_id=1, source_target_pairs={{0,1},{1,0},{2,3},{3,2},{4,5},{5,4},{6,7},{7,6},{8,9},{9,8},{10,11... | collective-permute-start | bytes 589832 | tf_op jit(solution)/shard_map/ppermute | solution.py:37
  105.6 3.2 %copy-start.14 = (bf16[256,384]{1,0:T(8,128)(2,1)}, bf16[256,384]{1,0:T(8,128)(2,1)S(1)}, u32[]{:S(2)}) copy-start(bf16[256,384]{1,0:T(8,128)(2,1)S(1)} %collective-permute-done.1.other_ref) | copy-start | bytes 589828
  111.6 18.8 %all-to-all-start.5 = ((bf16[32,8,512]{2,1,0:T(8,128)(2,1)}), bf16[32,8,512]{2,1,0:T(8,128)(2,1)S(1)}, u32[]{:S(2)}, u32[]{:S(2)}) async-start(bf16[32,8,512]{2,1,0:T(8,128)(2,1)} %bitcast.25), calls=%async_computation.5 | async-start | bytes 524288 | tf_op jit(solution)/shard_map/all_to_all | solution.py:33
  121.4 30.1 %copy-start.18 = (bf16[256]{0:T(256)(128)(2,1)S(1)}, bf16[256]{0:T(256)(128)(2,1)}, u32[]{:S(2)}) copy-start(bf16[256]{0:T(256)(128)(2,1)} %param.36) | copy-start | bytes 1540
  121.4 41.8 %copy-start.2 = (bf16[8,256]{1,0:T(8,128)(2,1)S(1)}, bf16[8,256]{1,0:T(8,128)(2,1)}, u32[]{:S(2)}) copy-start(bf16[8,256]{1,0:T(8,128)(2,1)} %get-tuple-element.10.first_ref) | copy-start | bytes 12292
  130.4 0.7 copy-start.4
  148.0 15.2 %all-to-all-start.7 = ((bf16[16,8,256]{2,1,0:T(8,128)(2,1)}), bf16[16,8,256]{2,1,0:T(8,128)(2,1)S(1)}, u32[]{:S(2)}, u32[]{:S(2)}) async-start(bf16[16,8,256]{2,1,0:T(8,128)(2,1)} %shard_map.209), calls=%async_computation.7 | async-start | bytes 131072 | tf_op jit(solution)/shard_map/all_to_all | solution.py:33
  163.2 5.9 %copy-start = (bf16[33792,256]{1,0:T(8,128)(2,1)S(1)}, bf16[33792,256]{1,0:T(8,128)(2,1)}, u32[]{:S(2)}) copy-start(bf16[33792,256]{1,0:T(8,128)(2,1)} %all-gather.3.cloned.1.call-done) | copy-start | bytes 51904516
  201.0 5.9 %copy-start.1 = (bf16[33792,256]{1,0:T(8,128)(2,1)S(1)}, bf16[33792,256]{1,0:T(8,128)(2,1)}, u32[]{:S(2)}) copy-start(bf16[33792,256]{1,0:T(8,128)(2,1)} %all-gather.3.cloned.1.call-done) | copy-start | bytes 51904516
  (2 other events, 1.2 us)
Sparse Core Ops, SparseCore 0:
  10.1 121.3 all-gather.2

commit v4 on v3

--- a/solution.py
+++ b/solution.py
@@ -37,7 +37,7 @@
     return lax.ppermute(x, "core", [(0, 1), (1, 0)])
 
 
-def local_call(kernel, shapes, args, *, scalars=0, far=(), scratch=(), limit=None):
+def local_call(kernel, shapes, args, *, scalars=0, far=(), scratch=(), limit=6 << 20):
     specs = [
         pl.BlockSpec(
             memory_space=pltpu.SMEM if i < scalars else pl.ANY if i in far else pltpu.VMEM
@@ -213,21 +213,12 @@
             out_ref[k, :, units + i : units + i + 1] = piece
 
 
-def last_kernel(units, hidden_ref, second_ref, weights_ref, out_ref, held, sems):
-    n = hidden_ref.shape[0]
-
-    def copy(k):
-        return pltpu.make_async_copy(
-            weights_ref.at[pl.ds(2 * k, 2), pl.ds(2 * units, units)], held.at[k], sems.at[k]
-        )
-
-    for k in range(n):
-        copy(k).start()
+def last_kernel(units, hidden_ref, second_ref, weights_ref, out_ref):
     total = jnp.zeros(out_ref.shape, F32)
-    for k in range(n):
-        copy(k).wait()
+    for k in range(hidden_ref.shape[0]):
         for i in range(2):
-            total += dot_nn(hidden_ref[k, :, i * PAD : i * PAD + units], held[k, i])
+            weight = weights_ref[2 * k + i, 2 * units : 3 * units]
+            total += dot_nn(hidden_ref[k, :, i * PAD : i * PAD + units], weight)
     out_ref[...] = (second_ref[...].astype(F32) + 0.5 * total).astype(BF16)
 
 
@@ -266,8 +257,8 @@
     later = lax.all_gather(later, TP, axis=0, tiled=False)
 
     gate_t, up_t = w_gate_pre.T, w_up_pre.T
+    stream = exchanged(jnp.broadcast_to(tokens[None], block), "z")
     other = from_partner(jnp.concatenate([gate_t, up_t, w_down_pre, w_out], axis=0))
-    stream = exchanged(jnp.broadcast_to(tokens[None], block), "z")
     (sent,) = local_call(
         gate_up_kernel, [(wide, BF16)], (stream, gain_pre[None], gate_t, up_t, other)
     )
@@ -329,7 +320,7 @@
         (exchanged(sent, "z"), first, gain_post[None], later),
         far=(3,),
         scratch=(pltpu.VMEM((n, 2, 2 * units, width), BF16), pltpu.SemaphoreType.DMA((n,))),
-        limit=24 << 20,
+        limit=46 << 20,
     )
     (hidden,) = local_call(
         functools.partial(hidden_kernel, units), [(narrow, BF16)], (exchanged(sent, KV),)
@@ -338,9 +329,7 @@
         functools.partial(last_kernel, units),
         [(tokens.shape, BF16)],
         (exchanged(hidden, KV), second, later),
-        far=(2,),
-        scratch=(pltpu.VMEM((n, 2, units, width), BF16), pltpu.SemaphoreType.DMA((n,))),
-        limit=16 << 20,
+        limit=22 << 20,
     )
     return (result, new_state.reshape(state.shape))
 

time: 221 us -> 187 us (0.85)
  Pallas kernels: 29.5 us -> 13.2 us
  local copies, waits for them, and re-layouts: 17.1 us -> 1.43 us
  blocking collectives: 77.8 us -> 74.3 us
  waiting for transfers between devices: 33.6 us -> 35.9 us
    pallas_call x10, Pallas kernels: 29.5 us -> 13.2 us  [local_call(): pl.pallas_call(kernel, out_shape=outs, in_specs=specs, out_specs=tuple((p...]
    unnamed x38 -> x28, local copies, waits for them, and re-layouts: 14.7 us -> 0.06 us
    all_to_all x6, blocking collectives: 77.8 us -> 74.3 us  [exchanged(): return lax.all_to_all(parts, axis, 0, 0, tiled=True)]
  transfers between devices with their start and end apart: 7 -> 7, of which waited for: 4 -> 5; matrix products, arithmetic and copies ran while one was open for 1% -> 1% of each run, Pallas kernels for 7% -> 3%
where the time goes in v4:
time: 187 us; the launch traced here: 183 us
  blocking collectives  74.3 us (40%)
  starting transfers between devices  40.8 us (22%)
  waiting for transfers between devices  35.9 us (19%)
  between operations  15.6 us (8%)
  Pallas kernels  13.2 us (7%)
  other arithmetic  2.17 us (1%)
    all_to_all x6, blocking collectives, exchanged(): return lax.all_to_all(parts, axis, 0, 0, tiled=True)  74.3 us
    all_to_all x4, waiting for transfers between devices, exchanged(): return lax.all_to_all(parts, axis, 0, 0, tiled=True)  35.6 us
    all_to_all x4, starting transfers between devices, exchanged(): return lax.all_to_all(parts, axis, 0, 0, tiled=True)  25.7 us
    ppermute x2, starting transfers between devices, from_partner(): return lax.ppermute(x, 'core', [(0, 1), (1, 0)])  15.1 us
    pallas_call x10, Pallas kernels, local_call(): pl.pallas_call(kernel, out_shape=outs, in_specs=specs, out_specs=tuple((p...  13.2 us
  transfers between devices with their start and end apart: 7, of which 5 were waited for; matrix products, arithmetic and copies ran while one was open for 1% of the time, Pallas kernels for 3%

profile of v4, /device:TPU:1, one launch (start us, length us, event | category | flops | bytes accessed | tf_op | source)
XLA Modules:
  0.0 183.5 jit_solution(2373447095814320428)
XLA Ops:
  7.3 2.1 %pad_maximum_fusion.1 = bf16[1056,256]{1,0:T(8,128)(2,1)} fusion(bf16[352,256]{1,0:T(8,128)(2,1)} %param.39, bf16[352,256]{1,0:T(8,128)(2,1)} %bitcast.34, bf16[352,256]{1,0:T(8,128)(2,1)} %bitcast.35), kind=kLoop, calls=%fused_computation.1 | loop fusion | flops 1622016 | bytes 1081344 | tf_op jit(solution)/shard_map/concatenate | solution.py:256
  9.5 8.7 %collective-permute-start = (bf16[1184,256]{1,0:T(8,128)(2,1)S(1)}, bf16[1184,256]{1,0:T(8,128)(2,1)S(1)}, u32[]{:S(2)}, u32[]{:S(2)}) collective-permute-start(bf16[1184,256]{1,0:T(8,128)(2,1)S(1)} %pad_maximum_fusion), channel_id=1, source_target_pairs={{0,1},{1,0},{2,3},{3,2},{4,5},{5,4},{6,7},{7,6},{8,9},{9,8},{10,11... | collective-permute-start | bytes 1818632 | tf_op jit(solution)/shard_map/ppermute | solution.py:37
  18.9 9.6 %all-to-all-start = ((bf16[16,8,256]{2,1,0:T(8,128)(2,1)}), bf16[16,8,256]{2,1,0:T(8,128)(2,1)S(1)}, u32[]{:S(2)}, u32[]{:S(2)}) async-start(bf16[16,8,256]{2,1,0:T(8,128)(2,1)} %broadcast_in_dim.24), calls=%async_computation | async-start | bytes 131072 | tf_op jit(solution)/shard_map/all_to_all | solution.py:33
  28.5 11.6 %all-to-all-done.rows_ref = bf16[16,8,256]{2,1,0:T(8,128)(2,1)S(1)} async-done(((bf16[16,8,256]{2,1,0:T(8,128)(2,1)}), bf16[16,8,256]{2,1,0:T(8,128)(2,1)S(1)}, u32[]{:S(2)}, u32[]{:S(2)}) %all-to-all-start) | async-done | bytes 65568 | tf_op jit(solution)/shard_map/all_to_all | solution.py:33
  40.5 14.8 %all_to_all.50.parts_ref = bf16[16,8,1536]{2,1,0:T(8,128)(2,1)S(1)} all-to-all(bf16[16,8,1536]{2,1,0:T(8,128)(2,1)S(1)} %shard_map.203), channel_id=1, replica_groups=mesh['kv_0'=4,'kv_1'=4,'z'=16,'core'=2] {'kv_0','kv_1'}, dimensions={0} | all-to-all | bytes 786432 | tf_op jit(solution)/shard_map/all_to_all | solution.py:33
  55.5 10.0 %all_to_all.51.hidden_ref = bf16[16,8,768]{2,1,0:T(8,128)(2,1)S(1)} all-to-all(bf16[16,8,768]{2,1,0:T(8,128)(2,1)S(1)} %shard_map.204), channel_id=1, replica_groups=mesh['kv_0'=4,'kv_1'=4,'z'=16,'core'=2] {'kv_0','kv_1'}, dimensions={0} | all-to-all | bytes 393216 | tf_op jit(solution)/shard_map/all_to_all | solution.py:33
  65.8 17.1 %all_to_all.52.parts_ref = bf16[16,8,256]{2,1,0:T(8,128)(2,1)S(1)} all-to-all(bf16[16,8,256]{2,1,0:T(8,128)(2,1)S(1)} %shard_map.205), channel_id=1, replica_groups=mesh['kv_0'=4,'kv_1'=4,'z'=16,'core'=2] {'z'}, dimensions={0} | all-to-all | bytes 131072 | tf_op jit(solution)/shard_map/all_to_all | solution.py:33
  82.9 0.7 shard_map.206
  83.5 3.5 %all-to-all-start.4 = ((bf16[16,8,256]{2,1,0:T(8,128)(2,1)}), bf16[16,8,256]{2,1,0:T(8,128)(2,1)S(1)}, u32[]{:S(2)}, u32[]{:S(2)}) async-start(bf16[16,8,256]{2,1,0:T(8,128)(2,1)} %get-tuple-element.8), calls=%async_computation.4 | async-start | bytes 131072 | tf_op jit(solution)/shard_map/all_to_all | solution.py:33
  87.1 6.3 %collective-permute-start.1 = (bf16[256,384]{1,0:T(8,128)(2,1)S(1)}, bf16[256,384]{1,0:T(8,128)(2,1)S(1)}, u32[]{:S(2)}, u32[]{:S(2)}) collective-permute-start(bf16[256,384]{1,0:T(8,128)(2,1)S(1)} %pad_maximum_fusion.2), channel_id=1, source_target_pairs={{0,1},{1,0},{2,3},{3,2},{4,5},{5,4},{6,7},{7,6},{8,9},{9,8},{10,11... | collective-permute-start | bytes 589832 | tf_op jit(solution)/shard_map/ppermute | solution.py:37
  93.4 0.7 dynamic-slice_bitcast_fusion
  94.5 4.7 %all-to-all-done.4.rows_ref = bf16[16,8,256]{2,1,0:T(8,128)(2,1)S(1)} async-done(((bf16[16,8,256]{2,1,0:T(8,128)(2,1)}), bf16[16,8,256]{2,1,0:T(8,128)(2,1)S(1)}, u32[]{:S(2)}, u32[]{:S(2)}) %all-to-all-start.4) | async-done | bytes 65568 | tf_op jit(solution)/shard_map/all_to_all | solution.py:33
  99.2 1.1 shard_map.207
  100.2 9.1 %all-to-all-start.5 = ((bf16[32,8,512]{2,1,0:T(8,128)(2,1)}), bf16[32,8,512]{2,1,0:T(8,128)(2,1)S(1)}, u32[]{:S(2)}, u32[]{:S(2)}) async-start(bf16[32,8,512]{2,1,0:T(8,128)(2,1)} %bitcast.5), calls=%async_computation.5 | async-start | bytes 524288 | tf_op jit(solution)/shard_map/all_to_all | solution.py:33
  110.7 7.7 %all-to-all-done.5 = bf16[32,8,512]{2,1,0:T(8,128)(2,1)S(1)} async-done(((bf16[32,8,512]{2,1,0:T(8,128)(2,1)}), bf16[32,8,512]{2,1,0:T(8,128)(2,1)S(1)}, u32[]{:S(2)}, u32[]{:S(2)}) %all-to-all-start.5) | async-done | bytes 262176 | tf_op jit(solution)/shard_map/all_to_all | solution.py:33
  118.3 2.0 %shard_map.208 = (f32[16,128,128]{2,1,0:T(8,128)}, bf16[16,16,128]{2,1,0:T(8,128)(2,1)S(1)}) custom-call(bf16[16,16,512]{2,1,0:T(8,128)(2,1)S(1)} %bitcast.26, f32[16,128,128]{2,1,0:T(8,128)S(1)} %bitcast.25, f32[1,1]{1,0:T(1,128)} %bitcast.21.base_ref, f32[1,1]{1,0:T(1,128)} %bitcast.22.shift_ref, bf16[1,128]{1,0:T(2,128)(2,1)S(1)} %bitcast.33), custom_call_target="tpu_custom_call" | custom-call | tf_op jit(solution)/shard_map/pallas_call | solution.py:48
  120.3 10.9 %all_to_all.53 = bf16[32,8,128]{2,1,0:T(8,128)(2,1)S(1)} all-to-all(bf16[32,8,128]{2,1,0:T(8,128)(2,1)S(1)} %bitcast.32), channel_id=1, replica_groups=mesh['kv_0'=4,'kv_1'=4,'z'=16,'core'=2] {'kv_0','kv_1','core'}, dimensions={0} | all-to-all | bytes 131072 | tf_op jit(solution)/shard_map/all_to_all | solution.py:33
  131.2 0.8 shard_map.209
  132.0 3.5 %all-to-all-start.7 = ((bf16[16,8,256]{2,1,0:T(8,128)(2,1)}), bf16[16,8,256]{2,1,0:T(8,128)(2,1)S(1)}, u32[]{:S(2)}, u32[]{:S(2)}) async-start(bf16[16,8,256]{2,1,0:T(8,128)(2,1)} %shard_map.209), calls=%async_computation.7 | async-start | bytes 131072 | tf_op jit(solution)/shard_map/all_to_all | solution.py:33
  135.5 11.6 %all-to-all-done.7.parts_ref = bf16[16,8,256]{2,1,0:T(8,128)(2,1)S(1)} async-done(((bf16[16,8,256]{2,1,0:T(8,128)(2,1)}), bf16[16,8,256]{2,1,0:T(8,128)(2,1)S(1)}, u32[]{:S(2)}, u32[]{:S(2)}) %all-to-all-start.7) | async-done | bytes 65568 | tf_op jit(solution)/shard_map/all_to_all | solution.py:33
  147.2 6.3 %shard_map.210 = (bf16[16,8,1536]{2,1,0:T(8,128)(2,1)S(1)}, bf16[8,256]{1,0:T(8,128)(2,1)S(1)}) custom-call(bf16[16,8,256]{2,1,0:T(8,128)(2,1)S(1)} %all-to-all-done.7.parts_ref, bf16[8,256]{1,0:T(8,128)(2,1)S(1)} %get-tuple-element.10.first_ref, bf16[1,256]{1,0:T(2,128)(2,1)S(1)} %broadcast_in_dim.30.gain_ref, bf16[32,1056,256]{2,1,0:T(8,128)(2,1)} %bitcast.23), custom_call_target="tpu_custom_call" | custom-call | tf_op jit(solution)/shard_map/pallas_call | solution.py:48
  153.5 11.7 %all_to_all.54.parts_ref = bf16[16,8,1536]{2,1,0:T(8,128)(2,1)S(1)} all-to-all(bf16[16,8,1536]{2,1,0:T(8,128)(2,1)S(1)} %get-tuple-element.11), channel_id=1, replica_groups=mesh['kv_0'=4,'kv_1'=4,'z'=16,'core'=2] {'kv_0','kv_1'}, dimensions={0} | all-to-all | bytes 786432 | tf_op jit(solution)/shard_map/all_to_all | solution.py:33
  165.4 9.8 %all_to_all.55.hidden_ref = bf16[16,8,768]{2,1,0:T(8,128)(2,1)S(1)} all-to-all(bf16[16,8,768]{2,1,0:T(8,128)(2,1)S(1)} %shard_map.211), channel_id=1, replica_groups=mesh['kv_0'=4,'kv_1'=4,'z'=16,'core'=2] {'kv_0','kv_1'}, dimensions={0} | all-to-all | bytes 393216 | tf_op jit(solution)/shard_map/all_to_all | solution.py:33
  175.1 1.5 shard_map.212
  (44 shorter events, 2.1 us)
Async XLA Ops:
  7.2 2.2 %copy-start.2 = (bf16[256,352]{0,1:T(8,128)(2,1)S(1)}, bf16[256,352]{0,1:T(8,128)(2,1)}, u32[]{:S(2)}) copy-start(bf16[256,352]{0,1:T(8,128)(2,1)} %param.23) | copy-start | bytes 540676
  7.2 2.2 %copy-start.3 = (bf16[256,352]{0,1:T(8,128)(2,1)S(1)}, bf16[256,352]{0,1:T(8,128)(2,1)}, u32[]{:S(2)}) copy-start(bf16[256,352]{0,1:T(8,128)(2,1)} %param.24) | copy-start | bytes 540676
  7.2 2.2 %copy-start.4 = (bf16[352,256]{1,0:T(8,128)(2,1)S(1)}, bf16[352,256]{1,0:T(8,128)(2,1)}, u32[]{:S(2)}) copy-start(bf16[352,256]{1,0:T(8,128)(2,1)} %own_ref.3) | copy-start | bytes 540676
  7.2 2.2 %copy-start.8 = (bf16[128,256]{1,0:T(8,128)(2,1)S(1)}, bf16[128,256]{1,0:T(8,128)(2,1)}, u32[]{:S(2)}) copy-start(bf16[128,256]{1,0:T(8,128)(2,1)} %own_ref.5) | copy-start | bytes 196612
  7.2 140.0 %all-gather.3.cloned.1.call-start = ((), (), s32[]{:S(2)}) async-start(), calls=%async_computation.10 | async-start | bytes 17842176 | tf_op jit(solution)/shard_map/all_gather | solution.py:257
  7.3 11.0 %copy-start.9 = (bf16[8,256]{1,0:T(8,128)(2,1)S(1)}, bf16[8,256]{1,0:T(8,128)(2,1)}, u32[]{:S(2)}) copy-start(bf16[8,256]{1,0:T(8,128)(2,1)} %own_ref.4) | copy-start | bytes 12292
  9.3 19.1 %copy-start.11 = (bf16[256]{0:T(256)(128)(2,1)S(1)}, bf16[256]{0:T(256)(128)(2,1)}, u32[]{:S(2)}) copy-start(bf16[256]{0:T(256)(128)(2,1)} %param.22) | copy-start | bytes 1540
  9.5 30.6 %collective-permute-start = (bf16[1184,256]{1,0:T(8,128)(2,1)S(1)}, bf16[1184,256]{1,0:T(8,128)(2,1)S(1)}, u32[]{:S(2)}, u32[]{:S(2)}) collective-permute-start(bf16[1184,256]{1,0:T(8,128)(2,1)S(1)} %pad_maximum_fusion), channel_id=1, source_target_pairs={{0,1},{1,0},{2,3},{3,2},{4,5},{5,4},{6,7},{7,6},{8,9},{9,8},{10,11... | collective-permute-start | bytes 1818632 | tf_op jit(solution)/shard_map/ppermute | solution.py:37
  18.9 21.2 %all-to-all-start = ((bf16[16,8,256]{2,1,0:T(8,128)(2,1)}), bf16[16,8,256]{2,1,0:T(8,128)(2,1)S(1)}, u32[]{:S(2)}, u32[]{:S(2)}) async-start(bf16[16,8,256]{2,1,0:T(8,128)(2,1)} %broadcast_in_dim.24), calls=%async_computation | async-start | bytes 131072 | tf_op jit(solution)/shard_map/all_to_all | solution.py:33
  55.3 31.8 %copy-start.5 = (bf16[256,128]{1,0:T(8,128)(2,1)S(1)}, bf16[256,128]{1,0:T(8,128)(2,1)}, u32[]{:S(2)}) copy-start(bf16[256,128]{1,0:T(8,128)(2,1)} %q_ref.1) | copy-start | bytes 196612
  55.3 31.8 %copy-start.6 = (bf16[256,128]{1,0:T(8,128)(2,1)S(1)}, bf16[256,128]{1,0:T(8,128)(2,1)}, u32[]{:S(2)}) copy-start(bf16[256,128]{1,0:T(8,128)(2,1)} %k_ref.1) | copy-start | bytes 196612
  55.3 31.8 %copy-start.7 = (bf16[256,128]{1,0:T(8,128)(2,1)S(1)}, bf16[256,128]{1,0:T(8,128)(2,1)}, u32[]{:S(2)}) copy-start(bf16[256,128]{1,0:T(8,128)(2,1)} %v_ref.1) | copy-start | bytes 196612
  55.5 38.0 %copy-start.12 = (bf16[256]{0:T(256)(128)(2,1)S(1)}, bf16[256]{0:T(256)(128)(2,1)}, u32[]{:S(2)}) copy-start(bf16[256]{0:T(256)(128)(2,1)} %param.26) | copy-start | bytes 1540
  65.7 52.6 %copy-start.1 = (f32[16,1,128,128]{3,2,1,0:T(8,128)S(1)}, f32[16,1,128,128]{3,2,1,0:T(8,128)}, u32[]{:S(2)}) copy-start(f32[16,1,128,128]{3,2,1,0:T(8,128)} %param.21) | copy-start | bytes 3145732
  65.7 52.6 %copy-start.10 = (bf16[128]{0:T(256)(128)(2,1)S(1)}, bf16[128]{0:T(256)(128)(2,1)}, u32[]{:S(2)}) copy-start(bf16[128]{0:T(256)(128)(2,1)} %param.34) | copy-start | bytes 772
  83.5 15.6 %all-to-all-start.4 = ((bf16[16,8,256]{2,1,0:T(8,128)(2,1)}), bf16[16,8,256]{2,1,0:T(8,128)(2,1)S(1)}, u32[]{:S(2)}, u32[]{:S(2)}) async-start(bf16[16,8,256]{2,1,0:T(8,128)(2,1)} %get-tuple-element.8), calls=%async_computation.4 | async-start | bytes 131072 | tf_op jit(solution)/shard_map/all_to_all | solution.py:33
  87.1 7.4 %collective-permute-start.1 = (bf16[256,384]{1,0:T(8,128)(2,1)S(1)}, bf16[256,384]{1,0:T(8,128)(2,1)S(1)}, u32[]{:S(2)}, u32[]{:S(2)}) collective-permute-start(bf16[256,384]{1,0:T(8,128)(2,1)S(1)} %pad_maximum_fusion.2), channel_id=1, source_target_pairs={{0,1},{1,0},{2,3},{3,2},{4,5},{5,4},{6,7},{7,6},{8,9},{9,8},{10,11... | collective-permute-start | bytes 589832 | tf_op jit(solution)/shard_map/ppermute | solution.py:37
  100.2 18.1 %all-to-all-start.5 = ((bf16[32,8,512]{2,1,0:T(8,128)(2,1)}), bf16[32,8,512]{2,1,0:T(8,128)(2,1)S(1)}, u32[]{:S(2)}, u32[]{:S(2)}) async-start(bf16[32,8,512]{2,1,0:T(8,128)(2,1)} %bitcast.5), calls=%async_computation.5 | async-start | bytes 524288 | tf_op jit(solution)/shard_map/all_to_all | solution.py:33
  109.3 26.2 %copy-start.13 = (bf16[256]{0:T(256)(128)(2,1)S(1)}, bf16[256]{0:T(256)(128)(2,1)}, u32[]{:S(2)}) copy-start(bf16[256]{0:T(256)(128)(2,1)} %param.36) | copy-start | bytes 1540
  132.0 15.2 %all-to-all-start.7 = ((bf16[16,8,256]{2,1,0:T(8,128)(2,1)}), bf16[16,8,256]{2,1,0:T(8,128)(2,1)S(1)}, u32[]{:S(2)}, u32[]{:S(2)}) async-start(bf16[16,8,256]{2,1,0:T(8,128)(2,1)} %shard_map.209), calls=%async_computation.7 | async-start | bytes 131072 | tf_op jit(solution)/shard_map/all_to_all | solution.py:33
  147.2 28.0 %copy-start = (bf16[33792,256]{1,0:T(8,128)(2,1)S(1)}, bf16[33792,256]{1,0:T(8,128)(2,1)}, u32[]{:S(2)}) copy-start(bf16[33792,256]{1,0:T(8,128)(2,1)} %all-gather.3.cloned.1.call-done) | copy-start | bytes 51904516
Sparse Core Ops, SparseCore 0:
  10.1 121.3 all-gather.2

commit v5 on v3

--- a/solution.py
+++ b/solution.py
@@ -37,7 +37,7 @@
     return lax.ppermute(x, "core", [(0, 1), (1, 0)])
 
 
-def local_call(kernel, shapes, args, *, scalars=0, far=(), scratch=(), limit=None):
+def local_call(kernel, shapes, args, *, scalars=0, far=(), scratch=(), limit=6 << 20):
     specs = [
         pl.BlockSpec(
             memory_space=pltpu.SMEM if i < scalars else pl.ANY if i in far else pltpu.VMEM
@@ -191,9 +191,7 @@
     n, rows, _ = out_ref.shape
 
     def copy(k):
-        return pltpu.make_async_copy(
-            weights_ref.at[pl.ds(2 * k, 2), pl.ds(0, 2 * units)], held.at[k], sems.at[k]
-        )
+        return pltpu.make_async_copy(weights_ref.at[pl.ds(2 * k, 2)], held.at[k], sems.at[k])
 
     for k in range(n):
         copy(k).start()
@@ -204,22 +202,22 @@
     scaled = (stream * gain_ref[...].astype(F32)).astype(BF16)
     pieces = in_three(jnp.sum(stream * stream, axis=1, keepdims=True))
     for k in range(n):
+        for i in range(4):
+            out_ref[k, :, i * PAD + units : (i + 1) * PAD] = jnp.zeros((rows, PAD - units), BF16)
+        for i, piece in enumerate(pieces):
+            out_ref[k, :, units + i : units + i + 1] = piece
+    for k in range(n):
         copy(k).wait()
         for i in range(4):
-            out_ref[k, :, i * PAD + units : (i + 1) * PAD] = jnp.zeros((rows, PAD - units), BF16)
             weight = held[k, i % 2, (i // 2) * units : (i // 2 + 1) * units]
             out_ref[k, :, i * PAD : i * PAD + units] = dot_nt(scaled, weight).astype(BF16)
-        for i, piece in enumerate(pieces):
-            out_ref[k, :, units + i : units + i + 1] = piece
 
 
 def last_kernel(units, hidden_ref, second_ref, weights_ref, out_ref, held, sems):
     n = hidden_ref.shape[0]
 
     def copy(k):
-        return pltpu.make_async_copy(
-            weights_ref.at[pl.ds(2 * k, 2), pl.ds(2 * units, units)], held.at[k], sems.at[k]
-        )
+        return pltpu.make_async_copy(weights_ref.at[pl.ds(2 * k, 2)], held.at[k], sems.at[k])
 
     for k in range(n):
         copy(k).start()
@@ -262,12 +260,12 @@
     wide = (n, rows, 4 * PAD)
     narrow = (n, rows, 2 * PAD)
 
-    later = jnp.concatenate([w_gate_post.T, w_up_post.T, w_down_post], axis=0)
-    later = lax.all_gather(later, TP, axis=0, tiled=False)
-
     gate_t, up_t = w_gate_pre.T, w_up_pre.T
+    stream = exchanged(jnp.broadcast_to(tokens[None], block), "z")
     other = from_partner(jnp.concatenate([gate_t, up_t, w_down_pre, w_out], axis=0))
-    stream = exchanged(jnp.broadcast_to(tokens[None], block), "z")
+    wide_own = jnp.concatenate([w_gate_post.T, w_up_post.T], axis=0)
+    wide_all = lax.all_gather(wide_own, TP, axis=0, tiled=False)
+    down_all = lax.all_gather(w_down_post, TP, axis=0, tiled=False)
     (sent,) = local_call(
         gate_up_kernel, [(wide, BF16)], (stream, gain_pre[None], gate_t, up_t, other)
     )
@@ -319,6 +317,7 @@
         scratch=(pltpu.VMEM((seqs, dim), F32),),
     )
     heads = exchanged(sent.reshape(2 * n, rows, dim), KVC).reshape(n, 2 * rows, dim)
+    heads, gain_last = lax.optimization_barrier((heads, gain_post[None]))
     (sent,) = local_call(
         out_kernel, [(block, BF16)], (core, heads, w_out, other), scalars=1
     )
@@ -326,10 +325,10 @@
     sent, second = local_call(
         functools.partial(wide_kernel, units),
         [(wide, BF16), (tokens.shape, BF16)],
-        (exchanged(sent, "z"), first, gain_post[None], later),
+        (exchanged(sent, "z"), first, gain_last, wide_all),
         far=(3,),
         scratch=(pltpu.VMEM((n, 2, 2 * units, width), BF16), pltpu.SemaphoreType.DMA((n,))),
-        limit=24 << 20,
+        limit=46 << 20,
     )
     (hidden,) = local_call(
         functools.partial(hidden_kernel, units), [(narrow, BF16)], (exchanged(sent, KV),)
@@ -337,10 +336,10 @@
     (result,) = local_call(
         functools.partial(last_kernel, units),
         [(tokens.shape, BF16)],
-        (exchanged(hidden, KV), second, later),
+        (exchanged(hidden, KV), second, down_all),
         far=(2,),
         scratch=(pltpu.VMEM((n, 2, units, width), BF16), pltpu.SemaphoreType.DMA((n,))),
-        limit=16 << 20,
+        limit=50 << 20,
     )
     return (result, new_state.reshape(state.shape))
 

time: 221 us -> 193 us (0.87)
  local copies, waits for them, and re-layouts: 17.1 us -> 1.45 us
  Pallas kernels: 29.5 us -> 16 us
  waiting for transfers between devices: 33.6 us -> 44.6 us
  blocking collectives: 77.8 us -> 67.3 us
  starting transfers between devices: 42.2 us -> 45.2 us
    unnamed x38 -> x26, local copies, waits for them, and re-layouts: 14.7 us -> 0.06 us
    pallas_call x10, Pallas kernels: 29.5 us -> 16 us  [local_call(): pl.pallas_call(kernel, out_shape=outs, in_specs=specs, out_specs=tuple((p...]
    all_gather x1 -> x2, waiting for transfers between devices: 0.01 us -> 12.8 us  [the longest x1 12.8 us: on_device(): down_all = lax.all_gather(w_down_post, TP, axis=0, tiled=False)]
    all_to_all x6 -> x5, blocking collectives: 77.8 us -> 67.3 us  [exchanged(): return lax.all_to_all(parts, axis, 0, 0, tiled=True)]
    all_to_all x4 -> x5, starting transfers between devices: 26.4 us -> 29.6 us  [exchanged(): return lax.all_to_all(parts, axis, 0, 0, tiled=True)]
    all_to_all x4 -> x5, waiting for transfers between devices: 33.6 us -> 30.7 us  [exchanged(): return lax.all_to_all(parts, axis, 0, 0, tiled=True)]
  transfers between devices with their start and end apart: 7 -> 9, of which waited for: 4 -> 6; matrix products, arithmetic and copies ran while one was open for 1% -> 1% of each run, Pallas kernels for 7% -> 6%
where the time goes in v5:
time: 193 us; the launch traced here: 192 us
  blocking collectives  67.3 us (35%)
  starting transfers between devices  45.2 us (23%)
  waiting for transfers between devices  44.6 us (23%)
  Pallas kernels  16 us (8%)
  between operations  15.7 us (8%)
  other arithmetic  2 us (1%)
    all_to_all x5, blocking collectives, exchanged(): return lax.all_to_all(parts, axis, 0, 0, tiled=True)  67.3 us
    all_to_all x5, waiting for transfers between devices, exchanged(): return lax.all_to_all(parts, axis, 0, 0, tiled=True)  30.7 us
    all_to_all x5, starting transfers between devices, exchanged(): return lax.all_to_all(parts, axis, 0, 0, tiled=True)  29.6 us
    pallas_call x10, Pallas kernels, local_call(): pl.pallas_call(kernel, out_shape=outs, in_specs=specs, out_specs=tuple((p...  16 us
    ppermute x2, starting transfers between devices, from_partner(): return lax.ppermute(x, 'core', [(0, 1), (1, 0)])  15.5 us
    all_gather x1, waiting for transfers between devices, on_device(): down_all = lax.all_gather(w_down_post, TP, axis=0, tiled=False)  12.8 us
  transfers between devices with their start and end apart: 9, of which 6 were waited for; matrix products, arithmetic and copies ran while one was open for 1% of the time, Pallas kernels for 6%

profile of v5, /device:TPU:1, one launch (start us, length us, event | category | flops | bytes accessed | tf_op | source)
XLA Modules:
  0.0 192.3 jit_solution(643011723726001832)
XLA Ops:
  7.3 1.9 %pad_maximum_fusion.1 = bf16[704,256]{1,0:T(8,128)(2,1)} fusion(bf16[352,256]{1,0:T(8,128)(2,1)} %bitcast.34, bf16[352,256]{1,0:T(8,128)(2,1)} %bitcast.35), kind=kLoop, calls=%fused_computation.1 | loop fusion | flops 720896 | bytes 720896 | tf_op jit(solution)/shard_map/concatenate | solution.py:266
  10.1 8.7 %collective-permute-start = (bf16[1184,256]{1,0:T(8,128)(2,1)S(1)}, bf16[1184,256]{1,0:T(8,128)(2,1)S(1)}, u32[]{:S(2)}, u32[]{:S(2)}) collective-permute-start(bf16[1184,256]{1,0:T(8,128)(2,1)S(1)} %pad_maximum_fusion), channel_id=1, source_target_pairs={{0,1},{1,0},{2,3},{3,2},{4,5},{5,4},{6,7},{7,6},{8,9},{9,8},{10,11... | collective-permute-start | bytes 1818632 | tf_op jit(solution)/shard_map/ppermute | solution.py:37
  19.5 9.6 %all-to-all-start = ((bf16[16,8,256]{2,1,0:T(8,128)(2,1)}), bf16[16,8,256]{2,1,0:T(8,128)(2,1)S(1)}, u32[]{:S(2)}, u32[]{:S(2)}) async-start(bf16[16,8,256]{2,1,0:T(8,128)(2,1)} %broadcast_in_dim.24), calls=%async_computation | async-start | bytes 131072 | tf_op jit(solution)/shard_map/all_to_all | solution.py:33
  29.1 11.6 %all-to-all-done.rows_ref = bf16[16,8,256]{2,1,0:T(8,128)(2,1)S(1)} async-done(((bf16[16,8,256]{2,1,0:T(8,128)(2,1)}), bf16[16,8,256]{2,1,0:T(8,128)(2,1)S(1)}, u32[]{:S(2)}, u32[]{:S(2)}) %all-to-all-start) | async-done | bytes 65568 | tf_op jit(solution)/shard_map/all_to_all | solution.py:33
  41.1 14.8 %all_to_all.50.parts_ref = bf16[16,8,1536]{2,1,0:T(8,128)(2,1)S(1)} all-to-all(bf16[16,8,1536]{2,1,0:T(8,128)(2,1)S(1)} %shard_map.203), channel_id=1, replica_groups=mesh['kv_0'=4,'kv_1'=4,'z'=16,'core'=2] {'kv_0','kv_1'}, dimensions={0} | all-to-all | bytes 786432 | tf_op jit(solution)/shard_map/all_to_all | solution.py:33
  56.1 10.0 %all_to_all.51.hidden_ref = bf16[16,8,768]{2,1,0:T(8,128)(2,1)S(1)} all-to-all(bf16[16,8,768]{2,1,0:T(8,128)(2,1)S(1)} %shard_map.204), channel_id=1, replica_groups=mesh['kv_0'=4,'kv_1'=4,'z'=16,'core'=2] {'kv_0','kv_1'}, dimensions={0} | all-to-all | bytes 393216 | tf_op jit(solution)/shard_map/all_to_all | solution.py:33
  66.4 16.6 %all_to_all.52.parts_ref = bf16[16,8,256]{2,1,0:T(8,128)(2,1)S(1)} all-to-all(bf16[16,8,256]{2,1,0:T(8,128)(2,1)S(1)} %shard_map.205), channel_id=1, replica_groups=mesh['kv_0'=4,'kv_1'=4,'z'=16,'core'=2] {'z'}, dimensions={0} | all-to-all | bytes 131072 | tf_op jit(solution)/shard_map/all_to_all | solution.py:33
  83.6 3.5 %all-to-all-start.4 = ((bf16[16,8,256]{2,1,0:T(8,128)(2,1)}), bf16[16,8,256]{2,1,0:T(8,128)(2,1)S(1)}, u32[]{:S(2)}, u32[]{:S(2)}) async-start(bf16[16,8,256]{2,1,0:T(8,128)(2,1)} %get-tuple-element.10), calls=%async_computation.4 | async-start | bytes 131072 | tf_op jit(solution)/shard_map/all_to_all | solution.py:33
  87.1 6.7 %collective-permute-start.1 = (bf16[256,384]{1,0:T(8,128)(2,1)S(1)}, bf16[256,384]{1,0:T(8,128)(2,1)S(1)}, u32[]{:S(2)}, u32[]{:S(2)}) collective-permute-start(bf16[256,384]{1,0:T(8,128)(2,1)S(1)} %pad_maximum_fusion.2), channel_id=1, source_target_pairs={{0,1},{1,0},{2,3},{3,2},{4,5},{5,4},{6,7},{7,6},{8,9},{9,8},{10,11... | collective-permute-start | bytes 589832 | tf_op jit(solution)/shard_map/ppermute | solution.py:37
  93.9 0.7 dynamic-slice_bitcast_fusion
  95.1 4.2 %all-to-all-done.4.rows_ref = bf16[16,8,256]{2,1,0:T(8,128)(2,1)S(1)} async-done(((bf16[16,8,256]{2,1,0:T(8,128)(2,1)}), bf16[16,8,256]{2,1,0:T(8,128)(2,1)S(1)}, u32[]{:S(2)}, u32[]{:S(2)}) %all-to-all-start.4) | async-done | bytes 65568 | tf_op jit(solution)/shard_map/all_to_all | solution.py:33
  99.3 1.1 shard_map.207
  100.3 9.3 %all-to-all-start.5 = ((bf16[32,8,512]{2,1,0:T(8,128)(2,1)}), bf16[32,8,512]{2,1,0:T(8,128)(2,1)S(1)}, u32[]{:S(2)}, u32[]{:S(2)}) async-start(bf16[32,8,512]{2,1,0:T(8,128)(2,1)} %bitcast.5), calls=%async_computation.5 | async-start | bytes 524288 | tf_op jit(solution)/shard_map/all_to_all | solution.py:33
  110.9 7.6 %all-to-all-done.5 = bf16[32,8,512]{2,1,0:T(8,128)(2,1)S(1)} async-done(((bf16[32,8,512]{2,1,0:T(8,128)(2,1)}), bf16[32,8,512]{2,1,0:T(8,128)(2,1)S(1)}, u32[]{:S(2)}, u32[]{:S(2)}) %all-to-all-start.5) | async-done | bytes 262176 | tf_op jit(solution)/shard_map/all_to_all | solution.py:33
  118.5 2.0 %shard_map.208 = (f32[16,128,128]{2,1,0:T(8,128)}, bf16[16,16,128]{2,1,0:T(8,128)(2,1)}) custom-call(bf16[16,16,512]{2,1,0:T(8,128)(2,1)S(1)} %bitcast.25, f32[16,128,128]{2,1,0:T(8,128)S(1)} %bitcast.24, f32[1,1]{1,0:T(1,128)} %bitcast.22.base_ref, f32[1,1]{1,0:T(1,128)} %bitcast.23.shift_ref, bf16[1,128]{1,0:T(2,128)(2,1)S(1)} %bitcast.31), custom_call_target="tpu_custom_call" | custom-call | tf_op jit(solution)/shard_map/pallas_call | solution.py:48
  120.5 3.8 %all-to-all-start.6 = ((bf16[32,8,128]{2,1,0:T(8,128)(2,1)}), bf16[32,8,128]{2,1,0:T(8,128)(2,1)S(1)}, u32[]{:S(2)}, u32[]{:S(2)}) async-start(bf16[32,8,128]{2,1,0:T(8,128)(2,1)} %bitcast.11), calls=%async_computation.6 | async-start | bytes 131072 | tf_op jit(solution)/shard_map/all_to_all | solution.py:33
  124.3 7.3 %all-to-all-done.6 = bf16[32,8,128]{2,1,0:T(8,128)(2,1)S(1)} async-done(((bf16[32,8,128]{2,1,0:T(8,128)(2,1)}), bf16[32,8,128]{2,1,0:T(8,128)(2,1)S(1)}, u32[]{:S(2)}, u32[]{:S(2)}) %all-to-all-start.6) | async-done | bytes 65568 | tf_op jit(solution)/shard_map/all_to_all | solution.py:33
  131.8 14.7 %all_to_all.53.parts_ref = bf16[16,8,256]{2,1,0:T(8,128)(2,1)S(1)} all-to-all(bf16[16,8,256]{2,1,0:T(8,128)(2,1)S(1)} %shard_map.209), channel_id=1, replica_groups=mesh['kv_0'=4,'kv_1'=4,'z'=16,'core'=2] {'z'}, dimensions={0} | all-to-all | bytes 131072 | tf_op jit(solution)/shard_map/all_to_all | solution.py:33
  146.5 6.1 %shard_map.210 = (bf16[16,8,1536]{2,1,0:T(8,128)(2,1)S(1)}, bf16[8,256]{1,0:T(8,128)(2,1)S(1)}) custom-call(bf16[16,8,256]{2,1,0:T(8,128)(2,1)S(1)} %all_to_all.53.parts_ref, bf16[8,256]{1,0:T(8,128)(2,1)S(1)} %get-tuple-element.13.first_ref, bf16[1,256]{1,0:T(2,128)(2,1)S(1)} %broadcast_in_dim.30.gain_ref, bf16[32,704,256]{2,1,0:T(8,128)(2,1)} %bitcast.32), custom_call_target="tpu_custom_call" | custom-call | tf_op jit(solution)/shard_map/pallas_call | solution.py:48
  152.7 11.2 %all_to_all.54.parts_ref = bf16[16,8,1536]{2,1,0:T(8,128)(2,1)S(1)} all-to-all(bf16[16,8,1536]{2,1,0:T(8,128)(2,1)S(1)} %get-tuple-element.15), channel_id=1, replica_groups=mesh['kv_0'=4,'kv_1'=4,'z'=16,'core'=2] {'kv_0','kv_1'}, dimensions={0} | all-to-all | bytes 786432 | tf_op jit(solution)/shard_map/all_to_all | solution.py:33
  163.9 0.9 shard_map.211
  164.8 3.5 %all-to-all-start.9 = ((bf16[16,8,768]{2,1,0:T(8,128)(2,1)}), bf16[16,8,768]{2,1,0:T(8,128)(2,1)S(1)}, u32[]{:S(2)}, u32[]{:S(2)}) async-start(bf16[16,8,768]{2,1,0:T(8,128)(2,1)} %shard_map.211), calls=%async_computation.9 | async-start | bytes 393216 | tf_op jit(solution)/shard_map/all_to_all | solution.py:33
  168.3 12.8 %all-gather.7.cloned.1.call-done = bf16[11264,256]{1,0:T(8,128)(2,1)} async-done(((bf16[352,256]{1,0:T(8,128)(2,1)}), bf16[11264,256]{1,0:T(8,128)(2,1)}) %all-gather.7.cloned.1.call-update) | async-done | bytes 5767184 | tf_op jit(solution)/shard_map/all_gather | solution.py:268
  181.1 4.3 %shard_map.212 = bf16[8,256]{1,0:T(8,128)(2,1)} custom-call(bf16[16,8,768]{2,1,0:T(8,128)(2,1)S(1)} %all-to-all-done.9.hidden_ref, bf16[8,256]{1,0:T(8,128)(2,1)S(1)} %get-tuple-element.16.second_ref, bf16[32,352,256]{2,1,0:T(8,128)(2,1)} %bitcast.33), custom_call_target="tpu_custom_call" | custom-call | tf_op jit(solution)/shard_map/pallas_call | solution.py:48
  (46 shorter events, 3.6 us)
Async XLA Ops:
  7.2 2.8 %copy-start.1 = (bf16[256,352]{0,1:T(8,128)(2,1)S(1)}, bf16[256,352]{0,1:T(8,128)(2,1)}, u32[]{:S(2)}) copy-start(bf16[256,352]{0,1:T(8,128)(2,1)} %param.23) | copy-start | bytes 540676
  7.2 2.8 %copy-start.2 = (bf16[256,352]{0,1:T(8,128)(2,1)S(1)}, bf16[256,352]{0,1:T(8,128)(2,1)}, u32[]{:S(2)}) copy-start(bf16[256,352]{0,1:T(8,128)(2,1)} %param.24) | copy-start | bytes 540676
  7.2 2.8 %copy-start.3 = (bf16[352,256]{1,0:T(8,128)(2,1)S(1)}, bf16[352,256]{1,0:T(8,128)(2,1)}, u32[]{:S(2)}) copy-start(bf16[352,256]{1,0:T(8,128)(2,1)} %own_ref.3) | copy-start | bytes 540676
  7.2 2.8 %copy-start.7 = (bf16[128,256]{1,0:T(8,128)(2,1)S(1)}, bf16[128,256]{1,0:T(8,128)(2,1)}, u32[]{:S(2)}) copy-start(bf16[128,256]{1,0:T(8,128)(2,1)} %own_ref.5) | copy-start | bytes 196612
  7.2 139.3 %all-gather.5.cloned.1.call-start = ((), (), s32[]{:S(2)}) async-start(), calls=%async_computation.10 | async-start | bytes 11894784 | tf_op jit(solution)/shard_map/all_gather | solution.py:267
  7.3 11.6 %copy-start.8 = (bf16[8,256]{1,0:T(8,128)(2,1)S(1)}, bf16[8,256]{1,0:T(8,128)(2,1)}, u32[]{:S(2)}) copy-start(bf16[8,256]{1,0:T(8,128)(2,1)} %own_ref.4) | copy-start | bytes 12292
  7.3 21.8 %copy-start.10 = (bf16[256]{0:T(256)(128)(2,1)S(1)}, bf16[256]{0:T(256)(128)(2,1)}, u32[]{:S(2)}) copy-start(bf16[256]{0:T(256)(128)(2,1)} %param.22) | copy-start | bytes 1540
  9.2 171.9 %all-gather.7.cloned.1.call-start = ((), (), s32[]{:S(2)}) async-start(), calls=%async_computation.11 | async-start | bytes 5947392 | tf_op jit(solution)/shard_map/all_gather | solution.py:268
  10.1 30.6 %collective-permute-start = (bf16[1184,256]{1,0:T(8,128)(2,1)S(1)}, bf16[1184,256]{1,0:T(8,128)(2,1)S(1)}, u32[]{:S(2)}, u32[]{:S(2)}) collective-permute-start(bf16[1184,256]{1,0:T(8,128)(2,1)S(1)} %pad_maximum_fusion), channel_id=1, source_target_pairs={{0,1},{1,0},{2,3},{3,2},{4,5},{5,4},{6,7},{7,6},{8,9},{9,8},{10,11... | collective-permute-start | bytes 1818632 | tf_op jit(solution)/shard_map/ppermute | solution.py:37
  19.5 21.2 %all-to-all-start = ((bf16[16,8,256]{2,1,0:T(8,128)(2,1)}), bf16[16,8,256]{2,1,0:T(8,128)(2,1)S(1)}, u32[]{:S(2)}, u32[]{:S(2)}) async-start(bf16[16,8,256]{2,1,0:T(8,128)(2,1)} %broadcast_in_dim.24), calls=%async_computation | async-start | bytes 131072 | tf_op jit(solution)/shard_map/all_to_all | solution.py:33
  55.9 31.2 %copy-start.4 = (bf16[256,128]{1,0:T(8,128)(2,1)S(1)}, bf16[256,128]{1,0:T(8,128)(2,1)}, u32[]{:S(2)}) copy-start(bf16[256,128]{1,0:T(8,128)(2,1)} %q_ref.1) | copy-start | bytes 196612
  55.9 31.2 %copy-start.5 = (bf16[256,128]{1,0:T(8,128)(2,1)S(1)}, bf16[256,128]{1,0:T(8,128)(2,1)}, u32[]{:S(2)}) copy-start(bf16[256,128]{1,0:T(8,128)(2,1)} %k_ref.1) | copy-start | bytes 196612
  55.9 31.2 %copy-start.6 = (bf16[256,128]{1,0:T(8,128)(2,1)S(1)}, bf16[256,128]{1,0:T(8,128)(2,1)}, u32[]{:S(2)}) copy-start(bf16[256,128]{1,0:T(8,128)(2,1)} %v_ref.1) | copy-start | bytes 196612
  56.1 37.8 %copy-start.11 = (bf16[256]{0:T(256)(128)(2,1)S(1)}, bf16[256]{0:T(256)(128)(2,1)}, u32[]{:S(2)}) copy-start(bf16[256]{0:T(256)(128)(2,1)} %param.26) | copy-start | bytes 1540
  66.3 52.2 %copy-start = (f32[16,1,128,128]{3,2,1,0:T(8,128)S(1)}, f32[16,1,128,128]{3,2,1,0:T(8,128)}, u32[]{:S(2)}) copy-start(f32[16,1,128,128]{3,2,1,0:T(8,128)} %param.21) | copy-start | bytes 3145732
  66.3 52.2 %copy-start.9 = (bf16[128]{0:T(256)(128)(2,1)S(1)}, bf16[128]{0:T(256)(128)(2,1)}, u32[]{:S(2)}) copy-start(bf16[128]{0:T(256)(128)(2,1)} %param.34) | copy-start | bytes 772
  83.6 15.7 %all-to-all-start.4 = ((bf16[16,8,256]{2,1,0:T(8,128)(2,1)}), bf16[16,8,256]{2,1,0:T(8,128)(2,1)S(1)}, u32[]{:S(2)}, u32[]{:S(2)}) async-start(bf16[16,8,256]{2,1,0:T(8,128)(2,1)} %get-tuple-element.10), calls=%async_computation.4 | async-start | bytes 131072 | tf_op jit(solution)/shard_map/all_to_all | solution.py:33
  87.1 7.9 %collective-permute-start.1 = (bf16[256,384]{1,0:T(8,128)(2,1)S(1)}, bf16[256,384]{1,0:T(8,128)(2,1)S(1)}, u32[]{:S(2)}, u32[]{:S(2)}) collective-permute-start(bf16[256,384]{1,0:T(8,128)(2,1)S(1)} %pad_maximum_fusion.2), channel_id=1, source_target_pairs={{0,1},{1,0},{2,3},{3,2},{4,5},{5,4},{6,7},{7,6},{8,9},{9,8},{10,11... | collective-permute-start | bytes 589832 | tf_op jit(solution)/shard_map/ppermute | solution.py:37
  99.3 25.0 %copy-start.12 = (bf16[256]{0:T(256)(128)(2,1)S(1)}, bf16[256]{0:T(256)(128)(2,1)}, u32[]{:S(2)}) copy-start(bf16[256]{0:T(256)(128)(2,1)} %param.36) | copy-start | bytes 1540
  100.3 18.2 %all-to-all-start.5 = ((bf16[32,8,512]{2,1,0:T(8,128)(2,1)}), bf16[32,8,512]{2,1,0:T(8,128)(2,1)S(1)}, u32[]{:S(2)}, u32[]{:S(2)}) async-start(bf16[32,8,512]{2,1,0:T(8,128)(2,1)} %bitcast.5), calls=%async_computation.5 | async-start | bytes 524288 | tf_op jit(solution)/shard_map/all_to_all | solution.py:33
  120.5 11.1 %all-to-all-start.6 = ((bf16[32,8,128]{2,1,0:T(8,128)(2,1)}), bf16[32,8,128]{2,1,0:T(8,128)(2,1)S(1)}, u32[]{:S(2)}, u32[]{:S(2)}) async-start(bf16[32,8,128]{2,1,0:T(8,128)(2,1)} %bitcast.11), calls=%async_computation.6 | async-start | bytes 131072 | tf_op jit(solution)/shard_map/all_to_all | solution.py:33
  164.8 16.3 %all-to-all-start.9 = ((bf16[16,8,768]{2,1,0:T(8,128)(2,1)}), bf16[16,8,768]{2,1,0:T(8,128)(2,1)S(1)}, u32[]{:S(2)}, u32[]{:S(2)}) async-start(bf16[16,8,768]{2,1,0:T(8,128)(2,1)} %shard_map.211), calls=%async_computation.9 | async-start | bytes 393216 | tf_op jit(solution)/shard_map/all_to_all | solution.py:33
Sparse Core Ops, SparseCore 0:
  10.1 94.8 all-gather.4
  107.1 73.8 all-gather.6

commit v6 on v4

--- a/solution.py
+++ b/solution.py
@@ -19,6 +19,7 @@
 
 
 PAD = 384
+AHEAD = 5
 
 
 def dot_nn(a, b):
@@ -195,7 +196,7 @@
             weights_ref.at[pl.ds(2 * k, 2), pl.ds(0, 2 * units)], held.at[k], sems.at[k]
         )
 
-    for k in range(n):
+    for k in range(AHEAD):
         copy(k).start()
     branch = jnp.sum(parts_ref[...].astype(F32), axis=0)
     second = (first_ref[...].astype(F32) + branch).astype(BF16)
@@ -204,13 +205,17 @@
     scaled = (stream * gain_ref[...].astype(F32)).astype(BF16)
     pieces = in_three(jnp.sum(stream * stream, axis=1, keepdims=True))
     for k in range(n):
-        copy(k).wait()
         for i in range(4):
             out_ref[k, :, i * PAD + units : (i + 1) * PAD] = jnp.zeros((rows, PAD - units), BF16)
+        for i, piece in enumerate(pieces):
+            out_ref[k, :, units + i : units + i + 1] = piece
+    for k in range(n):
+        copy(k).wait()
+        if k + AHEAD < n:
+            copy(k + AHEAD).start()
+        for i in range(4):
             weight = held[k, i % 2, (i // 2) * units : (i // 2 + 1) * units]
             out_ref[k, :, i * PAD : i * PAD + units] = dot_nt(scaled, weight).astype(BF16)
-        for i, piece in enumerate(pieces):
-            out_ref[k, :, units + i : units + i + 1] = piece
 
 
 def last_kernel(units, hidden_ref, second_ref, weights_ref, out_ref):
@@ -253,12 +258,11 @@
     wide = (n, rows, 4 * PAD)
     narrow = (n, rows, 2 * PAD)
 
-    later = jnp.concatenate([w_gate_post.T, w_up_post.T, w_down_post], axis=0)
-    later = lax.all_gather(later, TP, axis=0, tiled=False)
-
     gate_t, up_t = w_gate_pre.T, w_up_pre.T
     stream = exchanged(jnp.broadcast_to(tokens[None], block), "z")
     other = from_partner(jnp.concatenate([gate_t, up_t, w_down_pre, w_out], axis=0))
+    later = jnp.concatenate([w_gate_post.T, w_up_post.T, w_down_post], axis=0)
+    later = lax.all_gather(later, TP, axis=0, tiled=False)
     (sent,) = local_call(
         gate_up_kernel, [(wide, BF16)], (stream, gain_pre[None], gate_t, up_t, other)
     )

time: 187 us -> 187 us (level)
  no operation moved by 1% of the time
where the time goes in v6:
time: 187 us; the launch traced here: 183 us
  blocking collectives  74.3 us (40%)
  starting transfers between devices  40.8 us (22%)
  waiting for transfers between devices  35.9 us (19%)
  between operations  15.6 us (8%)
  Pallas kernels  13.2 us (7%)
  other arithmetic  2.17 us (1%)
    all_to_all x6, blocking collectives, exchanged(): return lax.all_to_all(parts, axis, 0, 0, tiled=True)  74.3 us
    all_to_all x4, waiting for transfers between devices, exchanged(): return lax.all_to_all(parts, axis, 0, 0, tiled=True)  35.6 us
    all_to_all x4, starting transfers between devices, exchanged(): return lax.all_to_all(parts, axis, 0, 0, tiled=True)  25.7 us
    ppermute x2, starting transfers between devices, from_partner(): return lax.ppermute(x, 'core', [(0, 1), (1, 0)])  15.1 us
    pallas_call x10, Pallas kernels, local_call(): pl.pallas_call(kernel, out_shape=outs, in_specs=specs, out_specs=tuple((p...  13.2 us
  transfers between devices with their start and end apart: 7, of which 5 were waited for; matrix products, arithmetic and copies ran while one was open for 1% of the time, Pallas kernels for 3%

profile of v6, /device:TPU:1, one launch (start us, length us, event | category | flops | bytes accessed | tf_op | source)
XLA Modules:
  0.0 183.5 jit_solution(8664852178625003403)
XLA Ops:
  7.3 2.1 %pad_maximum_fusion.1 = bf16[1056,256]{1,0:T(8,128)(2,1)} fusion(bf16[352,256]{1,0:T(8,128)(2,1)} %param.39, bf16[352,256]{1,0:T(8,128)(2,1)} %bitcast.34, bf16[352,256]{1,0:T(8,128)(2,1)} %bitcast.35), kind=kLoop, calls=%fused_computation.1 | loop fusion | flops 1622016 | bytes 1081344 | tf_op jit(solution)/shard_map/concatenate | solution.py:264
  9.5 8.7 %collective-permute-start = (bf16[1184,256]{1,0:T(8,128)(2,1)S(1)}, bf16[1184,256]{1,0:T(8,128)(2,1)S(1)}, u32[]{:S(2)}, u32[]{:S(2)}) collective-permute-start(bf16[1184,256]{1,0:T(8,128)(2,1)S(1)} %pad_maximum_fusion), channel_id=1, source_target_pairs={{0,1},{1,0},{2,3},{3,2},{4,5},{5,4},{6,7},{7,6},{8,9},{9,8},{10,11... | collective-permute-start | bytes 1818632 | tf_op jit(solution)/shard_map/ppermute | solution.py:38
  18.9 9.6 %all-to-all-start = ((bf16[16,8,256]{2,1,0:T(8,128)(2,1)}), bf16[16,8,256]{2,1,0:T(8,128)(2,1)S(1)}, u32[]{:S(2)}, u32[]{:S(2)}) async-start(bf16[16,8,256]{2,1,0:T(8,128)(2,1)} %broadcast_in_dim.24), calls=%async_computation | async-start | bytes 131072 | tf_op jit(solution)/shard_map/all_to_all | solution.py:34
  28.5 11.6 %all-to-all-done.rows_ref = bf16[16,8,256]{2,1,0:T(8,128)(2,1)S(1)} async-done(((bf16[16,8,256]{2,1,0:T(8,128)(2,1)}), bf16[16,8,256]{2,1,0:T(8,128)(2,1)S(1)}, u32[]{:S(2)}, u32[]{:S(2)}) %all-to-all-start) | async-done | bytes 65568 | tf_op jit(solution)/shard_map/all_to_all | solution.py:34
  40.5 14.8 %all_to_all.50.parts_ref = bf16[16,8,1536]{2,1,0:T(8,128)(2,1)S(1)} all-to-all(bf16[16,8,1536]{2,1,0:T(8,128)(2,1)S(1)} %shard_map.203), channel_id=1, replica_groups=mesh['kv_0'=4,'kv_1'=4,'z'=16,'core'=2] {'kv_0','kv_1'}, dimensions={0} | all-to-all | bytes 786432 | tf_op jit(solution)/shard_map/all_to_all | solution.py:34
  55.5 10.0 %all_to_all.51.hidden_ref = bf16[16,8,768]{2,1,0:T(8,128)(2,1)S(1)} all-to-all(bf16[16,8,768]{2,1,0:T(8,128)(2,1)S(1)} %shard_map.204), channel_id=1, replica_groups=mesh['kv_0'=4,'kv_1'=4,'z'=16,'core'=2] {'kv_0','kv_1'}, dimensions={0} | all-to-all | bytes 393216 | tf_op jit(solution)/shard_map/all_to_all | solution.py:34
  65.8 17.1 %all_to_all.52.parts_ref = bf16[16,8,256]{2,1,0:T(8,128)(2,1)S(1)} all-to-all(bf16[16,8,256]{2,1,0:T(8,128)(2,1)S(1)} %shard_map.205), channel_id=1, replica_groups=mesh['kv_0'=4,'kv_1'=4,'z'=16,'core'=2] {'z'}, dimensions={0} | all-to-all | bytes 131072 | tf_op jit(solution)/shard_map/all_to_all | solution.py:34
  82.9 0.7 shard_map.206
  83.5 3.5 %all-to-all-start.4 = ((bf16[16,8,256]{2,1,0:T(8,128)(2,1)}), bf16[16,8,256]{2,1,0:T(8,128)(2,1)S(1)}, u32[]{:S(2)}, u32[]{:S(2)}) async-start(bf16[16,8,256]{2,1,0:T(8,128)(2,1)} %get-tuple-element.8), calls=%async_computation.4 | async-start | bytes 131072 | tf_op jit(solution)/shard_map/all_to_all | solution.py:34
  87.1 6.3 %collective-permute-start.1 = (bf16[256,384]{1,0:T(8,128)(2,1)S(1)}, bf16[256,384]{1,0:T(8,128)(2,1)S(1)}, u32[]{:S(2)}, u32[]{:S(2)}) collective-permute-start(bf16[256,384]{1,0:T(8,128)(2,1)S(1)} %pad_maximum_fusion.2), channel_id=1, source_target_pairs={{0,1},{1,0},{2,3},{3,2},{4,5},{5,4},{6,7},{7,6},{8,9},{9,8},{10,11... | collective-permute-start | bytes 589832 | tf_op jit(solution)/shard_map/ppermute | solution.py:38
  93.4 0.7 dynamic-slice_bitcast_fusion
  94.5 4.7 %all-to-all-done.4.rows_ref = bf16[16,8,256]{2,1,0:T(8,128)(2,1)S(1)} async-done(((bf16[16,8,256]{2,1,0:T(8,128)(2,1)}), bf16[16,8,256]{2,1,0:T(8,128)(2,1)S(1)}, u32[]{:S(2)}, u32[]{:S(2)}) %all-to-all-start.4) | async-done | bytes 65568 | tf_op jit(solution)/shard_map/all_to_all | solution.py:34
  99.2 1.1 shard_map.207
  100.2 9.1 %all-to-all-start.5 = ((bf16[32,8,512]{2,1,0:T(8,128)(2,1)}), bf16[32,8,512]{2,1,0:T(8,128)(2,1)S(1)}, u32[]{:S(2)}, u32[]{:S(2)}) async-start(bf16[32,8,512]{2,1,0:T(8,128)(2,1)} %bitcast.5), calls=%async_computation.5 | async-start | bytes 524288 | tf_op jit(solution)/shard_map/all_to_all | solution.py:34
  110.7 7.7 %all-to-all-done.5 = bf16[32,8,512]{2,1,0:T(8,128)(2,1)S(1)} async-done(((bf16[32,8,512]{2,1,0:T(8,128)(2,1)}), bf16[32,8,512]{2,1,0:T(8,128)(2,1)S(1)}, u32[]{:S(2)}, u32[]{:S(2)}) %all-to-all-start.5) | async-done | bytes 262176 | tf_op jit(solution)/shard_map/all_to_all | solution.py:34
  118.3 2.0 %shard_map.208 = (f32[16,128,128]{2,1,0:T(8,128)}, bf16[16,16,128]{2,1,0:T(8,128)(2,1)S(1)}) custom-call(bf16[16,16,512]{2,1,0:T(8,128)(2,1)S(1)} %bitcast.26, f32[16,128,128]{2,1,0:T(8,128)S(1)} %bitcast.25, f32[1,1]{1,0:T(1,128)} %bitcast.21.base_ref, f32[1,1]{1,0:T(1,128)} %bitcast.22.shift_ref, bf16[1,128]{1,0:T(2,128)(2,1)S(1)} %bitcast.33), custom_call_target="tpu_custom_call" | custom-call | tf_op jit(solution)/shard_map/pallas_call | solution.py:49
  120.3 10.9 %all_to_all.53 = bf16[32,8,128]{2,1,0:T(8,128)(2,1)S(1)} all-to-all(bf16[32,8,128]{2,1,0:T(8,128)(2,1)S(1)} %bitcast.32), channel_id=1, replica_groups=mesh['kv_0'=4,'kv_1'=4,'z'=16,'core'=2] {'kv_0','kv_1','core'}, dimensions={0} | all-to-all | bytes 131072 | tf_op jit(solution)/shard_map/all_to_all | solution.py:34
  131.2 0.8 shard_map.209
  132.0 3.5 %all-to-all-start.7 = ((bf16[16,8,256]{2,1,0:T(8,128)(2,1)}), bf16[16,8,256]{2,1,0:T(8,128)(2,1)S(1)}, u32[]{:S(2)}, u32[]{:S(2)}) async-start(bf16[16,8,256]{2,1,0:T(8,128)(2,1)} %shard_map.209), calls=%async_computation.7 | async-start | bytes 131072 | tf_op jit(solution)/shard_map/all_to_all | solution.py:34
  135.5 11.6 %all-to-all-done.7.parts_ref = bf16[16,8,256]{2,1,0:T(8,128)(2,1)S(1)} async-done(((bf16[16,8,256]{2,1,0:T(8,128)(2,1)}), bf16[16,8,256]{2,1,0:T(8,128)(2,1)S(1)}, u32[]{:S(2)}, u32[]{:S(2)}) %all-to-all-start.7) | async-done | bytes 65568 | tf_op jit(solution)/shard_map/all_to_all | solution.py:34
  147.2 6.3 %shard_map.210 = (bf16[16,8,1536]{2,1,0:T(8,128)(2,1)S(1)}, bf16[8,256]{1,0:T(8,128)(2,1)S(1)}) custom-call(bf16[16,8,256]{2,1,0:T(8,128)(2,1)S(1)} %all-to-all-done.7.parts_ref, bf16[8,256]{1,0:T(8,128)(2,1)S(1)} %get-tuple-element.10.first_ref, bf16[1,256]{1,0:T(2,128)(2,1)S(1)} %broadcast_in_dim.30.gain_ref, bf16[32,1056,256]{2,1,0:T(8,128)(2,1)} %bitcast.23), custom_call_target="tpu_custom_call" | custom-call | tf_op jit(solution)/shard_map/pallas_call | solution.py:49
  153.5 11.7 %all_to_all.54.parts_ref = bf16[16,8,1536]{2,1,0:T(8,128)(2,1)S(1)} all-to-all(bf16[16,8,1536]{2,1,0:T(8,128)(2,1)S(1)} %get-tuple-element.11), channel_id=1, replica_groups=mesh['kv_0'=4,'kv_1'=4,'z'=16,'core'=2] {'kv_0','kv_1'}, dimensions={0} | all-to-all | bytes 786432 | tf_op jit(solution)/shard_map/all_to_all | solution.py:34
  165.4 9.8 %all_to_all.55.hidden_ref = bf16[16,8,768]{2,1,0:T(8,128)(2,1)S(1)} all-to-all(bf16[16,8,768]{2,1,0:T(8,128)(2,1)S(1)} %shard_map.211), channel_id=1, replica_groups=mesh['kv_0'=4,'kv_1'=4,'z'=16,'core'=2] {'kv_0','kv_1'}, dimensions={0} | all-to-all | bytes 393216 | tf_op jit(solution)/shard_map/all_to_all | solution.py:34
  175.1 1.5 shard_map.212
  (44 shorter events, 2.1 us)
Async XLA Ops:
  7.2 2.2 %copy-start.2 = (bf16[256,352]{0,1:T(8,128)(2,1)S(1)}, bf16[256,352]{0,1:T(8,128)(2,1)}, u32[]{:S(2)}) copy-start(bf16[256,352]{0,1:T(8,128)(2,1)} %param.23) | copy-start | bytes 540676
  7.2 2.2 %copy-start.3 = (bf16[256,352]{0,1:T(8,128)(2,1)S(1)}, bf16[256,352]{0,1:T(8,128)(2,1)}, u32[]{:S(2)}) copy-start(bf16[256,352]{0,1:T(8,128)(2,1)} %param.24) | copy-start | bytes 540676
  7.2 2.2 %copy-start.4 = (bf16[352,256]{1,0:T(8,128)(2,1)S(1)}, bf16[352,256]{1,0:T(8,128)(2,1)}, u32[]{:S(2)}) copy-start(bf16[352,256]{1,0:T(8,128)(2,1)} %own_ref.3) | copy-start | bytes 540676
  7.2 2.2 %copy-start.8 = (bf16[128,256]{1,0:T(8,128)(2,1)S(1)}, bf16[128,256]{1,0:T(8,128)(2,1)}, u32[]{:S(2)}) copy-start(bf16[128,256]{1,0:T(8,128)(2,1)} %own_ref.5) | copy-start | bytes 196612
  7.2 140.0 %all-gather.3.cloned.1.call-start = ((), (), s32[]{:S(2)}) async-start(), calls=%async_computation.10 | async-start | bytes 17842176 | tf_op jit(solution)/shard_map/all_gather | solution.py:265
  7.3 11.0 %copy-start.9 = (bf16[8,256]{1,0:T(8,128)(2,1)S(1)}, bf16[8,256]{1,0:T(8,128)(2,1)}, u32[]{:S(2)}) copy-start(bf16[8,256]{1,0:T(8,128)(2,1)} %own_ref.4) | copy-start | bytes 12292
  9.3 19.1 %copy-start.11 = (bf16[256]{0:T(256)(128)(2,1)S(1)}, bf16[256]{0:T(256)(128)(2,1)}, u32[]{:S(2)}) copy-start(bf16[256]{0:T(256)(128)(2,1)} %param.22) | copy-start | bytes 1540
  9.5 30.6 %collective-permute-start = (bf16[1184,256]{1,0:T(8,128)(2,1)S(1)}, bf16[1184,256]{1,0:T(8,128)(2,1)S(1)}, u32[]{:S(2)}, u32[]{:S(2)}) collective-permute-start(bf16[1184,256]{1,0:T(8,128)(2,1)S(1)} %pad_maximum_fusion), channel_id=1, source_target_pairs={{0,1},{1,0},{2,3},{3,2},{4,5},{5,4},{6,7},{7,6},{8,9},{9,8},{10,11... | collective-permute-start | bytes 1818632 | tf_op jit(solution)/shard_map/ppermute | solution.py:38
  18.9 21.2 %all-to-all-start = ((bf16[16,8,256]{2,1,0:T(8,128)(2,1)}), bf16[16,8,256]{2,1,0:T(8,128)(2,1)S(1)}, u32[]{:S(2)}, u32[]{:S(2)}) async-start(bf16[16,8,256]{2,1,0:T(8,128)(2,1)} %broadcast_in_dim.24), calls=%async_computation | async-start | bytes 131072 | tf_op jit(solution)/shard_map/all_to_all | solution.py:34
  55.3 31.8 %copy-start.5 = (bf16[256,128]{1,0:T(8,128)(2,1)S(1)}, bf16[256,128]{1,0:T(8,128)(2,1)}, u32[]{:S(2)}) copy-start(bf16[256,128]{1,0:T(8,128)(2,1)} %q_ref.1) | copy-start | bytes 196612
  55.3 31.8 %copy-start.6 = (bf16[256,128]{1,0:T(8,128)(2,1)S(1)}, bf16[256,128]{1,0:T(8,128)(2,1)}, u32[]{:S(2)}) copy-start(bf16[256,128]{1,0:T(8,128)(2,1)} %k_ref.1) | copy-start | bytes 196612
  55.3 31.8 %copy-start.7 = (bf16[256,128]{1,0:T(8,128)(2,1)S(1)}, bf16[256,128]{1,0:T(8,128)(2,1)}, u32[]{:S(2)}) copy-start(bf16[256,128]{1,0:T(8,128)(2,1)} %v_ref.1) | copy-start | bytes 196612
  55.5 38.0 %copy-start.12 = (bf16[256]{0:T(256)(128)(2,1)S(1)}, bf16[256]{0:T(256)(128)(2,1)}, u32[]{:S(2)}) copy-start(bf16[256]{0:T(256)(128)(2,1)} %param.26) | copy-start | bytes 1540
  65.7 52.6 %copy-start.1 = (f32[16,1,128,128]{3,2,1,0:T(8,128)S(1)}, f32[16,1,128,128]{3,2,1,0:T(8,128)}, u32[]{:S(2)}) copy-start(f32[16,1,128,128]{3,2,1,0:T(8,128)} %param.21) | copy-start | bytes 3145732
  65.7 52.6 %copy-start.10 = (bf16[128]{0:T(256)(128)(2,1)S(1)}, bf16[128]{0:T(256)(128)(2,1)}, u32[]{:S(2)}) copy-start(bf16[128]{0:T(256)(128)(2,1)} %param.34) | copy-start | bytes 772
  83.5 15.6 %all-to-all-start.4 = ((bf16[16,8,256]{2,1,0:T(8,128)(2,1)}), bf16[16,8,256]{2,1,0:T(8,128)(2,1)S(1)}, u32[]{:S(2)}, u32[]{:S(2)}) async-start(bf16[16,8,256]{2,1,0:T(8,128)(2,1)} %get-tuple-element.8), calls=%async_computation.4 | async-start | bytes 131072 | tf_op jit(solution)/shard_map/all_to_all | solution.py:34
  87.1 7.4 %collective-permute-start.1 = (bf16[256,384]{1,0:T(8,128)(2,1)S(1)}, bf16[256,384]{1,0:T(8,128)(2,1)S(1)}, u32[]{:S(2)}, u32[]{:S(2)}) collective-permute-start(bf16[256,384]{1,0:T(8,128)(2,1)S(1)} %pad_maximum_fusion.2), channel_id=1, source_target_pairs={{0,1},{1,0},{2,3},{3,2},{4,5},{5,4},{6,7},{7,6},{8,9},{9,8},{10,11... | collective-permute-start | bytes 589832 | tf_op jit(solution)/shard_map/ppermute | solution.py:38
  100.2 18.1 %all-to-all-start.5 = ((bf16[32,8,512]{2,1,0:T(8,128)(2,1)}), bf16[32,8,512]{2,1,0:T(8,128)(2,1)S(1)}, u32[]{:S(2)}, u32[]{:S(2)}) async-start(bf16[32,8,512]{2,1,0:T(8,128)(2,1)} %bitcast.5), calls=%async_computation.5 | async-start | bytes 524288 | tf_op jit(solution)/shard_map/all_to_all | solution.py:34
  109.3 26.2 %copy-start.13 = (bf16[256]{0:T(256)(128)(2,1)S(1)}, bf16[256]{0:T(256)(128)(2,1)}, u32[]{:S(2)}) copy-start(bf16[256]{0:T(256)(128)(2,1)} %param.36) | copy-start | bytes 1540
  132.0 15.2 %all-to-all-start.7 = ((bf16[16,8,256]{2,1,0:T(8,128)(2,1)}), bf16[16,8,256]{2,1,0:T(8,128)(2,1)S(1)}, u32[]{:S(2)}, u32[]{:S(2)}) async-start(bf16[16,8,256]{2,1,0:T(8,128)(2,1)} %shard_map.209), calls=%async_computation.7 | async-start | bytes 131072 | tf_op jit(solution)/shard_map/all_to_all | solution.py:34
  147.2 28.0 %copy-start = (bf16[33792,256]{1,0:T(8,128)(2,1)S(1)}, bf16[33792,256]{1,0:T(8,128)(2,1)}, u32[]{:S(2)}) copy-start(bf16[33792,256]{1,0:T(8,128)(2,1)} %all-gather.3.cloned.1.call-done) | copy-start | bytes 51904516
Sparse Core Ops, SparseCore 0:
  10.1 121.3 all-gather.2

commit v7 on v6

--- a/solution.py
+++ b/solution.py
@@ -38,7 +38,7 @@
     return lax.ppermute(x, "core", [(0, 1), (1, 0)])
 
 
-def local_call(kernel, shapes, args, *, scalars=0, far=(), scratch=(), limit=6 << 20):
+def local_call(kernel, shapes, args, *, scalars=0, far=(), scratch=(), limit=6 << 20, cost=None):
     specs = [
         pl.BlockSpec(
             memory_space=pltpu.SMEM if i < scalars else pl.ANY if i in far else pltpu.VMEM
@@ -53,6 +53,7 @@
         out_specs=tuple(pl.BlockSpec(memory_space=pltpu.VMEM) for _ in outs),
         scratch_shapes=list(scratch),
         compiler_params=pltpu.CompilerParams(vmem_limit_bytes=limit),
+        cost_estimate=cost,
     )(*args)
 
 
@@ -89,7 +90,8 @@
         )
 
 
-def hidden_kernel(units, parts_ref, out_ref):
+def hidden_kernel(units, parts_ref, *refs):
+    out_ref = refs[-1]
     total = jnp.sum(parts_ref[...].astype(F32), axis=0)
     squares = jnp.sum(total[:, units : units + 3], axis=1, keepdims=True)
     factor = scale_of(squares)
@@ -138,8 +140,18 @@
             out_ref[:, to, :, at : at + 1] = column.reshape(n, rows, 1).astype(BF16)
 
 
-def state_kernel(
-    parts_ref, state_ref, base_ref, shift_ref, head_gain_ref, state_out_ref, out_ref, held
+def read_kernel(
+    parts_ref,
+    state_ref,
+    base_ref,
+    shift_ref,
+    head_gain_ref,
+    keys_ref,
+    rate_ref,
+    correction_ref,
+    out_ref,
+    recalled,
+    queried,
 ):
     dim = state_ref.shape[2]
     got = jnp.sum(parts_ref[...].astype(F32), axis=0)
@@ -159,18 +171,24 @@
     queries_t, keys_t = queries.T, keys.T
     for b in range(state_ref.shape[0]):
         old = state_ref[b]
-        key, query = keys_t[:, b : b + 1], queries_t[:, b : b + 1]
-        rate_b = rate[b : b + 1]
-        recalled = jnp.sum(key * old, axis=0, keepdims=True)
-        correction = beta[b : b + 1] * (values[b : b + 1] - rate_b * recalled)
-        new = rate_b * old + key * correction
-        state_out_ref[b] = new
-        held[b : b + 1] = jnp.sum(query * new, axis=0, keepdims=True)
-    read = held[...]
+        recalled[b : b + 1] = jnp.sum(keys_t[:, b : b + 1] * old, axis=0, keepdims=True)
+        queried[b : b + 1] = jnp.sum(queries_t[:, b : b + 1] * old, axis=0, keepdims=True)
+    correction = beta * (values - rate * recalled[...])
+    read = rate * queried[...] + jnp.sum(keys * queries, axis=1, keepdims=True) * correction
     normed = read * lax.rsqrt(jnp.mean(read * read, axis=1, keepdims=True) + EPS)
     normed = (normed * head_gain_ref[...].astype(F32)).astype(BF16)
     for i in range(out_ref.shape[0]):
         out_ref[i] = normed
+    keys_ref[...] = keys_t
+    rate_ref[...] = rate
+    correction_ref[...] = correction
+
+
+def state_kernel(state_ref, keys_ref, rate_ref, correction_ref, out_ref):
+    keys_t, rate, correction = keys_ref[...], rate_ref[...], correction_ref[...]
+    for b in range(state_ref.shape[0]):
+        new = rate[b : b + 1] * state_ref[b] + keys_t[:, b : b + 1] * correction[b : b + 1]
+        out_ref[b] = new
 
 
 def out_kernel(core_ref, heads_ref, own_ref, other_ref, out_ref):
@@ -258,11 +276,12 @@
     wide = (n, rows, 4 * PAD)
     narrow = (n, rows, 2 * PAD)
 
+    later = jnp.concatenate([w_gate_post.T, w_up_post.T, w_down_post], axis=0)
+    later = lax.all_gather(later, TP, axis=0, tiled=False)
+
     gate_t, up_t = w_gate_pre.T, w_up_pre.T
     stream = exchanged(jnp.broadcast_to(tokens[None], block), "z")
     other = from_partner(jnp.concatenate([gate_t, up_t, w_down_pre, w_out], axis=0))
-    later = jnp.concatenate([w_gate_post.T, w_up_post.T, w_down_post], axis=0)
-    later = lax.all_gather(later, TP, axis=0, tiled=False)
     (sent,) = local_call(
         gate_up_kernel, [(wide, BF16)], (stream, gain_pre[None], gate_t, up_t, other)
     )
@@ -301,19 +320,21 @@
         scalars=1,
     )
     got = exchanged(sent.reshape(2 * n, rows, 4 * dim), KVC).reshape(n, 2 * rows, 4 * dim)
-    new_state, sent = local_call(
+    held = state.reshape(seqs, dim, dim)
+    keys_t, rate, correction, sent = local_call(
+        read_kernel,
+        [((dim, seqs), F32), ((seqs, 1), F32), ((seqs, dim), F32), ((n, seqs, dim), BF16)],
+        (got, held, decay_base[None], decay_shift[None], head_gain[None]),
+        scratch=(pltpu.VMEM((seqs, dim), F32), pltpu.VMEM((seqs, dim), F32)),
+    )
+    (new_state,) = local_call(
         state_kernel,
-        [((seqs, dim, dim), F32), ((n, seqs, dim), BF16)],
-        (
-            got,
-            state.reshape(seqs, dim, dim),
-            decay_base[None],
-            decay_shift[None],
-            head_gain[None],
-        ),
-        scratch=(pltpu.VMEM((seqs, dim), F32),),
+        [((seqs, dim, dim), F32)],
+        (held, keys_t, rate, correction),
+        cost=pl.CostEstimate(flops=1 << 28, bytes_accessed=8 * held.size, transcendentals=0),
     )
     heads = exchanged(sent.reshape(2 * n, rows, dim), KVC).reshape(n, 2 * rows, dim)
+    heads, new_state = lax.optimization_barrier((heads, new_state))
     (sent,) = local_call(
         out_kernel, [(block, BF16)], (core, heads, w_out, other), scalars=1
     )
@@ -327,7 +348,11 @@
         limit=46 << 20,
     )
     (hidden,) = local_call(
-        functools.partial(hidden_kernel, units), [(narrow, BF16)], (exchanged(sent, KV),)
+        functools.partial(hidden_kernel, units),
+        [(narrow, BF16)],
+        (exchanged(sent, KV), *(later,) * 4),
+        far=range(1, 5),
+        limit=40 << 20,
     )
     (result,) = local_call(
         functools.partial(last_kernel, units),

time: 187 us -> 187 us (level)
  blocking collectives: 74.3 us -> 63.9 us
  waiting for transfers between devices: 35.9 us -> 41.9 us
  starting transfers between devices: 40.8 us -> 44.5 us
    all_to_all x6 -> x5, blocking collectives: 74.3 us -> 63.9 us  [exchanged(): return lax.all_to_all(parts, axis, 0, 0, tiled=True)]
    all_to_all x4 -> x5, waiting for transfers between devices: 35.6 us -> 41.6 us  [exchanged(): return lax.all_to_all(parts, axis, 0, 0, tiled=True)]
    all_to_all x4 -> x5, starting transfers between devices: 25.7 us -> 29.4 us  [exchanged(): return lax.all_to_all(parts, axis, 0, 0, tiled=True)]
    pallas_call x10 -> x11, Pallas kernels: 13.2 us -> 14.2 us  [local_call(): pl.pallas_call(kernel, out_shape=outs, in_specs=specs, out_specs=tuple((p...]
  transfers between devices with their start and end apart: 7 -> 8, of which waited for: 5 -> 6; matrix products, arithmetic and copies ran while one was open for 1% -> 1% of each run, Pallas kernels for 3% -> 3%
where the time goes in v7:
time: 187 us; the launch traced here: 184 us
  blocking collectives  63.9 us (34%)
  starting transfers between devices  44.5 us (24%)
  waiting for transfers between devices  41.9 us (22%)
  between operations  15.7 us (8%)
  Pallas kernels  14.2 us (8%)
  other arithmetic  2.18 us (1%)
    all_to_all x5, blocking collectives, exchanged(): return lax.all_to_all(parts, axis, 0, 0, tiled=True)  63.9 us
    all_to_all x5, waiting for transfers between devices, exchanged(): return lax.all_to_all(parts, axis, 0, 0, tiled=True)  41.6 us
    all_to_all x5, starting transfers between devices, exchanged(): return lax.all_to_all(parts, axis, 0, 0, tiled=True)  29.4 us
    ppermute x2, starting transfers between devices, from_partner(): return lax.ppermute(x, 'core', [(0, 1), (1, 0)])  15 us
    pallas_call x11, Pallas kernels, local_call(): pl.pallas_call(kernel, out_shape=outs, in_specs=specs, out_specs=tuple((p...  14.2 us
  transfers between devices with their start and end apart: 8, of which 6 were waited for; matrix products, arithmetic and copies ran while one was open for 1% of the time, Pallas kernels for 3%

profile of v7, /device:TPU:1, one launch (start us, length us, event | category | flops | bytes accessed | tf_op | source)
XLA Modules:
  0.0 183.9 jit_solution(6100383561437060297)
XLA Ops:
  7.3 2.1 %pad_maximum_fusion.1 = bf16[1056,256]{1,0:T(8,128)(2,1)} fusion(bf16[352,256]{1,0:T(8,128)(2,1)} %param.39, bf16[352,256]{1,0:T(8,128)(2,1)} %bitcast.41, bf16[352,256]{1,0:T(8,128)(2,1)} %bitcast.42), kind=kLoop, calls=%fused_computation.1 | loop fusion | flops 1622016 | bytes 1081344 | tf_op jit(solution)/shard_map/concatenate | solution.py:279
  9.5 8.7 %collective-permute-start = (bf16[1184,256]{1,0:T(8,128)(2,1)S(1)}, bf16[1184,256]{1,0:T(8,128)(2,1)S(1)}, u32[]{:S(2)}, u32[]{:S(2)}) collective-permute-start(bf16[1184,256]{1,0:T(8,128)(2,1)S(1)} %pad_maximum_fusion), channel_id=1, source_target_pairs={{0,1},{1,0},{2,3},{3,2},{4,5},{5,4},{6,7},{7,6},{8,9},{9,8},{10,11... | collective-permute-start | bytes 1818632 | tf_op jit(solution)/shard_map/ppermute | solution.py:38
  18.9 9.6 %all-to-all-start = ((bf16[16,8,256]{2,1,0:T(8,128)(2,1)}), bf16[16,8,256]{2,1,0:T(8,128)(2,1)S(1)}, u32[]{:S(2)}, u32[]{:S(2)}) async-start(bf16[16,8,256]{2,1,0:T(8,128)(2,1)} %broadcast_in_dim.24), calls=%async_computation | async-start | bytes 131072 | tf_op jit(solution)/shard_map/all_to_all | solution.py:34
  28.5 11.6 %all-to-all-done.rows_ref = bf16[16,8,256]{2,1,0:T(8,128)(2,1)S(1)} async-done(((bf16[16,8,256]{2,1,0:T(8,128)(2,1)}), bf16[16,8,256]{2,1,0:T(8,128)(2,1)S(1)}, u32[]{:S(2)}, u32[]{:S(2)}) %all-to-all-start) | async-done | bytes 65568 | tf_op jit(solution)/shard_map/all_to_all | solution.py:34
  40.5 14.8 %all_to_all.50.parts_ref = bf16[16,8,1536]{2,1,0:T(8,128)(2,1)S(1)} all-to-all(bf16[16,8,1536]{2,1,0:T(8,128)(2,1)S(1)} %shard_map.203), channel_id=1, replica_groups=mesh['kv_0'=4,'kv_1'=4,'z'=16,'core'=2] {'kv_0','kv_1'}, dimensions={0} | all-to-all | bytes 786432 | tf_op jit(solution)/shard_map/all_to_all | solution.py:34
  55.5 10.0 %all_to_all.51.hidden_ref = bf16[16,8,768]{2,1,0:T(8,128)(2,1)S(1)} all-to-all(bf16[16,8,768]{2,1,0:T(8,128)(2,1)S(1)} %shard_map.204), channel_id=1, replica_groups=mesh['kv_0'=4,'kv_1'=4,'z'=16,'core'=2] {'kv_0','kv_1'}, dimensions={0} | all-to-all | bytes 393216 | tf_op jit(solution)/shard_map/all_to_all | solution.py:34
  65.8 17.1 %all_to_all.52.parts_ref = bf16[16,8,256]{2,1,0:T(8,128)(2,1)S(1)} all-to-all(bf16[16,8,256]{2,1,0:T(8,128)(2,1)S(1)} %shard_map.205), channel_id=1, replica_groups=mesh['kv_0'=4,'kv_1'=4,'z'=16,'core'=2] {'z'}, dimensions={0} | all-to-all | bytes 131072 | tf_op jit(solution)/shard_map/all_to_all | solution.py:34
  83.5 3.5 %all-to-all-start.4 = ((bf16[16,8,256]{2,1,0:T(8,128)(2,1)}), bf16[16,8,256]{2,1,0:T(8,128)(2,1)S(1)}, u32[]{:S(2)}, u32[]{:S(2)}) async-start(bf16[16,8,256]{2,1,0:T(8,128)(2,1)} %get-tuple-element.12), calls=%async_computation.4 | async-start | bytes 131072 | tf_op jit(solution)/shard_map/all_to_all | solution.py:34
  87.1 6.3 %collective-permute-start.1 = (bf16[256,384]{1,0:T(8,128)(2,1)S(1)}, bf16[256,384]{1,0:T(8,128)(2,1)S(1)}, u32[]{:S(2)}, u32[]{:S(2)}) collective-permute-start(bf16[256,384]{1,0:T(8,128)(2,1)S(1)} %pad_maximum_fusion.2), channel_id=1, source_target_pairs={{0,1},{1,0},{2,3},{3,2},{4,5},{5,4},{6,7},{7,6},{8,9},{9,8},{10,11... | collective-permute-start | bytes 589832 | tf_op jit(solution)/shard_map/ppermute | solution.py:38
  94.5 4.7 %all-to-all-done.4.rows_ref = bf16[16,8,256]{2,1,0:T(8,128)(2,1)S(1)} async-done(((bf16[16,8,256]{2,1,0:T(8,128)(2,1)}), bf16[16,8,256]{2,1,0:T(8,128)(2,1)S(1)}, u32[]{:S(2)}, u32[]{:S(2)}) %all-to-all-start.4) | async-done | bytes 65568 | tf_op jit(solution)/shard_map/all_to_all | solution.py:34
  99.2 1.1 shard_map.207
  100.3 9.1 %all-to-all-start.5 = ((bf16[32,8,512]{2,1,0:T(8,128)(2,1)}), bf16[32,8,512]{2,1,0:T(8,128)(2,1)S(1)}, u32[]{:S(2)}, u32[]{:S(2)}) async-start(bf16[32,8,512]{2,1,0:T(8,128)(2,1)} %bitcast.5), calls=%async_computation.5 | async-start | bytes 524288 | tf_op jit(solution)/shard_map/all_to_all | solution.py:34
  110.6 7.7 %all-to-all-done.5 = bf16[32,8,512]{2,1,0:T(8,128)(2,1)S(1)} async-done(((bf16[32,8,512]{2,1,0:T(8,128)(2,1)}), bf16[32,8,512]{2,1,0:T(8,128)(2,1)S(1)}, u32[]{:S(2)}, u32[]{:S(2)}) %all-to-all-start.5) | async-done | bytes 262176 | tf_op jit(solution)/shard_map/all_to_all | solution.py:34
  118.3 1.8 shard_map.208
  120.1 3.8 %all-to-all-start.6 = ((bf16[32,8,128]{2,1,0:T(8,128)(2,1)}), bf16[32,8,128]{2,1,0:T(8,128)(2,1)S(1)}, u32[]{:S(2)}, u32[]{:S(2)}) async-start(bf16[32,8,128]{2,1,0:T(8,128)(2,1)} %bitcast.11), calls=%async_computation.6 | async-start | bytes 131072 | tf_op jit(solution)/shard_map/all_to_all | solution.py:34
  123.9 1.4 shard_map.209
  125.3 5.9 %all-to-all-done.6 = bf16[32,8,128]{2,1,0:T(8,128)(2,1)S(1)} async-done(((bf16[32,8,128]{2,1,0:T(8,128)(2,1)}), bf16[32,8,128]{2,1,0:T(8,128)(2,1)S(1)}, u32[]{:S(2)}, u32[]{:S(2)}) %all-to-all-start.6) | async-done | bytes 65568 | tf_op jit(solution)/shard_map/all_to_all | solution.py:34
  131.2 0.8 shard_map.210
  132.0 3.5 %all-to-all-start.7 = ((bf16[16,8,256]{2,1,0:T(8,128)(2,1)}), bf16[16,8,256]{2,1,0:T(8,128)(2,1)S(1)}, u32[]{:S(2)}, u32[]{:S(2)}) async-start(bf16[16,8,256]{2,1,0:T(8,128)(2,1)} %shard_map.210), calls=%async_computation.7 | async-start | bytes 131072 | tf_op jit(solution)/shard_map/all_to_all | solution.py:34
  135.5 11.6 %all-to-all-done.7.parts_ref = bf16[16,8,256]{2,1,0:T(8,128)(2,1)S(1)} async-done(((bf16[16,8,256]{2,1,0:T(8,128)(2,1)}), bf16[16,8,256]{2,1,0:T(8,128)(2,1)S(1)}, u32[]{:S(2)}, u32[]{:S(2)}) %all-to-all-start.7) | async-done | bytes 65568 | tf_op jit(solution)/shard_map/all_to_all | solution.py:34
  147.2 6.1 %shard_map.211 = (bf16[16,8,1536]{2,1,0:T(8,128)(2,1)S(1)}, bf16[8,256]{1,0:T(8,128)(2,1)S(1)}) custom-call(bf16[16,8,256]{2,1,0:T(8,128)(2,1)S(1)} %all-to-all-done.7.parts_ref, bf16[8,256]{1,0:T(8,128)(2,1)S(1)} %get-tuple-element.18.first_ref, bf16[1,256]{1,0:T(2,128)(2,1)S(1)} %broadcast_in_dim.30.gain_ref, bf16[32,1056,256]{2,1,0:T(8,128)(2,1)} %bitcast.23), custom_call_target="tpu_custom_call" | custom-call | tf_op jit(solution)/shard_map/pallas_call | solution.py:49
  153.3 11.7 %all_to_all.53.parts_ref = bf16[16,8,1536]{2,1,0:T(8,128)(2,1)S(1)} all-to-all(bf16[16,8,1536]{2,1,0:T(8,128)(2,1)S(1)} %get-tuple-element.19), channel_id=1, replica_groups=mesh['kv_0'=4,'kv_1'=4,'z'=16,'core'=2] {'kv_0','kv_1'}, dimensions={0} | all-to-all | bytes 786432 | tf_op jit(solution)/shard_map/all_to_all | solution.py:34
  165.2 10.3 %all_to_all.54.hidden_ref = bf16[16,8,768]{2,1,0:T(8,128)(2,1)S(1)} all-to-all(bf16[16,8,768]{2,1,0:T(8,128)(2,1)S(1)} %shard_map.212), channel_id=1, replica_groups=mesh['kv_0'=4,'kv_1'=4,'z'=16,'core'=2] {'kv_0','kv_1'}, dimensions={0} | all-to-all | bytes 393216 | tf_op jit(solution)/shard_map/all_to_all | solution.py:34
  175.6 1.5 shard_map.213
  (55 shorter events, 3.5 us)
Async XLA Ops:
  7.2 2.2 %copy-start.7 = (bf16[128,256]{1,0:T(8,128)(2,1)S(1)}, bf16[128,256]{1,0:T(8,128)(2,1)}, u32[]{:S(2)}) copy-start(bf16[128,256]{1,0:T(8,128)(2,1)} %own_ref.5) | copy-start | bytes 196612
  7.2 2.2 %copy-start.3 = (bf16[352,256]{1,0:T(8,128)(2,1)S(1)}, bf16[352,256]{1,0:T(8,128)(2,1)}, u32[]{:S(2)}) copy-start(bf16[352,256]{1,0:T(8,128)(2,1)} %own_ref.3) | copy-start | bytes 540676
  7.2 140.0 %all-gather.3.cloned.1.call-start = ((), (), s32[]{:S(2)}) async-start(), calls=%async_computation.10 | async-start | bytes 17842176 | tf_op jit(solution)/shard_map/all_gather | solution.py:280
  7.3 11.0 %copy-start.8 = (bf16[8,256]{1,0:T(8,128)(2,1)S(1)}, bf16[8,256]{1,0:T(8,128)(2,1)}, u32[]{:S(2)}) copy-start(bf16[8,256]{1,0:T(8,128)(2,1)} %own_ref.4) | copy-start | bytes 12292
  9.4 19.1 %copy-start.10 = (bf16[256]{0:T(256)(128)(2,1)S(1)}, bf16[256]{0:T(256)(128)(2,1)}, u32[]{:S(2)}) copy-start(bf16[256]{0:T(256)(128)(2,1)} %param.22) | copy-start | bytes 1540
  9.5 30.6 %collective-permute-start = (bf16[1184,256]{1,0:T(8,128)(2,1)S(1)}, bf16[1184,256]{1,0:T(8,128)(2,1)S(1)}, u32[]{:S(2)}, u32[]{:S(2)}) collective-permute-start(bf16[1184,256]{1,0:T(8,128)(2,1)S(1)} %pad_maximum_fusion), channel_id=1, source_target_pairs={{0,1},{1,0},{2,3},{3,2},{4,5},{5,4},{6,7},{7,6},{8,9},{9,8},{10,11... | collective-permute-start | bytes 1818632 | tf_op jit(solution)/shard_map/ppermute | solution.py:38
  18.9 21.2 %all-to-all-start = ((bf16[16,8,256]{2,1,0:T(8,128)(2,1)}), bf16[16,8,256]{2,1,0:T(8,128)(2,1)S(1)}, u32[]{:S(2)}, u32[]{:S(2)}) async-start(bf16[16,8,256]{2,1,0:T(8,128)(2,1)} %broadcast_in_dim.24), calls=%async_computation | async-start | bytes 131072 | tf_op jit(solution)/shard_map/all_to_all | solution.py:34
  55.3 31.8 %copy-start.4 = (bf16[256,128]{1,0:T(8,128)(2,1)S(1)}, bf16[256,128]{1,0:T(8,128)(2,1)}, u32[]{:S(2)}) copy-start(bf16[256,128]{1,0:T(8,128)(2,1)} %q_ref.1) | copy-start | bytes 196612
  55.3 31.8 %copy-start.5 = (bf16[256,128]{1,0:T(8,128)(2,1)S(1)}, bf16[256,128]{1,0:T(8,128)(2,1)}, u32[]{:S(2)}) copy-start(bf16[256,128]{1,0:T(8,128)(2,1)} %k_ref.1) | copy-start | bytes 196612
  55.3 31.8 %copy-start.6 = (bf16[256,128]{1,0:T(8,128)(2,1)S(1)}, bf16[256,128]{1,0:T(8,128)(2,1)}, u32[]{:S(2)}) copy-start(bf16[256,128]{1,0:T(8,128)(2,1)} %v_ref.1) | copy-start | bytes 196612
  55.5 38.0 %copy-start.11 = (bf16[256]{0:T(256)(128)(2,1)S(1)}, bf16[256]{0:T(256)(128)(2,1)}, u32[]{:S(2)}) copy-start(bf16[256]{0:T(256)(128)(2,1)} %param.26) | copy-start | bytes 1540
  65.7 52.6 %copy-start = (f32[16,1,128,128]{3,2,1,0:T(8,128)S(1)}, f32[16,1,128,128]{3,2,1,0:T(8,128)}, u32[]{:S(2)}) copy-start(f32[16,1,128,128]{3,2,1,0:T(8,128)} %param.21) | copy-start | bytes 3145732
  65.8 52.6 %copy-start.9 = (bf16[128]{0:T(256)(128)(2,1)S(1)}, bf16[128]{0:T(256)(128)(2,1)}, u32[]{:S(2)}) copy-start(bf16[128]{0:T(256)(128)(2,1)} %param.34) | copy-start | bytes 772
  83.5 15.7 %all-to-all-start.4 = ((bf16[16,8,256]{2,1,0:T(8,128)(2,1)}), bf16[16,8,256]{2,1,0:T(8,128)(2,1)S(1)}, u32[]{:S(2)}, u32[]{:S(2)}) async-start(bf16[16,8,256]{2,1,0:T(8,128)(2,1)} %get-tuple-element.12), calls=%async_computation.4 | async-start | bytes 131072 | tf_op jit(solution)/shard_map/all_to_all | solution.py:34
  87.1 7.4 %collective-permute-start.1 = (bf16[256,384]{1,0:T(8,128)(2,1)S(1)}, bf16[256,384]{1,0:T(8,128)(2,1)S(1)}, u32[]{:S(2)}, u32[]{:S(2)}) collective-permute-start(bf16[256,384]{1,0:T(8,128)(2,1)S(1)} %pad_maximum_fusion.2), channel_id=1, source_target_pairs={{0,1},{1,0},{2,3},{3,2},{4,5},{5,4},{6,7},{7,6},{8,9},{9,8},{10,11... | collective-permute-start | bytes 589832 | tf_op jit(solution)/shard_map/ppermute | solution.py:38
  100.3 18.1 %all-to-all-start.5 = ((bf16[32,8,512]{2,1,0:T(8,128)(2,1)}), bf16[32,8,512]{2,1,0:T(8,128)(2,1)S(1)}, u32[]{:S(2)}, u32[]{:S(2)}) async-start(bf16[32,8,512]{2,1,0:T(8,128)(2,1)} %bitcast.5), calls=%async_computation.5 | async-start | bytes 524288 | tf_op jit(solution)/shard_map/all_to_all | solution.py:34
  120.1 11.1 %all-to-all-start.6 = ((bf16[32,8,128]{2,1,0:T(8,128)(2,1)}), bf16[32,8,128]{2,1,0:T(8,128)(2,1)S(1)}, u32[]{:S(2)}, u32[]{:S(2)}) async-start(bf16[32,8,128]{2,1,0:T(8,128)(2,1)} %bitcast.11), calls=%async_computation.6 | async-start | bytes 131072 | tf_op jit(solution)/shard_map/all_to_all | solution.py:34
  123.9 11.6 %copy-start.12 = (bf16[256]{0:T(256)(128)(2,1)S(1)}, bf16[256]{0:T(256)(128)(2,1)}, u32[]{:S(2)}) copy-start(bf16[256]{0:T(256)(128)(2,1)} %param.36) | copy-start | bytes 1540
  132.0 15.2 %all-to-all-start.7 = ((bf16[16,8,256]{2,1,0:T(8,128)(2,1)}), bf16[16,8,256]{2,1,0:T(8,128)(2,1)S(1)}, u32[]{:S(2)}, u32[]{:S(2)}) async-start(bf16[16,8,256]{2,1,0:T(8,128)(2,1)} %shard_map.210), calls=%async_computation.7 | async-start | bytes 131072 | tf_op jit(solution)/shard_map/all_to_all | solution.py:34
  153.3 22.2 %slice-start = ((s8[17301504]{0:T(1024)(128)(4,1)}), s8[4194304]{0:T(1024)(128)(4,1)S(1)}, s32[]{:S(2)}) async-start(s8[17301504]{0:T(1024)(128)(4,1)} %bitcast.28), calls=%async_computation.11 | async-start | bytes 8388608
  165.0 10.5 %slice-start.1 = ((s8[17301504]{0:T(1024)(128)(4,1)}), s8[4194304]{0:T(1024)(128)(4,1)S(1)}, s32[]{:S(2)}) async-start(s8[17301504]{0:T(1024)(128)(4,1)} %bitcast.28), calls=%async_computation.12 | async-start | bytes 8388608
  165.0 10.5 %slice-start.2 = ((s8[17301504]{0:T(1024)(128)(4,1)}), s8[4194304]{0:T(1024)(128)(4,1)S(1)}, s32[]{:S(2)}) async-start(s8[17301504]{0:T(1024)(128)(4,1)} %bitcast.28), calls=%async_computation.13 | async-start | bytes 8388608
  165.0 10.5 %slice-start.3 = ((s8[17301504]{0:T(1024)(128)(4,1)}), s8[4194304]{0:T(1024)(128)(4,1)S(1)}, s32[]{:S(2)}) async-start(s8[17301504]{0:T(1024)(128)(4,1)} %bitcast.28), calls=%async_computation.14 | async-start | bytes 8388608
  165.0 10.5 %slice-start.4 = ((s8[17301504]{0:T(1024)(128)(4,1)}), s8[524288]{0:T(1024)(128)(4,1)S(1)}, s32[]{:S(2)}) async-start(s8[17301504]{0:T(1024)(128)(4,1)} %bitcast.28), calls=%async_computation.15 | async-start | bytes 1048576
  (2 other events, 4.5 us)
Sparse Core Ops, SparseCore 0:
  10.1 121.4 all-gather.2

commit v8 on v7

--- a/solution.py
+++ b/solution.py
@@ -55,6 +55,29 @@
         compiler_params=pltpu.CompilerParams(vmem_limit_bytes=limit),
         cost_estimate=cost,
     )(*args)
+
+
+def join_kernel(*refs):
+    parts, out_ref, sems = refs[:-2], refs[-2], refs[-1]
+    copies, at = [], 0
+    for i, part in enumerate(parts):
+        rows = part.shape[0]
+        copies.append(pltpu.make_async_copy(part, out_ref.at[pl.ds(at, rows)], sems.at[i]))
+        copies[-1].start()
+        at += rows
+    for copy in copies:
+        copy.wait()
+
+
+def joined(*parts):
+    rows, width = sum(part.shape[0] for part in parts), parts[0].shape[1]
+    return pl.pallas_call(
+        join_kernel,
+        out_shape=jax.ShapeDtypeStruct((rows, width), parts[0].dtype),
+        in_specs=[pl.BlockSpec(memory_space=pl.ANY)] * len(parts),
+        out_specs=pl.BlockSpec(memory_space=pl.ANY),
+        scratch_shapes=[pltpu.SemaphoreType.DMA((len(parts),))],
+    )(*parts)
 
 
 def rows_of(ref):
@@ -276,7 +299,7 @@
     wide = (n, rows, 4 * PAD)
     narrow = (n, rows, 2 * PAD)
 
-    later = jnp.concatenate([w_gate_post.T, w_up_post.T, w_down_post], axis=0)
+    later = joined(w_gate_post.T, w_up_post.T, w_down_post)
     later = lax.all_gather(later, TP, axis=0, tiled=False)
 
     gate_t, up_t = w_gate_pre.T, w_up_pre.T

time: 187 us -> 202 us (1.080)
  Pallas kernels: 14.2 us -> 31.7 us
  other arithmetic: 2.18 us -> 0.08 us
    pallas_call x0 -> x1, Pallas kernels: none -> 17.5 us  [joined(): pl.pallas_call(join_kernel, out_shape=jax.ShapeDtypeStruct((rows, width),...]
    concatenate x1 -> x0, other arithmetic: 2.1 us -> none  [on_device(): later = jnp.concatenate([w_gate_post.T, w_up_post.T, w_down_post], axis=0)]
where the time goes in v8:
time: 202 us; the launch traced here: 199 us
  blocking collectives  63.1 us (31%)
  starting transfers between devices  46.2 us (23%)
  waiting for transfers between devices  41.1 us (20%)
  Pallas kernels  31.7 us (16%)
  between operations  15.7 us (8%)
    all_to_all x5, blocking collectives, exchanged(): return lax.all_to_all(parts, axis, 0, 0, tiled=True)  63.1 us
    all_to_all x5, waiting for transfers between devices, exchanged(): return lax.all_to_all(parts, axis, 0, 0, tiled=True)  40.8 us
    all_to_all x5, starting transfers between devices, exchanged(): return lax.all_to_all(parts, axis, 0, 0, tiled=True)  30.3 us
    pallas_call x1, Pallas kernels, joined(): pl.pallas_call(join_kernel, out_shape=jax.ShapeDtypeStruct((rows, width),...  17.5 us
    ppermute x2, starting transfers between devices, from_partner(): return lax.ppermute(x, 'core', [(0, 1), (1, 0)])  15.9 us
    pallas_call x11, Pallas kernels, local_call(): pl.pallas_call(kernel, out_shape=outs, in_specs=specs, out_specs=tuple((p...  14.2 us
  transfers between devices with their start and end apart: 8, of which 6 were waited for; matrix products, arithmetic and copies ran while one was open for 1% of the time, Pallas kernels for 3%

profile of v8, /device:TPU:1, one launch (start us, length us, event | category | flops | bytes accessed | tf_op | source)
XLA Modules:
  0.0 199.3 jit_solution(14569270522226642399)
XLA Ops:
  7.3 17.5 %shard_map.211 = bf16[1056,256]{1,0:T(8,128)(2,1)} custom-call(bf16[352,256]{1,0:T(8,128)(2,1)} %bitcast.41, bf16[352,256]{1,0:T(8,128)(2,1)} %bitcast.42, bf16[352,256]{1,0:T(8,128)(2,1)} %refs_2_.1), custom_call_target="tpu_custom_call" | custom-call | tf_op jit(solution)/shard_map/pallas_call | solution.py:74
  24.9 8.7 %collective-permute-start = (bf16[1184,256]{1,0:T(8,128)(2,1)S(1)}, bf16[1184,256]{1,0:T(8,128)(2,1)S(1)}, u32[]{:S(2)}, u32[]{:S(2)}) collective-permute-start(bf16[1184,256]{1,0:T(8,128)(2,1)S(1)} %pad_maximum_fusion), channel_id=1, source_target_pairs={{0,1},{1,0},{2,3},{3,2},{4,5},{5,4},{6,7},{7,6},{8,9},{9,8},{10,11... | collective-permute-start | bytes 1818632 | tf_op jit(solution)/shard_map/ppermute | solution.py:38
  34.3 9.6 %all-to-all-start = ((bf16[16,8,256]{2,1,0:T(8,128)(2,1)}), bf16[16,8,256]{2,1,0:T(8,128)(2,1)S(1)}, u32[]{:S(2)}, u32[]{:S(2)}) async-start(bf16[16,8,256]{2,1,0:T(8,128)(2,1)} %broadcast_in_dim.24), calls=%async_computation | async-start | bytes 131072 | tf_op jit(solution)/shard_map/all_to_all | solution.py:34
  43.9 11.6 %all-to-all-done.rows_ref = bf16[16,8,256]{2,1,0:T(8,128)(2,1)S(1)} async-done(((bf16[16,8,256]{2,1,0:T(8,128)(2,1)}), bf16[16,8,256]{2,1,0:T(8,128)(2,1)S(1)}, u32[]{:S(2)}, u32[]{:S(2)}) %all-to-all-start) | async-done | bytes 65568 | tf_op jit(solution)/shard_map/all_to_all | solution.py:34
  55.9 14.8 %all_to_all.50.parts_ref = bf16[16,8,1536]{2,1,0:T(8,128)(2,1)S(1)} all-to-all(bf16[16,8,1536]{2,1,0:T(8,128)(2,1)S(1)} %shard_map.203), channel_id=1, replica_groups=mesh['kv_0'=4,'kv_1'=4,'z'=16,'core'=2] {'kv_0','kv_1'}, dimensions={0} | all-to-all | bytes 786432 | tf_op jit(solution)/shard_map/all_to_all | solution.py:34
  70.9 10.0 %all_to_all.51.hidden_ref = bf16[16,8,768]{2,1,0:T(8,128)(2,1)S(1)} all-to-all(bf16[16,8,768]{2,1,0:T(8,128)(2,1)S(1)} %shard_map.204), channel_id=1, replica_groups=mesh['kv_0'=4,'kv_1'=4,'z'=16,'core'=2] {'kv_0','kv_1'}, dimensions={0} | all-to-all | bytes 393216 | tf_op jit(solution)/shard_map/all_to_all | solution.py:34
  81.2 16.2 %all_to_all.52.parts_ref = bf16[16,8,256]{2,1,0:T(8,128)(2,1)S(1)} all-to-all(bf16[16,8,256]{2,1,0:T(8,128)(2,1)S(1)} %shard_map.205), channel_id=1, replica_groups=mesh['kv_0'=4,'kv_1'=4,'z'=16,'core'=2] {'z'}, dimensions={0} | all-to-all | bytes 131072 | tf_op jit(solution)/shard_map/all_to_all | solution.py:34
  98.1 3.5 %all-to-all-start.4 = ((bf16[16,8,256]{2,1,0:T(8,128)(2,1)}), bf16[16,8,256]{2,1,0:T(8,128)(2,1)S(1)}, u32[]{:S(2)}, u32[]{:S(2)}) async-start(bf16[16,8,256]{2,1,0:T(8,128)(2,1)} %get-tuple-element.12), calls=%async_computation.4 | async-start | bytes 131072 | tf_op jit(solution)/shard_map/all_to_all | solution.py:34
  101.7 7.2 %collective-permute-start.1 = (bf16[256,384]{1,0:T(8,128)(2,1)S(1)}, bf16[256,384]{1,0:T(8,128)(2,1)S(1)}, u32[]{:S(2)}, u32[]{:S(2)}) collective-permute-start(bf16[256,384]{1,0:T(8,128)(2,1)S(1)} %pad_maximum_fusion.1), channel_id=1, source_target_pairs={{0,1},{1,0},{2,3},{3,2},{4,5},{5,4},{6,7},{7,6},{8,9},{9,8},{10,11... | collective-permute-start | bytes 589832 | tf_op jit(solution)/shard_map/ppermute | solution.py:38
  109.9 3.9 %all-to-all-done.4.rows_ref = bf16[16,8,256]{2,1,0:T(8,128)(2,1)S(1)} async-done(((bf16[16,8,256]{2,1,0:T(8,128)(2,1)}), bf16[16,8,256]{2,1,0:T(8,128)(2,1)S(1)}, u32[]{:S(2)}, u32[]{:S(2)}) %all-to-all-start.4) | async-done | bytes 65568 | tf_op jit(solution)/shard_map/all_to_all | solution.py:34
  113.7 1.1 shard_map.207
  114.8 9.9 %all-to-all-start.5 = ((bf16[32,8,512]{2,1,0:T(8,128)(2,1)}), bf16[32,8,512]{2,1,0:T(8,128)(2,1)S(1)}, u32[]{:S(2)}, u32[]{:S(2)}) async-start(bf16[32,8,512]{2,1,0:T(8,128)(2,1)} %bitcast.5), calls=%async_computation.5 | async-start | bytes 524288 | tf_op jit(solution)/shard_map/all_to_all | solution.py:34
  126.0 7.7 %all-to-all-done.5 = bf16[32,8,512]{2,1,0:T(8,128)(2,1)S(1)} async-done(((bf16[32,8,512]{2,1,0:T(8,128)(2,1)}), bf16[32,8,512]{2,1,0:T(8,128)(2,1)S(1)}, u32[]{:S(2)}, u32[]{:S(2)}) %all-to-all-start.5) | async-done | bytes 262176 | tf_op jit(solution)/shard_map/all_to_all | solution.py:34
  133.7 1.8 shard_map.208
  135.5 3.8 %all-to-all-start.6 = ((bf16[32,8,128]{2,1,0:T(8,128)(2,1)}), bf16[32,8,128]{2,1,0:T(8,128)(2,1)S(1)}, u32[]{:S(2)}, u32[]{:S(2)}) async-start(bf16[32,8,128]{2,1,0:T(8,128)(2,1)} %bitcast.11), calls=%async_computation.6 | async-start | bytes 131072 | tf_op jit(solution)/shard_map/all_to_all | solution.py:34
  139.3 1.4 shard_map.209
  140.7 5.9 %all-to-all-done.6 = bf16[32,8,128]{2,1,0:T(8,128)(2,1)S(1)} async-done(((bf16[32,8,128]{2,1,0:T(8,128)(2,1)}), bf16[32,8,128]{2,1,0:T(8,128)(2,1)S(1)}, u32[]{:S(2)}, u32[]{:S(2)}) %all-to-all-start.6) | async-done | bytes 65568 | tf_op jit(solution)/shard_map/all_to_all | solution.py:34
  146.6 0.8 shard_map.210
  147.4 3.5 %all-to-all-start.7 = ((bf16[16,8,256]{2,1,0:T(8,128)(2,1)}), bf16[16,8,256]{2,1,0:T(8,128)(2,1)S(1)}, u32[]{:S(2)}, u32[]{:S(2)}) async-start(bf16[16,8,256]{2,1,0:T(8,128)(2,1)} %shard_map.210), calls=%async_computation.7 | async-start | bytes 131072 | tf_op jit(solution)/shard_map/all_to_all | solution.py:34
  151.0 11.6 %all-to-all-done.7.parts_ref = bf16[16,8,256]{2,1,0:T(8,128)(2,1)S(1)} async-done(((bf16[16,8,256]{2,1,0:T(8,128)(2,1)}), bf16[16,8,256]{2,1,0:T(8,128)(2,1)S(1)}, u32[]{:S(2)}, u32[]{:S(2)}) %all-to-all-start.7) | async-done | bytes 65568 | tf_op jit(solution)/shard_map/all_to_all | solution.py:34
  162.6 6.1 %shard_map.212 = (bf16[16,8,1536]{2,1,0:T(8,128)(2,1)S(1)}, bf16[8,256]{1,0:T(8,128)(2,1)S(1)}) custom-call(bf16[16,8,256]{2,1,0:T(8,128)(2,1)S(1)} %all-to-all-done.7.parts_ref, bf16[8,256]{1,0:T(8,128)(2,1)S(1)} %get-tuple-element.18.first_ref, bf16[1,256]{1,0:T(2,128)(2,1)S(1)} %broadcast_in_dim.30.gain_ref, bf16[32,1056,256]{2,1,0:T(8,128)(2,1)} %bitcast.23), custom_call_target="tpu_custom_call" | custom-call | tf_op jit(solution)/shard_map/pallas_call | solution.py:49
  168.7 11.7 %all_to_all.53.parts_ref = bf16[16,8,1536]{2,1,0:T(8,128)(2,1)S(1)} all-to-all(bf16[16,8,1536]{2,1,0:T(8,128)(2,1)S(1)} %get-tuple-element.19), channel_id=1, replica_groups=mesh['kv_0'=4,'kv_1'=4,'z'=16,'core'=2] {'kv_0','kv_1'}, dimensions={0} | all-to-all | bytes 786432 | tf_op jit(solution)/shard_map/all_to_all | solution.py:34
  180.7 10.3 %all_to_all.54.hidden_ref = bf16[16,8,768]{2,1,0:T(8,128)(2,1)S(1)} all-to-all(bf16[16,8,768]{2,1,0:T(8,128)(2,1)S(1)} %shard_map.213), channel_id=1, replica_groups=mesh['kv_0'=4,'kv_1'=4,'z'=16,'core'=2] {'kv_0','kv_1'}, dimensions={0} | all-to-all | bytes 393216 | tf_op jit(solution)/shard_map/all_to_all | solution.py:34
  191.0 1.5 shard_map.214
  (55 shorter events, 3.5 us)
Async XLA Ops:
  7.2 17.6 %copy-start.7 = (bf16[128,256]{1,0:T(8,128)(2,1)S(1)}, bf16[128,256]{1,0:T(8,128)(2,1)}, u32[]{:S(2)}) copy-start(bf16[128,256]{1,0:T(8,128)(2,1)} %own_ref.5) | copy-start | bytes 196612
  7.2 17.6 %copy-start.3 = (bf16[352,256]{1,0:T(8,128)(2,1)S(1)}, bf16[352,256]{1,0:T(8,128)(2,1)}, u32[]{:S(2)}) copy-start(bf16[352,256]{1,0:T(8,128)(2,1)} %own_ref.3) | copy-start | bytes 540676
  7.2 17.6 %copy-start.2 = (bf16[256,352]{0,1:T(8,128)(2,1)S(1)}, bf16[256,352]{0,1:T(8,128)(2,1)}, u32[]{:S(2)}) copy-start(bf16[256,352]{0,1:T(8,128)(2,1)} %param.24) | copy-start | bytes 540676
  7.2 17.6 %copy-start.1 = (bf16[256,352]{0,1:T(8,128)(2,1)S(1)}, bf16[256,352]{0,1:T(8,128)(2,1)}, u32[]{:S(2)}) copy-start(bf16[256,352]{0,1:T(8,128)(2,1)} %param.23) | copy-start | bytes 540676
  7.2 155.4 %all-gather.3.cloned.1.call-start = ((), (), s32[]{:S(2)}) async-start(), calls=%async_computation.10 | async-start | bytes 17842176 | tf_op jit(solution)/shard_map/all_gather | solution.py:303
  7.3 26.4 %copy-start.8 = (bf16[8,256]{1,0:T(8,128)(2,1)S(1)}, bf16[8,256]{1,0:T(8,128)(2,1)}, u32[]{:S(2)}) copy-start(bf16[8,256]{1,0:T(8,128)(2,1)} %own_ref.4) | copy-start | bytes 12292
  24.8 19.1 %copy-start.10 = (bf16[256]{0:T(256)(128)(2,1)S(1)}, bf16[256]{0:T(256)(128)(2,1)}, u32[]{:S(2)}) copy-start(bf16[256]{0:T(256)(128)(2,1)} %param.22) | copy-start | bytes 1540
  24.9 30.6 %collective-permute-start = (bf16[1184,256]{1,0:T(8,128)(2,1)S(1)}, bf16[1184,256]{1,0:T(8,128)(2,1)S(1)}, u32[]{:S(2)}, u32[]{:S(2)}) collective-permute-start(bf16[1184,256]{1,0:T(8,128)(2,1)S(1)} %pad_maximum_fusion), channel_id=1, source_target_pairs={{0,1},{1,0},{2,3},{3,2},{4,5},{5,4},{6,7},{7,6},{8,9},{9,8},{10,11... | collective-permute-start | bytes 1818632 | tf_op jit(solution)/shard_map/ppermute | solution.py:38
  34.3 21.2 %all-to-all-start = ((bf16[16,8,256]{2,1,0:T(8,128)(2,1)}), bf16[16,8,256]{2,1,0:T(8,128)(2,1)S(1)}, u32[]{:S(2)}, u32[]{:S(2)}) async-start(bf16[16,8,256]{2,1,0:T(8,128)(2,1)} %broadcast_in_dim.24), calls=%async_computation | async-start | bytes 131072 | tf_op jit(solution)/shard_map/all_to_all | solution.py:34
  70.7 30.9 %copy-start.4 = (bf16[256,128]{1,0:T(8,128)(2,1)S(1)}, bf16[256,128]{1,0:T(8,128)(2,1)}, u32[]{:S(2)}) copy-start(bf16[256,128]{1,0:T(8,128)(2,1)} %q_ref.1) | copy-start | bytes 196612
  70.7 30.9 %copy-start.5 = (bf16[256,128]{1,0:T(8,128)(2,1)S(1)}, bf16[256,128]{1,0:T(8,128)(2,1)}, u32[]{:S(2)}) copy-start(bf16[256,128]{1,0:T(8,128)(2,1)} %k_ref.1) | copy-start | bytes 196612
  70.7 30.9 %copy-start.6 = (bf16[256,128]{1,0:T(8,128)(2,1)S(1)}, bf16[256,128]{1,0:T(8,128)(2,1)}, u32[]{:S(2)}) copy-start(bf16[256,128]{1,0:T(8,128)(2,1)} %v_ref.1) | copy-start | bytes 196612
  70.9 37.9 %copy-start.11 = (bf16[256]{0:T(256)(128)(2,1)S(1)}, bf16[256]{0:T(256)(128)(2,1)}, u32[]{:S(2)}) copy-start(bf16[256]{0:T(256)(128)(2,1)} %param.26) | copy-start | bytes 1540
  81.2 52.6 %copy-start = (f32[16,1,128,128]{3,2,1,0:T(8,128)S(1)}, f32[16,1,128,128]{3,2,1,0:T(8,128)}, u32[]{:S(2)}) copy-start(f32[16,1,128,128]{3,2,1,0:T(8,128)} %param.21) | copy-start | bytes 3145732
  81.2 52.6 %copy-start.9 = (bf16[128]{0:T(256)(128)(2,1)S(1)}, bf16[128]{0:T(256)(128)(2,1)}, u32[]{:S(2)}) copy-start(bf16[128]{0:T(256)(128)(2,1)} %param.34) | copy-start | bytes 772
  98.1 15.7 %all-to-all-start.4 = ((bf16[16,8,256]{2,1,0:T(8,128)(2,1)}), bf16[16,8,256]{2,1,0:T(8,128)(2,1)S(1)}, u32[]{:S(2)}, u32[]{:S(2)}) async-start(bf16[16,8,256]{2,1,0:T(8,128)(2,1)} %get-tuple-element.12), calls=%async_computation.4 | async-start | bytes 131072 | tf_op jit(solution)/shard_map/all_to_all | solution.py:34
  101.7 8.2 %collective-permute-start.1 = (bf16[256,384]{1,0:T(8,128)(2,1)S(1)}, bf16[256,384]{1,0:T(8,128)(2,1)S(1)}, u32[]{:S(2)}, u32[]{:S(2)}) collective-permute-start(bf16[256,384]{1,0:T(8,128)(2,1)S(1)} %pad_maximum_fusion.1), channel_id=1, source_target_pairs={{0,1},{1,0},{2,3},{3,2},{4,5},{5,4},{6,7},{7,6},{8,9},{9,8},{10,11... | collective-permute-start | bytes 589832 | tf_op jit(solution)/shard_map/ppermute | solution.py:38
  114.8 18.9 %all-to-all-start.5 = ((bf16[32,8,512]{2,1,0:T(8,128)(2,1)}), bf16[32,8,512]{2,1,0:T(8,128)(2,1)S(1)}, u32[]{:S(2)}, u32[]{:S(2)}) async-start(bf16[32,8,512]{2,1,0:T(8,128)(2,1)} %bitcast.5), calls=%async_computation.5 | async-start | bytes 524288 | tf_op jit(solution)/shard_map/all_to_all | solution.py:34
  135.5 11.1 %all-to-all-start.6 = ((bf16[32,8,128]{2,1,0:T(8,128)(2,1)}), bf16[32,8,128]{2,1,0:T(8,128)(2,1)S(1)}, u32[]{:S(2)}, u32[]{:S(2)}) async-start(bf16[32,8,128]{2,1,0:T(8,128)(2,1)} %bitcast.11), calls=%async_computation.6 | async-start | bytes 131072 | tf_op jit(solution)/shard_map/all_to_all | solution.py:34
  139.3 11.6 %copy-start.12 = (bf16[256]{0:T(256)(128)(2,1)S(1)}, bf16[256]{0:T(256)(128)(2,1)}, u32[]{:S(2)}) copy-start(bf16[256]{0:T(256)(128)(2,1)} %param.36) | copy-start | bytes 1540
  147.4 15.2 %all-to-all-start.7 = ((bf16[16,8,256]{2,1,0:T(8,128)(2,1)}), bf16[16,8,256]{2,1,0:T(8,128)(2,1)S(1)}, u32[]{:S(2)}, u32[]{:S(2)}) async-start(bf16[16,8,256]{2,1,0:T(8,128)(2,1)} %shard_map.210), calls=%async_computation.7 | async-start | bytes 131072 | tf_op jit(solution)/shard_map/all_to_all | solution.py:34
  168.7 22.2 %slice-start = ((s8[17301504]{0:T(1024)(128)(4,1)}), s8[4194304]{0:T(1024)(128)(4,1)S(1)}, s32[]{:S(2)}) async-start(s8[17301504]{0:T(1024)(128)(4,1)} %bitcast.28), calls=%async_computation.11 | async-start | bytes 8388608
  180.5 10.5 %slice-start.3 = ((s8[17301504]{0:T(1024)(128)(4,1)}), s8[4194304]{0:T(1024)(128)(4,1)S(1)}, s32[]{:S(2)}) async-start(s8[17301504]{0:T(1024)(128)(4,1)} %bitcast.28), calls=%async_computation.14 | async-start | bytes 8388608
  180.5 10.5 %slice-start.4 = ((s8[17301504]{0:T(1024)(128)(4,1)}), s8[524288]{0:T(1024)(128)(4,1)S(1)}, s32[]{:S(2)}) async-start(s8[17301504]{0:T(1024)(128)(4,1)} %bitcast.28), calls=%async_computation.15 | async-start | bytes 1048576
  (2 other events, 21.1 us)
Sparse Core Ops, SparseCore 0:
  24.9 121.5 all-gather.2
